TPU v7x, 128 devices: a 2x2x16 block of a 8x8x16 slice. The times are simulated.
128 devices in a mesh: grp: 4 (over y, x), ep: 32 (over z, core).
Axes of the slice: x: 2, y: 2, z: 16, core: 2. Of those that a mesh axis runs over, the one named last changes fastest.
The devices are a block of a 8x8x16 slice.
Arguments:
- hidden: bfloat16 [384, 2048], P(('grp', 'ep')), parts along dimension 0, may hold values from -6 to 6
- conv_window: bfloat16 [384, 3, 6144], P(('grp', 'ep')), parts along dimension 0, may hold values from -6 to 6
- ssm_state: float32 [384, 64, 64, 128], P(('grp', 'ep')), parts along dimension 0, may hold values from -1.75 to 1.75
- gate_proj: bfloat16 [2048, 4096], P(None, 'ep'), may hold values from -0.125 to 0.125
- input_proj: bfloat16 [2048, 4096], P(None, 'ep'), may hold values from -0.125 to 0.125
- write_proj: bfloat16 [2048, 1024], P(None, 'ep'), may hold values from -0.125 to 0.125
- read_proj: bfloat16 [2048, 1024], P(None, 'ep'), may hold values from -0.125 to 0.125
- step_proj: bfloat16 [2048, 64], replicated, may hold values from -0.125 to 0.125
- step_bias: float32 [64], replicated, may hold values from -2 to 1
- decay_log: float32 [64], replicated, may hold values from -2.3 to 1.4
- decay_shift: float32 [384, 64], P(('grp', 'ep')), parts along dimension 0, may hold values from -0.7 to 0
- skip_scale: float32 [64], replicated, may hold values from -4 to 4
- conv_taps: bfloat16 [4, 6144], replicated, may hold values from -3 to 3
- conv_bias: float32 [6144], replicated, may hold values from -3 to 3
- mix_gain: float32 [2048], replicated, may hold values from 0.1 to 1.9
- group_gain: float32 [4096], replicated, may hold values from 0.1 to 1.9
- out_proj: bfloat16 [4096, 2048], P(None, 'ep'), may hold values from -0.09375 to 0.09375
- ffn_gain: float32 [2048], replicated, may hold values from 0.1 to 1.9
- router: bfloat16 [2048, 32], replicated, may hold values from -0.125 to 0.125
- expert_ids: int32 [384, 6], P(('grp', 'ep')), parts along dimension 0, may hold values from 0 to 31, all different within a row; in each aligned block of 3 rows (0 to 2, 3 to 5, ...) at most 2 rows name the same one
- expert_gate: bfloat16 [32, 2048, 512], P('ep'), may hold values from -0.125 to 0.125
- expert_up: bfloat16 [32, 2048, 512], P('ep'), may hold values from -0.125 to 0.125
- expert_down: bfloat16 [32, 512, 2048], P('ep'), may hold values from -0.25 to 0.25
- shared_gate: bfloat16 [2048, 512], P('ep'), may hold values from -0.125 to 0.125
- shared_up: bfloat16 [2048, 512], P('ep'), may hold values from -0.125 to 0.125
- shared_down: bfloat16 [512, 2048], replicated, may hold values from -0.25 to 0.25
Outputs:
- layer_out: bfloat16 [384, 2048], P(('grp', 'ep')), parts along dimension 0
- next_state: float32 [384, 64, 64, 128], P(('grp', 'ep')), parts along dimension 0
- next_window: bfloat16 [384, 3, 6144], P(('grp', 'ep')), parts along dimension 0
There are 4 independent parts, one for each index of `grp`. A program takes and returns all parts, laid end to end along the dimension named above; an argument that names none is the same for every part. Nothing has to cross between parts.
Inputs may be any that keep to these rules, and one draw needn't show every extreme that they name: `expert_ids`: each row names 6 different experts; in the rows of one device no expert is named by more than 2 rows, and in every draw some device's rows name some expert exactly 2 times.
All inputs are finite; a program needn't handle non-finite values.
Results may differ from a plain program's by a relative error of at most 0.019.
Values may be sent and summed in bfloat16 or wider, within the bound.
No kernel may reach another device: no remote copies, remote signals or barrier semaphores. Data moves between devices by JAX's collectives and lax.ppermute only.
A program may use at most 128 MiB of HBM per device.

v0:
```python
import jax
import jax.numpy as jnp
from jax import lax
from jax.sharding import Mesh
from jax.sharding import PartitionSpec as P

HEAD_DIM = 64
GROUPS = 8
STATE = 128
CAP = 2
EP = ("ep_0", "ep_1")
GRP_EP = ("grp", "ep_0", "ep_1")


epsilon = 1e-06
routed_scale = 2.5


def from_everyone(shard, axis):
    count = lax.axis_size(axis)
    return lax.all_to_all(
        jnp.broadcast_to(shard[None], (count, *shard.shape)), axis, 0, 0, tiled=True
    )


def in_order(pieces, dim):
    dims = list(pieces.shape[1:])
    dims[dim] *= pieces.shape[0]
    return jnp.moveaxis(pieces, 0, dim).reshape(dims)


def gathered_copies(shard, axis, dim):
    pieces = from_everyone(shard, axis)
    return in_order(pieces, dim)


def all_blocks(shard, axes, turns):
    pieces = shard
    for k in turns:
        pieces = lax.all_gather(pieces, axes[k])
    done = turns[::-1]
    back = [done.index(k) for k in range(len(axes))]
    pieces = pieces.transpose(*back, *range(len(axes), pieces.ndim))
    return pieces.reshape(-1, *shard.shape)


def whole_of(shard, axes, turns, dim):
    return in_order(all_blocks(shard, axes, turns), dim)


def cut_along(shard, dim, count):
    before, after = (shard.shape[:dim], shard.shape[dim + 1 :])
    return jnp.moveaxis(shard.reshape(*before, count, -1, *after), dim, 0)


def summed_on_arrival(shard, axis, dim):
    pieces = cut_along(shard, dim, lax.axis_size(axis))
    arrived = lax.all_to_all(pieces, axis, split_axis=0, concat_axis=0, tiled=True)
    return arrived.astype(jnp.float32).sum(axis=0)


def row_scale(values):
    return lax.rsqrt(jnp.mean(values * values, axis=-1, keepdims=True) + epsilon)


def matmul(left, right):
    return jnp.dot(left, right, preferred_element_type=jnp.float32)


def expert_result(rows_in, weight_gate, weight_up, weight_down):
    expert_hidden = (jax.nn.silu(matmul(rows_in, weight_gate)) * matmul(rows_in, weight_up)).astype(
        jnp.bfloat16
    )
    return matmul(expert_hidden, weight_down).astype(jnp.bfloat16)


def route_weights(routed_in, router, chosen):
    scores = jax.nn.sigmoid(matmul(routed_in, router))
    picked = jnp.take_along_axis(scores, chosen, axis=1)
    return routed_scale * picked / jnp.sum(picked, axis=1, keepdims=True)


def shards(
    hidden,
    conv_window,
    ssm_state,
    gate_proj,
    input_proj,
    write_proj,
    read_proj,
    step_proj,
    step_bias,
    decay_log,
    decay_shift,
    skip_scale,
    conv_taps,
    conv_bias,
    mix_gain,
    group_gain,
    out_proj,
    ffn_gain,
    router,
    expert_ids,
    expert_gate,
    expert_up,
    expert_down,
    shared_gate,
    shared_up,
    shared_down,
):
    local_rows = hidden.shape[0]
    device_index = lax.axis_index(EP)
    gathered = gathered_copies(hidden, EP, 0)
    gathered_wide = gathered.astype(jnp.float32)
    normed = (gathered_wide * row_scale(gathered_wide) * mix_gain).astype(jnp.bfloat16)
    gate_part = matmul(normed, gate_proj).astype(jnp.bfloat16)
    input_part = matmul(normed, input_proj).astype(jnp.bfloat16)
    write_part = matmul(normed, write_proj).astype(jnp.bfloat16)
    read_part = matmul(normed, read_proj).astype(jnp.bfloat16)
    gate_rows, input_rows, write_rows, read_rows = (
        lax.all_to_all(gate_part, EP, split_axis=0, concat_axis=1, tiled=True),
        lax.all_to_all(input_part, EP, split_axis=0, concat_axis=1, tiled=True),
        lax.all_to_all(write_part, EP, split_axis=0, concat_axis=1, tiled=True),
        lax.all_to_all(read_part, EP, split_axis=0, concat_axis=1, tiled=True),
    )
    normed_local = lax.dynamic_slice_in_dim(normed, device_index * local_rows, local_rows, 0)
    step_raw = matmul(normed_local, step_proj)
    inner_width = gate_rows.shape[1]
    state_span = GROUPS * STATE
    head_count = step_bias.shape[0]
    per_group = head_count // GROUPS
    fresh_row = jnp.concatenate([input_rows, write_rows, read_rows], axis=1)
    window = jnp.concatenate([conv_window, fresh_row[:, None, :]], axis=1)
    convolved = jax.nn.silu(
        jnp.sum(window.astype(jnp.float32) * conv_taps.astype(jnp.float32)[None], axis=1)
        + conv_bias
    )
    head_input = convolved[:, :inner_width].reshape(local_rows, GROUPS, per_group, HEAD_DIM)
    write_vec = convolved[:, inner_width : inner_width + state_span].reshape(
        local_rows, GROUPS, STATE
    )
    read_vec = convolved[:, inner_width + state_span :].reshape(local_rows, GROUPS, STATE)
    step_size = jax.nn.softplus(step_raw + step_bias)
    decay_rate = jnp.exp(decay_shift - step_size * jnp.exp(decay_log)).reshape(
        local_rows, GROUPS, per_group
    )
    step_group = step_size.reshape(local_rows, GROUPS, per_group)
    carried = ssm_state.reshape(local_rows, GROUPS, per_group, HEAD_DIM, STATE)
    next_state = (
        decay_rate[..., None, None] * carried
        + (step_group[..., None] * head_input)[..., None] * write_vec[:, :, None, None, :]
    )
    mixed_out = jnp.einsum("sgepn,sgn->sgep", next_state, read_vec)
    mixed_out = mixed_out + skip_scale.reshape(GROUPS, per_group)[None, :, :, None] * head_input
    mixed_out = mixed_out.reshape(local_rows, inner_width).astype(jnp.bfloat16)
    gated_out = mixed_out.astype(jnp.float32) * jax.nn.silu(gate_rows.astype(jnp.float32))
    blocks = gated_out.reshape(local_rows, GROUPS, -1)
    gated_out = ((blocks * row_scale(blocks)).reshape(local_rows, inner_width) * group_gain).astype(
        jnp.bfloat16
    )
    col_width = out_proj.shape[1]
    resid_cols = lax.dynamic_slice_in_dim(gathered_wide, device_index * col_width, col_width, 1)
    resid_part = (resid_cols + matmul(whole_of(gated_out, EP, (0, 1), 0), out_proj)).astype(
        jnp.bfloat16
    )
    gain_part = lax.dynamic_slice_in_dim(ffn_gain, device_index * col_width, col_width, 0)
    shared_part = (resid_part.astype(jnp.float32) * gain_part).astype(jnp.bfloat16)
    shared_pre = summed_on_arrival(
        jnp.concatenate(
            [matmul(shared_part, shared_gate), matmul(shared_part, shared_up)], axis=1
        ).astype(jnp.bfloat16),
        EP,
        0,
    )
    exp_dev = expert_gate.shape[0]
    resid = lax.all_to_all(resid_part, EP, split_axis=0, concat_axis=1, tiled=True)
    resid_wide = resid.astype(jnp.float32)
    norm_scale = row_scale(resid_wide)
    routed_in = (resid_wide * norm_scale * ffn_gain).astype(jnp.bfloat16)
    weights = route_weights(routed_in, router, expert_ids)
    expert_total = router.shape[1]
    member = jnp.any(
        expert_ids[:, :, None] == jnp.arange(expert_total, dtype=jnp.int32)[None, None, :], axis=1
    ).astype(jnp.int32)
    earlier = jnp.cumsum(member, axis=0) - member
    slot_index = jnp.take_along_axis(earlier, expert_ids, axis=1)
    places = expert_ids * CAP + slot_index
    dispatch_table = jnp.any(
        places[None, :, :] == jnp.arange(expert_total * CAP, dtype=jnp.int32)[:, None, None], axis=2
    ).astype(jnp.bfloat16)
    outbound = (
        matmul(dispatch_table, routed_in)
        .astype(jnp.bfloat16)
        .reshape(lax.axis_size(EP), exp_dev, CAP, routed_in.shape[1])
    )
    arrived = lax.all_to_all(outbound, EP, split_axis=0, concat_axis=0, tiled=True)
    rows_in = arrived[:, 0].reshape(-1, arrived.shape[-1])
    result = expert_result(rows_in, expert_gate[0], expert_up[0], expert_down[0])
    results = [result.reshape(arrived.shape[0], arrived.shape[2], arrived.shape[3])]
    returned = lax.all_to_all(
        jnp.stack(results, axis=1), EP, split_axis=0, concat_axis=0, tiled=True
    )
    returned_flat = returned.reshape(expert_total * CAP, returned.shape[-1])
    picked = jnp.take(returned_flat, places.reshape(-1), axis=0).reshape(
        local_rows, expert_ids.shape[1], returned.shape[-1]
    )
    routed = jnp.sum(picked.astype(jnp.float32) * weights[:, :, None], axis=1)
    hidden_units = shared_down.shape[0]
    shared_hidden = (
        jax.nn.silu(norm_scale * shared_pre[:, :hidden_units])
        * (norm_scale * shared_pre[:, hidden_units:])
    ).astype(jnp.bfloat16)
    layer_out = (resid_wide + routed + matmul(shared_hidden, shared_down)).astype(jnp.bfloat16)
    return (layer_out, next_state.reshape(ssm_state.shape), window[:, 1:])


def solution(mesh):
    torus = Mesh(mesh.devices.reshape(mesh.shape["grp"], 16, 2), ("grp", "ep_0", "ep_1"))
    return jax.shard_map(
        shards,
        mesh=torus,
        in_specs=(
            P(GRP_EP, None),
            P(GRP_EP, None, None),
            P(GRP_EP, None, None, None),
            P(None, EP),
            P(None, EP),
            P(None, EP),
            P(None, EP),
            P(),
            P(),
            P(),
            P(GRP_EP, None),
            P(),
            P(),
            P(),
            P(),
            P(),
            P(None, EP),
            P(),
            P(),
            P(GRP_EP, None),
            P(EP, None, None),
            P(EP, None, None),
            P(EP, None, None),
            P(EP, None),
            P(EP, None),
            P(),
        ),
        out_specs=(P(GRP_EP, None), P(GRP_EP, None, None, None), P(GRP_EP, None, None)),
        check_vma=False,
    )
```

profile of v0, /device:TPU:69, one launch (start us, length us, event | category | flops | bytes accessed | tf_op | source)
XLA Modules:
  0.0 271.9 jit_solution(13049437831377829950)
XLA Ops:
  0.7 1.9 broadcast_in_dim.11
  2.6 18.5 %all-to-all-start = ((bf16[32,3,2048]{2,1,0:T(4,128)(2,1)}), bf16[32,3,2048]{2,1,0:T(4,128)(2,1)S(1)}, u32[]{:S(2)}, u32[]{:S(2)}) async-start(bf16[32,3,2048]{2,1,0:T(4,128)(2,1)} %broadcast_in_dim.11), calls=%async_computation | async-start | bytes 1048576 | tf_op jit(solution)/shard_map/all_to_all | solution.py:21
  22.6 1.3 mul.284
  27.7 1.3 dynamic_slice.11
  30.3 24.1 %all-to-all-done = bf16[32,3,2048]{2,1,0:T(4,128)(2,1)S(1)} async-done(((bf16[32,3,2048]{2,1,0:T(4,128)(2,1)}), bf16[32,3,2048]{2,1,0:T(4,128)(2,1)S(1)}, u32[]{:S(2)}, u32[]{:S(2)}) %all-to-all-start) | async-done | bytes 393248 | tf_op jit(solution)/shard_map/all_to_all | solution.py:21
  57.9 4.2 %all-to-all-start.2 = ((bf16[32,3,32]{2,1,0:T(4,128)(2,1)}), bf16[32,3,32]{2,1,0:T(4,128)(2,1)S(1)}, u32[]{:S(2)}, u32[]{:S(2)}) async-start(bf16[32,3,32]{2,1,0:T(4,128)(2,1)} %all_to_all.79), calls=%async_computation.2 | async-start | bytes 65536 | tf_op jit(solution)/shard_map/all_to_all | solution.py:123
  62.2 1.3 convolution_convert_fusion.5
  63.5 1.3 convolution_convert_fusion.4
  66.7 7.6 %all-to-all-done.2 = bf16[32,3,32]{2,1,0:T(4,128)(2,1)S(1)} async-done(((bf16[32,3,32]{2,1,0:T(4,128)(2,1)}), bf16[32,3,32]{2,1,0:T(4,128)(2,1)S(1)}, u32[]{:S(2)}, u32[]{:S(2)}) %all-to-all-start.2) | async-done | bytes 6176 | tf_op jit(solution)/shard_map/all_to_all | solution.py:123
  74.3 5.1 %all-to-all-start.3 = ((bf16[32,3,32]{2,1,0:T(4,128)(2,1)}), bf16[32,3,32]{2,1,0:T(4,128)(2,1)S(1)}, u32[]{:S(2)}, u32[]{:S(2)}) async-start(bf16[32,3,32]{2,1,0:T(4,128)(2,1)} %all_to_all.83), calls=%async_computation.3 | async-start | bytes 65536 | tf_op jit(solution)/shard_map/all_to_all | solution.py:124
  82.0 9.2 %all-to-all-done.3 = bf16[32,3,32]{2,1,0:T(4,128)(2,1)S(1)} async-done(((bf16[32,3,32]{2,1,0:T(4,128)(2,1)}), bf16[32,3,32]{2,1,0:T(4,128)(2,1)S(1)}, u32[]{:S(2)}, u32[]{:S(2)}) %all-to-all-start.3) | async-done | bytes 6176 | tf_op jit(solution)/shard_map/all_to_all | solution.py:124
  91.2 4.9 %all-to-all-start.1 = ((bf16[32,3,128]{2,1,0:T(4,128)(2,1)}), bf16[32,3,128]{2,1,0:T(4,128)(2,1)S(1)}, u32[]{:S(2)}, u32[]{:S(2)}) async-start(bf16[32,3,128]{2,1,0:T(4,128)(2,1)} %all_to_all.75), calls=%async_computation.1 | async-start | bytes 65536 | tf_op jit(solution)/shard_map/all_to_all | solution.py:122
  96.5 11.7 %all-to-all-done.1 = bf16[32,3,128]{2,1,0:T(4,128)(2,1)S(1)} async-done(((bf16[32,3,128]{2,1,0:T(4,128)(2,1)}), bf16[32,3,128]{2,1,0:T(4,128)(2,1)S(1)}, u32[]{:S(2)}, u32[]{:S(2)}) %all-to-all-start.1) | async-done | bytes 24608 | tf_op jit(solution)/shard_map/all_to_all | solution.py:122
  108.3 4.8 %all-to-all-start.4 = ((bf16[32,3,128]{2,1,0:T(4,128)(2,1)}), bf16[32,3,128]{2,1,0:T(4,128)(2,1)S(1)}, u32[]{:S(2)}, u32[]{:S(2)}) async-start(bf16[32,3,128]{2,1,0:T(4,128)(2,1)} %all_to_all.87), calls=%async_computation.4 | async-start | bytes 65536 | tf_op jit(solution)/shard_map/all_to_all | solution.py:121
  115.4 9.8 %all-to-all-done.4 = bf16[32,3,128]{2,1,0:T(4,128)(2,1)S(1)} async-done(((bf16[32,3,128]{2,1,0:T(4,128)(2,1)}), bf16[32,3,128]{2,1,0:T(4,128)(2,1)S(1)}, u32[]{:S(2)}, u32[]{:S(2)}) %all-to-all-start.4) | async-done | bytes 24608 | tf_op jit(solution)/shard_map/all_to_all | solution.py:121
  125.4 4.7 %fusion = f32[3,8,1,8,64]{4,2,3,1,0:T(1,128)S(1)} fusion(f32[3,8,128,1,1]{2,3,4,1,0:T(1,128)S(1)} %bitcast.105, f32[3,8,8,64,128]{4,3,2,1,0:T(8,128)} %bitcast.96, f32[3,8,128]{2,1,0:T(8,128)S(1)} %bitcast.103, f32[3,8,8,64]{3,2,1,0:T(8,128)S(1)} %broadcast_multiply_fusion.1, f32[3,8,8]{2,1,0:T(8,128)S(1)} %mul.271), kind=kOutput, calls=%fused_computation.4 | convolution fusion | flops 7864320 | bytes 6415104 | tf_op jit(solution)/shard_map/sgepn,sgn->sgep/dot_general | solution.py:153
  131.4 22.4 %all_gather.10 = bf16[16,3,4096]{2,1,0:T(4,128)(2,1)S(1)} all-gather(bf16[1,3,4096]{2,1,0:T(4,128)(2,1)S(1)} %multiply_convert_fusion.1), channel_id=1, replica_groups=mesh['grp'=4,'ep_0'=16,'ep_1'=2] {'ep_0'}, dimensions={0}, use_global_device_ids=true | all-gather | bytes 417792 | tf_op jit(solution)/shard_map/all_gather | solution.py:40
  154.0 10.1 %all-gather = bf16[32,3,4096]{2,0,1:T(8,128)(2,1)S(1)} all-gather(bf16[16,3,4096]{2,0,1:T(8,128)(2,1)S(1)} %copy.71), channel_id=2, replica_groups=mesh['grp'=4,'ep_0'=16,'ep_1'=2] {'ep_1'}, dimensions={0}, use_global_device_ids=true | all-gather | bytes 1179648 | tf_op jit(solution)/shard_map/all_gather | solution.py:40
  164.9 1.4 reshape_reshape.3
  166.3 1.7 fusion.21
  168.7 5.6 %all-to-all-start.5 = ((bf16[32,3,64]{2,1,0:T(4,128)(2,1)}), bf16[32,3,64]{2,1,0:T(4,128)(2,1)S(1)}, u32[]{:S(2)}, u32[]{:S(2)}) async-start(bf16[32,3,64]{2,1,0:T(4,128)(2,1)} %all_to_all.89), calls=%async_computation.5 | async-start | bytes 65536 | tf_op jit(solution)/shard_map/all_to_all | solution.py:176
  176.9 9.3 %all-to-all-done.5 = bf16[32,3,64]{2,1,0:T(4,128)(2,1)S(1)} async-done(((bf16[32,3,64]{2,1,0:T(4,128)(2,1)}), bf16[32,3,64]{2,1,0:T(4,128)(2,1)S(1)}, u32[]{:S(2)}, u32[]{:S(2)}) %all-to-all-start.5) | async-done | bytes 12320 | tf_op jit(solution)/shard_map/all_to_all | solution.py:176
  188.3 5.0 %all-to-all-start.6 = ((bf16[32,1,2,2048]{3,2,1,0:T(2,128)(2,1)}), bf16[32,1,2,2048]{3,2,1,0:T(2,128)(2,1)S(1)}, u32[]{:S(2)}, u32[]{:S(2)}) async-start(bf16[32,1,2,2048]{3,2,1,0:T(2,128)(2,1)} %bitcast.16), calls=%async_computation.6 | async-start | bytes 524288 | tf_op jit(solution)/shard_map/all_to_all | solution.py:196
  195.1 19.6 %all-to-all-done.6 = bf16[32,1,2,2048]{3,2,1,0:T(2,128)(2,1)S(1)} async-done(((bf16[32,1,2,2048]{3,2,1,0:T(2,128)(2,1)}), bf16[32,1,2,2048]{3,2,1,0:T(2,128)(2,1)S(1)}, u32[]{:S(2)}, u32[]{:S(2)}) %all-to-all-start.6) | async-done | bytes 262176 | tf_op jit(solution)/shard_map/all_to_all | solution.py:196
  214.7 5.3 %all-to-all-start.8 = ((bf16[32,3,1024]{2,1,0:T(4,128)(2,1)}), bf16[32,3,1024]{2,1,0:T(4,128)(2,1)S(1)}, u32[]{:S(2)}, u32[]{:S(2)}) async-start(bf16[32,3,1024]{2,1,0:T(4,128)(2,1)} %pad_maximum_fusion), calls=%async_computation.8 | async-start | bytes 524288 | tf_op jit(solution)/shard_map/all_to_all | solution.py:58
  220.1 2.1 fusion.11
  222.2 2.5 convolution_convert_fusion
  225.6 15.8 %all-to-all-done.8 = bf16[32,3,1024]{2,1,0:T(4,128)(2,1)S(1)} async-done(((bf16[32,3,1024]{2,1,0:T(4,128)(2,1)}), bf16[32,3,1024]{2,1,0:T(4,128)(2,1)S(1)}, u32[]{:S(2)}, u32[]{:S(2)}) %all-to-all-start.8) | async-done | bytes 196640 | tf_op jit(solution)/shard_map/all_to_all | solution.py:58
  241.5 5.3 %all-to-all-start.7 = ((bf16[32,1,2,2048]{3,2,1,0:T(2,128)(2,1)}), bf16[32,1,2,2048]{3,2,1,0:T(2,128)(2,1)S(1)}, u32[]{:S(2)}, u32[]{:S(2)}) async-start(bf16[32,1,2,2048]{3,2,1,0:T(2,128)(2,1)} %bitcast.20), calls=%async_computation.7 | async-start | bytes 524288 | tf_op jit(solution)/shard_map/all_to_all | solution.py:200
  246.8 7.0 %multiply_add_fusion = f32[3,64,64,128]{3,2,1,0:T(8,128)} fusion(f32[3,64,64,128]{3,2,1,0:T(8,128)} %param.28, f32[3,64,128]{2,1,0:T(8,128)S(1)} %broadcast_bitcast_fusion, f32[3,64,64]{2,1,0:T(8,128)S(1)} %broadcast_multiply_fusion, f32[3,64]{1,0:T(4,128)S(1)} %copy-done.6), kind=kLoop, calls=%fused_computation.3 | loop fusion | flops 4718592 | bytes 12731136 | tf_op jit(solution)/shard_map/add | solution.py:150
  255.3 12.9 %all-to-all-done.7 = bf16[32,1,2,2048]{3,2,1,0:T(2,128)(2,1)S(1)} async-done(((bf16[32,1,2,2048]{3,2,1,0:T(2,128)(2,1)}), bf16[32,1,2,2048]{3,2,1,0:T(2,128)(2,1)S(1)}, u32[]{:S(2)}, u32[]{:S(2)}) %all-to-all-start.7) | async-done | bytes 262176 | tf_op jit(solution)/shard_map/all_to_all | solution.py:200
  269.2 2.6 fusion.7
  (114 shorter events, 30.2 us)
Async XLA Ops:
  0.6 221.6 %copy-start = (bf16[1,512,2048]{2,1,0:T(8,128)(2,1)S(1)}, bf16[1,512,2048]{2,1,0:T(8,128)(2,1)}, u32[]{:S(2)}) copy-start(bf16[1,512,2048]{2,1,0:T(8,128)(2,1)} %param.48) | copy-start | bytes 6291460
  0.6 78.8 %copy-start.11 = (f32[64]{0:T(128)S(1)}, f32[64]{0:T(128)}, u32[]{:S(2)}) copy-start(f32[64]{0:T(128)} %param.34) | copy-start | bytes 772
  0.7 78.8 %copy-start.9 = (f32[3,64]{1,0:T(4,128)S(1)}, f32[3,64]{1,0:T(4,128)}, u32[]{:S(2)}) copy-start(f32[3,64]{1,0:T(4,128)} %param.36) | copy-start | bytes 2308
  2.6 51.8 %all-to-all-start = ((bf16[32,3,2048]{2,1,0:T(4,128)(2,1)}), bf16[32,3,2048]{2,1,0:T(4,128)(2,1)S(1)}, u32[]{:S(2)}, u32[]{:S(2)}) async-start(bf16[32,3,2048]{2,1,0:T(4,128)(2,1)} %broadcast_in_dim.11), calls=%async_computation | async-start | bytes 1048576 | tf_op jit(solution)/shard_map/all_to_all | solution.py:21
  56.0 74.1 %copy-start.7 = (f32[8,8]{1,0:T(8,128)S(1)}, f32[8,8]{1,0:T(8,128)}, u32[]{:S(2)}) copy-start(f32[8,8]{1,0:T(8,128)} %mul.284) | copy-start | bytes 772
  57.9 16.4 %all-to-all-start.2 = ((bf16[32,3,32]{2,1,0:T(4,128)(2,1)}), bf16[32,3,32]{2,1,0:T(4,128)(2,1)S(1)}, u32[]{:S(2)}, u32[]{:S(2)}) async-start(bf16[32,3,32]{2,1,0:T(4,128)(2,1)} %all_to_all.79), calls=%async_computation.2 | async-start | bytes 65536 | tf_op jit(solution)/shard_map/all_to_all | solution.py:123
  74.3 16.9 %all-to-all-start.3 = ((bf16[32,3,32]{2,1,0:T(4,128)(2,1)}), bf16[32,3,32]{2,1,0:T(4,128)(2,1)S(1)}, u32[]{:S(2)}, u32[]{:S(2)}) async-start(bf16[32,3,32]{2,1,0:T(4,128)(2,1)} %all_to_all.83), calls=%async_computation.3 | async-start | bytes 65536 | tf_op jit(solution)/shard_map/all_to_all | solution.py:124
  80.6 83.6 %copy-start.3 = (f32[3,64]{1,0:T(4,128)}, f32[3,64]{1,0:T(4,128)S(1)}, u32[]{:S(2)}) copy-start(f32[3,64]{1,0:T(4,128)S(1)} %get-tuple-element.10) | copy-start | bytes 2308
  80.6 83.6 %copy-start.5 = (f32[3,64]{1,0:T(4,128)}, f32[3,64]{1,0:T(4,128)S(1)}, u32[]{:S(2)}) copy-start(f32[3,64]{1,0:T(4,128)S(1)} %get-tuple-element.9) | copy-start | bytes 2308
  91.2 17.1 %all-to-all-start.1 = ((bf16[32,3,128]{2,1,0:T(4,128)(2,1)}), bf16[32,3,128]{2,1,0:T(4,128)(2,1)S(1)}, u32[]{:S(2)}, u32[]{:S(2)}) async-start(bf16[32,3,128]{2,1,0:T(4,128)(2,1)} %all_to_all.75), calls=%async_computation.1 | async-start | bytes 65536 | tf_op jit(solution)/shard_map/all_to_all | solution.py:122
  108.3 16.9 %all-to-all-start.4 = ((bf16[32,3,128]{2,1,0:T(4,128)(2,1)}), bf16[32,3,128]{2,1,0:T(4,128)(2,1)S(1)}, u32[]{:S(2)}, u32[]{:S(2)}) async-start(bf16[32,3,128]{2,1,0:T(4,128)(2,1)} %all_to_all.87), calls=%async_computation.4 | async-start | bytes 65536 | tf_op jit(solution)/shard_map/all_to_all | solution.py:121
  130.1 64.1 %copy-start.1 = (bf16[3,3,6144]{2,1,0:T(4,128)(2,1)S(1)}, bf16[3,3,6144]{2,1,0:T(4,128)(2,1)}, u32[]{:S(2)}) copy-start(bf16[3,3,6144]{2,1,0:T(4,128)(2,1)} %param.27) | copy-start | bytes 331780
  164.2 29.9 %copy-start.4 = (f32[3,64]{1,0:T(4,128)S(1)}, f32[3,64]{1,0:T(4,128)}, u32[]{:S(2)}) copy-start(f32[3,64]{1,0:T(4,128)} %copy-done.3) | copy-start | bytes 2308
  168.7 17.4 %all-to-all-start.5 = ((bf16[32,3,64]{2,1,0:T(4,128)(2,1)}), bf16[32,3,64]{2,1,0:T(4,128)(2,1)S(1)}, u32[]{:S(2)}, u32[]{:S(2)}) async-start(bf16[32,3,64]{2,1,0:T(4,128)(2,1)} %all_to_all.89), calls=%async_computation.5 | async-start | bytes 65536 | tf_op jit(solution)/shard_map/all_to_all | solution.py:176
  176.8 70.0 %copy-start.6 = (f32[3,64]{1,0:T(4,128)S(1)}, f32[3,64]{1,0:T(4,128)}, u32[]{:S(2)}) copy-start(f32[3,64]{1,0:T(4,128)} %copy-done.5) | copy-start | bytes 2308
  188.3 26.4 %all-to-all-start.6 = ((bf16[32,1,2,2048]{3,2,1,0:T(2,128)(2,1)}), bf16[32,1,2,2048]{3,2,1,0:T(2,128)(2,1)S(1)}, u32[]{:S(2)}, u32[]{:S(2)}) async-start(bf16[32,1,2,2048]{3,2,1,0:T(2,128)(2,1)} %bitcast.16), calls=%async_computation.6 | async-start | bytes 524288 | tf_op jit(solution)/shard_map/all_to_all | solution.py:196
  214.7 26.7 %all-to-all-start.8 = ((bf16[32,3,1024]{2,1,0:T(4,128)(2,1)}), bf16[32,3,1024]{2,1,0:T(4,128)(2,1)S(1)}, u32[]{:S(2)}, u32[]{:S(2)}) async-start(bf16[32,3,1024]{2,1,0:T(4,128)(2,1)} %pad_maximum_fusion), calls=%async_computation.8 | async-start | bytes 524288 | tf_op jit(solution)/shard_map/all_to_all | solution.py:58
  241.5 26.7 %all-to-all-start.7 = ((bf16[32,1,2,2048]{3,2,1,0:T(2,128)(2,1)}), bf16[32,1,2,2048]{3,2,1,0:T(2,128)(2,1)S(1)}, u32[]{:S(2)}, u32[]{:S(2)}) async-start(bf16[32,1,2,2048]{3,2,1,0:T(2,128)(2,1)} %bitcast.20), calls=%async_computation.7 | async-start | bytes 524288 | tf_op jit(solution)/shard_map/all_to_all | solution.py:200
  246.8 7.0 %copy-start.8 = (f32[2048]{0:T(1024)S(1)}, f32[2048]{0:T(1024)}, u32[]{:S(2)}) copy-start(f32[2048]{0:T(1024)} %param.43) | copy-start | bytes 24580
  246.8 7.0 %copy-start.12 = (bf16[2048,32]{0,1:T(8,128)(2,1)S(1)}, bf16[2048,32]{0,1:T(8,128)(2,1)}, u32[]{:S(2)}) copy-start(bf16[2048,32]{0,1:T(8,128)(2,1)} %param.44) | copy-start | bytes 393220
  246.8 8.2 %copy-start.2 = (s32[3,6]{1,0:T(4,128)S(1)}, s32[3,6]{1,0:T(4,128)}, u32[]{:S(2)}) copy-start(s32[3,6]{1,0:T(4,128)} %param.45) | copy-start | bytes 220
  246.8 22.3 %copy-start.10 = (pred[3,6]{1,0:T(4,128)(4,1)S(1)}, pred[3,6]{1,0:T(4,128)(4,1)}, u32[]{:S(2)}) copy-start(pred[3,6]{1,0:T(4,128)(4,1)} %get-tuple-element.3) | copy-start | bytes 58
where the time goes:
time: 274 us; the launch traced here: 272 us
  waiting for transfers between devices  120 us (44%)
  starting transfers between devices  58.7 us (21%)
  blocking collectives  32.5 us (12%)
  matrix products  23 us (8%)
  other arithmetic  18.6 us (7%)
  local copies, waits for them, and re-layouts  17.8 us (6%)
    all_gather x2, blocking collectives, all_blocks(): pieces = lax.all_gather(pieces, axes[k])  32.5 us
    all_to_all x1, waiting for transfers between devices, from_everyone(): lax.all_to_all(jnp.broadcast_to(shard[None], (count, *shard.shape)), axis...  24.1 us
    all_to_all x1, waiting for transfers between devices, shards(): lax.all_to_all(outbound, EP, split_axis=0, concat_axis=0, tiled=True)  19.6 us
    all_to_all x1, starting transfers between devices, from_everyone(): lax.all_to_all(jnp.broadcast_to(shard[None], (count, *shard.shape)), axis...  18.5 us
    dot_general x13, matrix products, matmul(): return jnp.dot(left, right, preferred_element_type=jnp.float32)  18.3 us
    all_to_all x1, waiting for transfers between devices, summed_on_arrival(): lax.all_to_all(pieces, axis, split_axis=0, concat_axis=0, tiled=True)  15.8 us
    all_to_all x1, waiting for transfers between devices, shards(): lax.all_to_all(jnp.stack(results, axis=1), EP, split_axis=0, concat_axis=...  12.9 us
    all_to_all x1, waiting for transfers between devices, shards(): lax.all_to_all(input_part, EP, split_axis=0, concat_axis=1, tiled=True)  11.7 us
  transfers between devices with their start and end apart: 9, of which 9 were waited for; matrix products, arithmetic and copies ran while one was open for 13% of the time, Pallas kernels for 0%

commit v1 on v0

v1 whole, which is shorter than its diff:
```python
import jax
import jax.numpy as jnp
from jax import lax
from jax.sharding import Mesh
from jax.sharding import PartitionSpec as P

HEAD_DIM = 64
GROUPS = 8
STATE = 128
CAP = 2
EP = ("zh", "zl", "core")
NEAR = ("zl", "core")
GRP_EP = ("grp",) + EP

epsilon = 1e-06
routed_scale = 2.5


def row_scale(values):
    return lax.rsqrt(jnp.mean(values * values, axis=-1, keepdims=True) + epsilon)


def matmul(left, right):
    return jnp.dot(left, right, preferred_element_type=jnp.float32)


def contract(left, right, left_dim, right_dim):
    return lax.dot_general(
        left, right, (((left_dim,), (right_dim,)), ((), ())), preferred_element_type=jnp.float32
    )


def split_pair(values):
    high = values.astype(jnp.bfloat16)
    low = (values - high.astype(jnp.float32)).astype(jnp.bfloat16)
    return high, low


def shards(
    hidden,
    conv_window,
    ssm_state,
    gate_proj,
    input_proj,
    write_proj,
    read_proj,
    step_proj,
    step_bias,
    decay_log,
    decay_shift,
    skip_scale,
    conv_taps,
    conv_bias,
    mix_gain,
    group_gain,
    out_proj,
    ffn_gain,
    router,
    expert_ids,
    expert_gate,
    expert_up,
    expert_down,
    shared_gate,
    shared_up,
    shared_down,
):
    rows = hidden.shape[0]
    width = hidden.shape[1]
    index = lax.axis_index(EP)
    count = lax.axis_size(EP)
    near = lax.axis_size(NEAR)
    experts = router.shape[1]
    units = shared_gate.shape[1]
    features = shared_gate.shape[0]
    near_units = units // near

    near_weights = jnp.concatenate(
        [
            jnp.moveaxis(shared_gate.reshape(features, near, near_units), 1, 0),
            jnp.moveaxis(shared_up.reshape(features, near, near_units), 1, 0),
        ],
        axis=2,
    )
    near_weights = lax.all_to_all(near_weights, NEAR, 0, 0, tiled=True)
    near_weights = near_weights.reshape(near * features, 2 * near_units)

    gathered = lax.all_gather(hidden, EP)
    gathered_wide = jnp.moveaxis(gathered, 0, 1).reshape(rows * count, width).astype(jnp.float32)
    normed = (gathered_wide * row_scale(gathered_wide) * mix_gain).astype(jnp.bfloat16)
    member = jnp.any(
        expert_ids[:, :, None] == jnp.arange(experts, dtype=jnp.int32)[None, None, :], axis=1
    )
    parts = jnp.concatenate(
        [
            matmul(normed, gate_proj).astype(jnp.bfloat16),
            matmul(normed, input_proj).astype(jnp.bfloat16),
            matmul(normed, write_proj).astype(jnp.bfloat16),
            matmul(normed, read_proj).astype(jnp.bfloat16),
        ],
        axis=1,
    )
    parts = jnp.moveaxis(parts.reshape(rows, count, -1), 1, 0)
    named = member.astype(jnp.bfloat16).T.reshape(count, rows, 1)
    pieces = lax.all_to_all(jnp.concatenate([parts, named], axis=2), EP, 0, 0, tiled=True)

    hidden_wide = hidden.astype(jnp.float32)
    normed_local = (hidden_wide * row_scale(hidden_wide) * mix_gain).astype(jnp.bfloat16)
    step_raw = matmul(normed_local, step_proj)

    widths = [gate_proj.shape[1], input_proj.shape[1], write_proj.shape[1], read_proj.shape[1]]
    fields, start = [], 0
    for size in widths:
        fields.append(
            jnp.moveaxis(pieces[:, :, start : start + size], 0, 1).reshape(rows, count * size)
        )
        start += size
    gate_rows, input_rows, write_rows, read_rows = fields
    chosen = pieces[:, :, start].T.reshape(1, rows * count)

    inner_width = gate_rows.shape[1]
    state_span = GROUPS * STATE
    head_count = step_bias.shape[0]
    per_group = head_count // GROUPS
    fresh_row = jnp.concatenate([input_rows, write_rows, read_rows], axis=1)
    window = jnp.concatenate([conv_window, fresh_row[:, None, :]], axis=1)
    convolved = jax.nn.silu(
        jnp.sum(window.astype(jnp.float32) * conv_taps.astype(jnp.float32)[None], axis=1)
        + conv_bias
    )
    head_input = convolved[:, :inner_width].reshape(rows, GROUPS, per_group, HEAD_DIM)
    write_vec = convolved[:, inner_width : inner_width + state_span].reshape(rows, GROUPS, STATE)
    read_vec = convolved[:, inner_width + state_span :].reshape(rows, GROUPS, STATE)
    step_size = jax.nn.softplus(step_raw + step_bias)
    decay_rate = jnp.exp(decay_shift - step_size * jnp.exp(decay_log)).reshape(
        rows, GROUPS, per_group
    )
    step_group = step_size.reshape(rows, GROUPS, per_group)
    carried = ssm_state.reshape(rows, GROUPS, per_group, HEAD_DIM, STATE)
    next_state = (
        decay_rate[..., None, None] * carried
        + (step_group[..., None] * head_input)[..., None] * write_vec[:, :, None, None, :]
    )
    mixed_out = jnp.einsum("sgepn,sgn->sgep", next_state, read_vec)
    mixed_out = mixed_out + skip_scale.reshape(GROUPS, per_group)[None, :, :, None] * head_input
    mixed_out = mixed_out.reshape(rows, inner_width).astype(jnp.bfloat16)
    gated_out = mixed_out.astype(jnp.float32) * jax.nn.silu(gate_rows.astype(jnp.float32))
    blocks = gated_out.reshape(rows, GROUPS, -1)
    gated_out = ((blocks * row_scale(blocks)).reshape(rows, inner_width) * group_gain).astype(
        jnp.bfloat16
    )

    col_width = out_proj.shape[1]
    gated_all = jnp.moveaxis(lax.all_gather(gated_out, EP), 0, 1).reshape(rows * count, inner_width)
    resid_cols = lax.dynamic_slice_in_dim(gathered_wide, index * col_width, col_width, 1).T
    resid_part = (resid_cols + contract(out_proj, gated_all, 0, 1)).astype(jnp.bfloat16)
    resid_all = lax.all_gather(resid_part, EP).reshape(width, rows * count)

    resid_wide = resid_all.astype(jnp.float32)
    norm_all = lax.rsqrt(jnp.mean(resid_wide * resid_wide, axis=0, keepdims=True) + epsilon)
    routed_in = (resid_wide * norm_all * ffn_gain[:, None]).astype(jnp.bfloat16)
    shared_in = (resid_wide * ffn_gain[:, None]).astype(jnp.bfloat16)

    order = jnp.arange(rows * count, dtype=jnp.int32)[None]
    chosen_rows = chosen.reshape(rows, count)
    earlier = (jnp.cumsum(chosen_rows, axis=0) - chosen_rows).reshape(1, rows * count)
    slot = jnp.arange(CAP * count, dtype=jnp.int32)[:, None]
    pick = (
        (slot % count == order % count)
        & (chosen > 0.5)
        & (earlier.astype(jnp.int32) == slot // count)
    ).astype(jnp.bfloat16)
    expert_hidden = (
        jax.nn.silu(contract(routed_in, expert_gate[0], 0, 0))
        * contract(routed_in, expert_up[0], 0, 0)
    ).astype(jnp.bfloat16)
    expert_rows = matmul(pick, expert_hidden).astype(jnp.bfloat16)
    result = matmul(expert_rows, expert_down[0]).astype(jnp.bfloat16)

    block = near * features
    shared_block = lax.dynamic_slice_in_dim(shared_in, (index // near) * block, block, 0)
    shared_part = contract(shared_block, near_weights, 0, 0).astype(jnp.bfloat16)
    shared_part = shared_part.reshape(rows, count, 2, near_units)
    shared_part = shared_part.transpose(1, 2, 0, 3).reshape(count, CAP, rows * near_units)
    outbound = jnp.concatenate(
        [jnp.moveaxis(result.reshape(CAP, count, width), 1, 0), shared_part], axis=2
    )
    returned = lax.all_to_all(outbound, EP, 0, 0, tiled=True)

    own = (
        jnp.arange(rows * count, dtype=jnp.int32)[None]
        == jnp.arange(rows, dtype=jnp.int32)[:, None] * count + index
    ).astype(jnp.bfloat16)
    resid_own = contract(own, resid_all, 1, 1)
    norm_scale = row_scale(resid_own)
    routed_own = (resid_own * norm_scale * ffn_gain).astype(jnp.bfloat16)
    scores = jnp.where(member, jax.nn.sigmoid(matmul(routed_own, router)), 0.0)
    weights = routed_scale * scores / jnp.sum(scores, axis=1, keepdims=True)
    own_member = member.astype(jnp.int32)
    own_slot = jnp.cumsum(own_member, axis=0) - own_member
    by_slot = jnp.concatenate([jnp.where(own_slot == s, weights, 0.0) for s in range(CAP)], axis=1)
    back = jnp.moveaxis(returned[:, :, :width], 1, 0).reshape(CAP * count, width)
    high, low = split_pair(by_slot)
    routed = matmul(high, back) + matmul(low, back)
    pre = returned[:, :, width:].reshape(count // near, near, 2, rows, near_units)
    pre = jnp.sum(pre.astype(jnp.float32), axis=0).transpose(1, 2, 0, 3).reshape(2, rows, units)
    shared_hidden = (jax.nn.silu(norm_scale * pre[0]) * (norm_scale * pre[1])).astype(jnp.bfloat16)
    layer_out = (resid_own + routed + matmul(shared_hidden, shared_down)).astype(jnp.bfloat16)
    return (layer_out, next_state.reshape(ssm_state.shape), window[:, 1:])


def solution(mesh):
    torus = Mesh(mesh.devices.reshape(mesh.shape["grp"], -1, 2, 2), GRP_EP)
    return jax.shard_map(
        shards,
        mesh=torus,
        in_specs=(
            P(GRP_EP, None),
            P(GRP_EP, None, None),
            P(GRP_EP, None, None, None),
            P(None, EP),
            P(None, EP),
            P(None, EP),
            P(None, EP),
            P(),
            P(),
            P(),
            P(GRP_EP, None),
            P(),
            P(),
            P(),
            P(),
            P(),
            P(None, EP),
            P(),
            P(),
            P(GRP_EP, None),
            P(EP, None, None),
            P(EP, None, None),
            P(EP, None, None),
            P(EP, None),
            P(EP, None),
            P(),
        ),
        out_specs=(P(GRP_EP, None), P(GRP_EP, None, None, None), P(GRP_EP, None, None)),
        check_vma=False,
    )
```

time: 274 us -> 207 us (0.76)
  waiting for transfers between devices: 120 us -> 17.7 us
  blocking collectives: 32.5 us -> 103 us
  starting transfers between devices: 58.7 us -> 20.1 us
  other arithmetic: 18.6 us -> 23.7 us
    all_to_all x9 -> x3, waiting for transfers between devices: 120 us -> 17.7 us  [the longest x1 16.2 us: shards(): returned = lax.all_to_all(outbound, EP, 0, 0, tiled=True)]
    all_gather x2 -> x3, blocking collectives: 32.5 us -> 103 us  [the longest x1 42.4 us: shards(): gathered = lax.all_gather(hidden, EP)]
    all_to_all x9 -> x3, starting transfers between devices: 58.7 us -> 20.1 us  [the longest x1 9.49 us: shards(): returned = lax.all_to_all(outbound, EP, 0, 0, tiled=True)]
    dot_general x0 -> x4, matrix products: none -> 5.53 us  [contract(): lax.dot_general(left, right, (((left_dim,), (right_dim,)), ((), ())), pre...]
    dot_general x13 -> x11, matrix products: 18.3 us -> 13.7 us  [matmul(): return jnp.dot(left, right, preferred_element_type=jnp.float32)]
    all_to_all x9 -> x0, local copies, waits for them, and re-layouts: 3.43 us -> none  [the longest x3 0.76 us: shards(): lax.all_to_all(write_part, EP, split_axis=0, concat_axis=1, tiled=True)]
  transfers between devices with their start and end apart: 9 -> 3, of which waited for: 9 -> 2; matrix products, arithmetic and copies ran while one was open for 13% -> 23% of each run, Pallas kernels for 0% -> 0%
where the time goes in v1:
time: 207 us; the launch traced here: 206 us
  blocking collectives  103 us (50%)
  matrix products  24 us (12%)
  other arithmetic  23.7 us (11%)
  starting transfers between devices  20.1 us (10%)
  waiting for transfers between devices  17.7 us (9%)
  local copies, waits for them, and re-layouts  16.2 us (8%)
    all_gather x1, blocking collectives, shards(): gathered = lax.all_gather(hidden, EP)  42.4 us
    all_gather x1, blocking collectives, shards(): lax.all_gather(gated_out, EP)  32 us
    all_gather x1, blocking collectives, shards(): resid_all = lax.all_gather(resid_part, EP).reshape(width, rows * count)  28.8 us
    all_to_all x1, waiting for transfers between devices, shards(): returned = lax.all_to_all(outbound, EP, 0, 0, tiled=True)  16.2 us
    dot_general x11, matrix products, matmul(): return jnp.dot(left, right, preferred_element_type=jnp.float32)  13.7 us
    all_to_all x1, starting transfers between devices, shards(): returned = lax.all_to_all(outbound, EP, 0, 0, tiled=True)  9.49 us
    add x1, other arithmetic, shards(): decay_rate[..., None, None] * carried  6.95 us
    all_to_all x1, starting transfers between devices, shards(): lax.all_to_all(jnp.concatenate([parts, named], axis=2), EP, 0, 0, tiled=T...  5.98 us
  transfers between devices with their start and end apart: 3, of which 2 were waited for; matrix products, arithmetic and copies ran while one was open for 23% of the time, Pallas kernels for 0%

profile of v1, /device:TPU:69, one launch (start us, length us, event | category | flops | bytes accessed | tf_op | source)
XLA Modules:
  0.0 206.1 jit_solution(4048649212426845937)
XLA Ops:
  0.7 42.4 %all-gather.2 = bf16[32,3,2048]{2,1,0:T(4,128)(2,1)S(1)} all-gather(bf16[1,3,2048]{2,1,0:T(4,128)(2,1)} %bitcast.172), channel_id=2, replica_groups=mesh['grp'=4,'zh'=8,'zl'=2,'core'=2] {'zh','zl','core'}, dimensions={0}, use_global_device_ids=true | all-gather | bytes 405504 | tf_op jit(solution)/shard_map/all_gather | solution.py:87
  44.9 1.1 convolution_convert_fusion.5
  46.2 1.8 convolution_convert_fusion.4
  48.7 1.3 convolution_convert_fusion.2
  50.0 1.3 convolution_convert_fusion.3
  53.1 6.0 %all-to-all-start = ((bf16[32,3,321]{2,1,0:T(4,128)(2,1)}), bf16[32,3,321]{2,1,0:T(4,128)(2,1)S(1)}, u32[]{:S(2)}, u32[]{:S(2)}) async-start(bf16[32,3,321]{2,1,0:T(4,128)(2,1)} %pad_maximum_fusion.3), calls=%async_computation | async-start | bytes 196608 | tf_op jit(solution)/shard_map/all_to_all | solution.py:104
  60.0 0.9 reshape.373
  61.0 1.2 subtract_exponential_fusion
  65.0 1.3 mul.334
  67.6 1.4 mul.357
  69.0 1.3 dynamic-slice
  72.1 1.4 all-to-all-done
  73.6 4.7 %all-to-all-start.1 = ((bf16[4,64,256]{2,1,0:T(8,128)(2,1)}), bf16[4,64,256]{2,1,0:T(8,128)(2,1)S(1)}, u32[]{:S(2)}, u32[]{:S(2)}) async-start(bf16[4,64,256]{2,1,0:T(8,128)(2,1)} %copy.134), calls=%async_computation.1 | async-start | bytes 262144 | tf_op jit(solution)/shard_map/all_to_all | solution.py:84
  82.1 4.7 %fusion = f32[3,8,1,8,64]{4,2,3,1,0:T(1,128)S(1)} fusion(f32[3,8,128,1,1]{2,3,4,1,0:T(1,128)} %bitcast.173, f32[3,8,8,64,128]{4,3,2,1,0:T(8,128)} %bitcast.154, f32[3,8,128]{2,1,0:T(8,128)} %bitcast.170, f32[3,8,8,64]{3,2,1,0:T(8,128)S(1)} %broadcast_multiply_fusion.1, f32[3,8,8]{2,1,0:T(8,128)} %mul.316), kind=kOutput, calls=%fused_computation.1 | convolution fusion | flops 7864320 | bytes 6415104 | tf_op jit(solution)/shard_map/sgepn,sgn->sgep/dot_general | solution.py:143
  88.1 32.0 %all_gather.18 = bf16[32,3,4096]{2,1,0:T(4,128)(2,1)S(1)} all-gather(bf16[1,3,4096]{2,1,0:T(4,128)(2,1)S(1)} %multiply_convert_fusion.2), channel_id=1, replica_groups=mesh['grp'=4,'zh'=8,'zl'=2,'core'=2] {'zh','zl','core'}, dimensions={0}, use_global_device_ids=true | all-gather | bytes 811008 | tf_op jit(solution)/shard_map/all_gather | solution.py:153
  120.7 1.2 fusion.27
  121.9 28.8 %all-gather.1 = bf16[2048,96]{1,0:T(8,128)(2,1)S(1)} all-gather(bf16[64,96]{1,0:T(8,128)(2,1)S(1)} %fusion.27), channel_id=3, replica_groups=mesh['grp'=4,'zh'=8,'zl'=2,'core'=2] {'zh','zl','core'}, dimensions={0}, use_global_device_ids=true | all-gather | bytes 405504 | tf_op jit(solution)/shard_map/all_gather | solution.py:156
  151.0 1.0 convert_element_type.245
  152.8 1.3 broadcast_bitcast_fusion
  154.1 1.1 multiply_reduce_fusion.4
  157.4 1.1 multiply_convert_fusion
  158.5 2.1 %fusion.12 = f32[96,512]{1,0:T(8,128)S(1)} fusion(bf16[2048,96]{1,0:T(8,128)(2,1)S(1)} %bitcast.155, bf16[1,2048,512]{2,1,0:T(8,128)(2,1)} %param.46), kind=kOutput, calls=%fused_computation.16 | convolution fusion | flops 201326592 | bytes 2686976 | tf_op jit(solution)/shard_map/dot_general | solution.py:28
  160.6 2.3 %fusion.23 = bf16[64,512]{1,0:T(8,128)(2,1)S(1)} fusion(bf16[2048,96]{1,0:T(8,128)(2,1)S(1)} %bitcast.156, bf16[1,2048,512]{2,1,0:T(8,128)(2,1)} %param.47, f32[96,512]{1,0:T(8,128)S(1)} %fusion.12, s32[96]{0:T(128)S(1)} %reshape.385, s32[96]{0:T(128)} %and_select_fusion.1, s32[64]{0:T(128)} %get-tuple-element.21, s32[64]{0:T(128)} %get-tuple-element.22, ...), kind=kOutput, calls=%fused_computation.21 | convolution fusion | flops 207970304 | bytes 2753888 | tf_op jit(solution)/shard_map/dot_general | solution.py:24
  163.7 1.2 fusion.88
  165.7 1.0 broadcast_multiply_fusion
  166.7 1.2 convolution_convert_fusion.1
  168.0 1.0 pad_maximum_fusion
  169.0 9.5 %all-to-all-start.2 = ((bf16[32,2,2432]{2,1,0:T(2,128)(2,1)}), bf16[32,2,2432]{2,1,0:T(2,128)(2,1)S(1)}, u32[]{:S(2)}, u32[]{:S(2)}) async-start(bf16[32,2,2432]{2,1,0:T(2,128)(2,1)} %pad_maximum_fusion), calls=%async_computation.2 | async-start | bytes 622592 | tf_op jit(solution)/shard_map/all_to_all | solution.py:187
  178.6 7.0 %multiply_add_fusion = f32[3,64,64,128]{3,2,1,0:T(8,128)} fusion(f32[3,64,64,128]{3,2,1,0:T(8,128)} %param.28, f32[3,64,128]{2,1,0:T(8,128)S(1)} %copy-done.3, f32[3,64,64]{2,1,0:T(8,128)S(1)} %broadcast_multiply_fusion, f32[3,64]{1,0:T(4,128)} %copy-done.12), kind=kLoop, calls=%fused_computation | loop fusion | flops 4718592 | bytes 12731136 | tf_op jit(solution)/shard_map/add | solution.py:140
  185.5 0.9 fusion.37
  186.4 16.2 %all-to-all-done.2 = bf16[32,2,2432]{2,1,0:T(2,128)(2,1)S(1)} async-done(((bf16[32,2,2432]{2,1,0:T(2,128)(2,1)}), bf16[32,2,2432]{2,1,0:T(2,128)(2,1)S(1)}, u32[]{:S(2)}, u32[]{:S(2)}) %all-to-all-start.2) | async-done | bytes 311328 | tf_op jit(solution)/shard_map/all_to_all | solution.py:187
  203.5 2.6 %fusion.8 = bf16[3,2048]{1,0:T(4,128)(2,1)} fusion(f32[3,2048]{1,0:T(4,128)S(1)} %fusion.7, bf16[512,2048]{1,0:T(8,128)(2,1)} %param.51, f32[2,3,4,128]{3,1,2,0:T(4,128)S(1)} %bitcast.174, f32[3]{0:T(128)S(1)} %copy-done.16), kind=kOutput, calls=%fused_computation.12 | convolution fusion | flops 6316032 | bytes 2146316 | tf_op jit(solution)/shard_map/dot_general | solution.py:24
  (116 shorter events, 22.7 us)
Async XLA Ops:
  0.6 162.2 %copy-start = (bf16[1,512,2048]{2,1,0:T(8,128)(2,1)S(1)}, bf16[1,512,2048]{2,1,0:T(8,128)(2,1)}, u32[]{:S(2)}) copy-start(bf16[1,512,2048]{2,1,0:T(8,128)(2,1)} %param.48) | copy-start | bytes 6291460
  0.6 58.5 %copy-start.6 = (bf16[3,2048]{1,0:T(4,128)(2,1)S(1)}, bf16[3,2048]{1,0:T(4,128)(2,1)}, u32[]{:S(2)}) copy-start(bf16[3,2048]{1,0:T(4,128)(2,1)} %param.26) | copy-start | bytes 36868
  0.7 59.3 %copy-start.7 = (bf16[64,512]{1,0:T(8,128)(2,1)S(1)}, bf16[64,512]{1,0:T(8,128)(2,1)}, u32[]{:S(2)}) copy-start(bf16[64,512]{1,0:T(8,128)(2,1)} %param.49) | copy-start | bytes 196612
  0.7 78.0 %copy-start.1 = (bf16[3,3,6144]{2,1,0:T(4,128)(2,1)S(1)}, bf16[3,3,6144]{2,1,0:T(4,128)(2,1)}, u32[]{:S(2)}) copy-start(bf16[3,3,6144]{2,1,0:T(4,128)(2,1)} %param.27) | copy-start | bytes 331780
  52.3 8.7 %copy-start.13 = (pred[3,32]{1,0:T(4,128)(4,1)}, pred[3,32]{1,0:T(4,128)(4,1)S(1)}, u32[]{:S(2)}) copy-start(pred[3,32]{1,0:T(4,128)(4,1)S(1)} %fusion.66) | copy-start | bytes 292
  53.1 20.4 %all-to-all-start = ((bf16[32,3,321]{2,1,0:T(4,128)(2,1)}), bf16[32,3,321]{2,1,0:T(4,128)(2,1)S(1)}, u32[]{:S(2)}, u32[]{:S(2)}) async-start(bf16[32,3,321]{2,1,0:T(4,128)(2,1)} %pad_maximum_fusion.3), calls=%async_computation | async-start | bytes 196608 | tf_op jit(solution)/shard_map/all_to_all | solution.py:104
  62.2 16.4 %copy-start.12 = (f32[3,64]{1,0:T(4,128)}, f32[3,64]{1,0:T(4,128)S(1)}, u32[]{:S(2)}) copy-start(f32[3,64]{1,0:T(4,128)S(1)} %get-tuple-element.15) | copy-start | bytes 2308
  62.2 16.5 %copy-start.10 = (f32[3,64]{1,0:T(4,128)}, f32[3,64]{1,0:T(4,128)S(1)}, u32[]{:S(2)}) copy-start(f32[3,64]{1,0:T(4,128)S(1)} %get-tuple-element.16) | copy-start | bytes 2308
  73.6 93.1 %all-to-all-start.1 = ((bf16[4,64,256]{2,1,0:T(8,128)(2,1)}), bf16[4,64,256]{2,1,0:T(8,128)(2,1)S(1)}, u32[]{:S(2)}, u32[]{:S(2)}) async-start(bf16[4,64,256]{2,1,0:T(8,128)(2,1)} %copy.134), calls=%async_computation.1 | async-start | bytes 262144 | tf_op jit(solution)/shard_map/all_to_all | solution.py:84
  78.2 42.5 %copy-start.2 = (bf16[4096,64]{0,1:T(8,128)(2,1)S(1)}, bf16[4096,64]{0,1:T(8,128)(2,1)}, u32[]{:S(2)}) copy-start(bf16[4096,64]{0,1:T(8,128)(2,1)} %param.42) | copy-start | bytes 1572868
  78.6 8.2 %copy-start.8 = (f32[8,8]{1,0:T(8,128)S(1)}, f32[8,8]{1,0:T(8,128)}, u32[]{:S(2)}) copy-start(f32[8,8]{1,0:T(8,128)} %mul.334) | copy-start | bytes 772
  150.7 12.9 %copy-start.9 = (f32[2048]{0:T(1024)S(1)}, f32[2048]{0:T(1024)}, u32[]{:S(2)}) copy-start(f32[2048]{0:T(1024)} %param.43) | copy-start | bytes 24580
  150.7 12.9 %copy-start.14 = (pred[3,32]{1,0:T(4,128)(4,1)S(1)}, pred[3,32]{1,0:T(4,128)(4,1)}, u32[]{:S(2)}) copy-start(pred[3,32]{1,0:T(4,128)(4,1)} %copy-done.13) | copy-start | bytes 292
  151.0 14.7 %copy-start.11 = (f32[3,64]{1,0:T(4,128)S(1)}, f32[3,64]{1,0:T(4,128)}, u32[]{:S(2)}) copy-start(f32[3,64]{1,0:T(4,128)} %copy-done.10) | copy-start | bytes 2308
  155.2 11.5 %copy-start.4 = (f32[3,2048]{1,0:T(4,128)}, f32[3,2048]{1,0:T(4,128)S(1)}, u32[]{:S(2)}) copy-start(f32[3,2048]{1,0:T(4,128)S(1)} %get-tuple-element.18) | copy-start | bytes 73732
  156.7 6.9 %copy-start.15 = (f32[3]{0:T(128)S(1)}, f32[3]{0:T(128)}, u32[]{:S(2)}) copy-start(f32[3]{0:T(128)} %add_rsqrt_fusion.2) | copy-start | bytes 40
  158.5 20.1 %copy-start.3 = (f32[3,64,128]{2,1,0:T(8,128)S(1)}, f32[3,64,128]{2,1,0:T(8,128)}, u32[]{:S(2)}) copy-start(f32[3,64,128]{2,1,0:T(8,128)} %broadcast_bitcast_fusion) | copy-start | bytes 294916
  169.0 33.6 %all-to-all-start.2 = ((bf16[32,2,2432]{2,1,0:T(2,128)(2,1)}), bf16[32,2,2432]{2,1,0:T(2,128)(2,1)S(1)}, u32[]{:S(2)}, u32[]{:S(2)}) async-start(bf16[32,2,2432]{2,1,0:T(2,128)(2,1)} %pad_maximum_fusion), calls=%async_computation.2 | async-start | bytes 622592 | tf_op jit(solution)/shard_map/all_to_all | solution.py:187
  178.5 24.5 %copy-start.5 = (f32[3,2048]{1,0:T(4,128)S(1)}, f32[3,2048]{1,0:T(4,128)}, u32[]{:S(2)}) copy-start(f32[3,2048]{1,0:T(4,128)} %copy-done.4) | copy-start | bytes 73732
  178.5 24.9 %copy-start.16 = (f32[3]{0:T(128)S(1)}, f32[3]{0:T(128)}, u32[]{:S(2)}) copy-start(f32[3]{0:T(128)} %add_rsqrt_fusion.2) | copy-start | bytes 40

commit v2 on v1

--- a/solution.py
+++ b/solution.py
@@ -2,6 +2,8 @@
 import jax.numpy as jnp
 from jax import lax
 from jax.sharding import Mesh
+from jax.experimental import pallas as pl
+from jax.experimental.pallas import tpu as pltpu
 from jax.sharding import PartitionSpec as P
 
 HEAD_DIM = 64
@@ -11,6 +13,9 @@
 EP = ("zh", "zl", "core")
 NEAR = ("zl", "core")
 GRP_EP = ("grp",) + EP
+NEAR_FIRST = NEAR + ("zh",)
+SLAB = 4
+LANES = 128
 
 epsilon = 1e-06
 routed_scale = 2.5
@@ -34,6 +39,147 @@
     high = values.astype(jnp.bfloat16)
     low = (values - high.astype(jnp.float32)).astype(jnp.bfloat16)
     return high, low
+
+
+def near_gather(shard):
+    count = lax.axis_size("zh")
+    across = lax.all_to_all(
+        jnp.broadcast_to(shard[None], (count, *shard.shape)), "zh", 0, 0, tiled=True
+    )
+    return lax.all_gather(across, NEAR)
+
+
+def expert_kernel(
+    place,
+    resid,
+    gain,
+    chosen,
+    near_weights,
+    gate_hbm,
+    up_hbm,
+    down_hbm,
+    out,
+    own,
+    gate,
+    up,
+    down,
+    wide,
+    routed,
+    shared,
+    partial,
+    gate_sem,
+    up_sem,
+    down_sem,
+):
+    near, far, features, lanes = resid.shape
+    width = near * far * features
+    units = down.shape[0]
+    half = width // 2
+    copies = []
+    for part in range(2):
+        span = pl.ds(part * half, half)
+        copies.append(
+            (
+                pltpu.make_async_copy(gate_hbm.at[0, span], gate.at[span], gate_sem.at[part]),
+                pltpu.make_async_copy(up_hbm.at[0, span], up.at[span], up_sem.at[part]),
+            )
+        )
+    down_copy = pltpu.make_async_copy(down_hbm.at[0], down, down_sem)
+    for pair in copies:
+        for copy in pair:
+            copy.start()
+    down_copy.start()
+
+    square = jnp.zeros((lanes, 1), jnp.float32)
+    for z in range(far):
+        for pair in range(near // 2):
+            block = jnp.concatenate([resid[2 * pair, z], resid[2 * pair + 1, z]], axis=0)
+            rows = block.astype(jnp.float32).T
+            start = (z * near + 2 * pair) * features
+            wide[:, start : start + 2 * features] = rows
+            square += jnp.sum(rows * rows, axis=1, keepdims=True)
+    scale = lax.rsqrt(square / width + epsilon)
+    values = wide[...]
+    routed[...] = (values * scale * gain[...]).astype(jnp.bfloat16)
+    shared[...] = (values * gain[...]).astype(jnp.bfloat16)
+
+    me = place[0]
+    count = chosen.shape[0]
+    slabs = chosen.shape[1]
+    for row in range(own.shape[0]):
+        own[row : row + 1, :] = wide[pl.ds(me * slabs + row, 1), :]
+    block = near * features
+    start = pl.multiple_of((me // near) * block, block)
+    pre = jnp.dot(
+        shared[:, pl.ds(start, block)], near_weights[...], preferred_element_type=jnp.float32
+    )
+    for s in range(CAP):
+        partial[s] = pre[:, s * LANES : (s + 1) * LANES]
+    for s in range(CAP):
+        for row in range(slabs):
+            out[s * count : (s + 1) * count, width + row * LANES : width + (row + 1) * LANES] = (
+                partial[s, pl.ds(row, count, stride=slabs), :]
+            ).astype(jnp.bfloat16)
+
+    gate_pre = jnp.zeros((lanes, units), jnp.float32)
+    up_pre = jnp.zeros((lanes, units), jnp.float32)
+    for part in range(2):
+        span = slice(part * half, (part + 1) * half)
+        for copy in copies[part]:
+            copy.wait()
+        gate_pre += jnp.dot(routed[:, span], gate[span], preferred_element_type=jnp.float32)
+        up_pre += jnp.dot(routed[:, span], up[span], preferred_element_type=jnp.float32)
+    expert_hidden = (gate_pre / (1.0 + jnp.exp(-gate_pre)) * up_pre).astype(jnp.bfloat16)
+
+    lane = lax.broadcasted_iota(jnp.int32, (count, lanes), 1)
+    line = lax.broadcasted_iota(jnp.int32, (count, lanes), 0)
+    flags = chosen[...]
+    down_copy.wait()
+    for s in range(CAP):
+        pick = jnp.zeros((count, lanes), jnp.float32)
+        earlier = jnp.zeros((count, 1), jnp.float32)
+        for row in range(slabs):
+            flag = flags[:, row : row + 1]
+            taken = jnp.where(earlier == float(s), flag, 0.0)
+            pick = jnp.where(lane == line * slabs + row, taken, pick)
+            earlier = earlier + flag
+        rows = jnp.dot(
+            pick.astype(jnp.bfloat16), expert_hidden, preferred_element_type=jnp.float32
+        ).astype(jnp.bfloat16)
+        out[s * count : (s + 1) * count, :width] = jnp.dot(
+            rows, down[...], preferred_element_type=jnp.float32
+        ).astype(jnp.bfloat16)
+
+
+def expert_rows(place, resid, gain, chosen, near_weights, gate, up, down):
+    near, far, features, lanes = resid.shape
+    width = near * far * features
+    units = down.shape[1]
+    count, slabs = chosen.shape
+    vmem = pl.BlockSpec(memory_space=pltpu.VMEM)
+    hbm = pl.BlockSpec(memory_space=pltpu.HBM)
+    return pl.pallas_call(
+        expert_kernel,
+        name="expert_rows",
+        out_shape=(
+            jax.ShapeDtypeStruct((CAP * count, width + slabs * LANES), jnp.bfloat16),
+            jax.ShapeDtypeStruct((slabs, width), jnp.float32),
+        ),
+        in_specs=[pl.BlockSpec(memory_space=pltpu.SMEM), vmem, vmem, vmem, vmem, hbm, hbm, hbm],
+        out_specs=(vmem, vmem),
+        scratch_shapes=[
+            pltpu.VMEM((width, units), jnp.bfloat16),
+            pltpu.VMEM((width, units), jnp.bfloat16),
+            pltpu.VMEM((units, width), jnp.bfloat16),
+            pltpu.VMEM((lanes, width), jnp.float32),
+            pltpu.VMEM((lanes, width), jnp.bfloat16),
+            pltpu.VMEM((lanes, width), jnp.bfloat16),
+            pltpu.VMEM((CAP, lanes, near_weights.shape[1] // CAP), jnp.float32),
+            pltpu.SemaphoreType.DMA((2,)),
+            pltpu.SemaphoreType.DMA((2,)),
+            pltpu.SemaphoreType.DMA,
+        ],
+    )(place, resid, gain, chosen, near_weights, gate, up, down)
 
 
 def shards(
@@ -84,8 +230,8 @@
     near_weights = lax.all_to_all(near_weights, NEAR, 0, 0, tiled=True)
     near_weights = near_weights.reshape(near * features, 2 * near_units)
 
-    gathered = lax.all_gather(hidden, EP)
-    gathered_wide = jnp.moveaxis(gathered, 0, 1).reshape(rows * count, width).astype(jnp.float32)
+    slab = jnp.pad(hidden, ((0, SLAB - rows), (0, 0)))
+    gathered_wide = near_gather(slab).reshape(count * SLAB, width).astype(jnp.float32)
     normed = (gathered_wide * row_scale(gathered_wide) * mix_gain).astype(jnp.bfloat16)
     member = jnp.any(
         expert_ids[:, :, None] == jnp.arange(experts, dtype=jnp.int32)[None, None, :], axis=1
@@ -99,9 +245,18 @@
         ],
         axis=1,
     )
-    parts = jnp.moveaxis(parts.reshape(rows, count, -1), 1, 0)
-    named = member.astype(jnp.bfloat16).T.reshape(count, rows, 1)
-    pieces = lax.all_to_all(jnp.concatenate([parts, named], axis=2), EP, 0, 0, tiled=True)
+    far = lax.axis_size("zh")
+    named = jnp.pad(member.astype(jnp.bfloat16), ((0, SLAB - rows), (0, 0)))
+    named = named.reshape(SLAB, far, near).transpose(2, 1, 0).reshape(count, SLAB, 1)
+    pieces = lax.all_to_all(
+        jnp.concatenate([parts.reshape(count, SLAB, -1), named], axis=2),
+        NEAR_FIRST,
+        0,
+        0,
+        tiled=True,
+    )
+    pieces = pieces.reshape(near, far, SLAB, -1).transpose(1, 0, 2, 3).reshape(count, SLAB, -1)
+    pieces = pieces[:, :rows]
 
     hidden_wide = hidden.astype(jnp.float32)
     normed_local = (hidden_wide * row_scale(hidden_wide) * mix_gain).astype(jnp.bfloat16)
@@ -115,7 +270,7 @@
         )
         start += size
     gate_rows, input_rows, write_rows, read_rows = fields
-    chosen = pieces[:, :, start].T.reshape(1, rows * count)
+    chosen = pieces[:, :, start].astype(jnp.float32)
 
     inner_width = gate_rows.shape[1]
     state_span = GROUPS * STATE
@@ -150,47 +305,27 @@
     )
 
     col_width = out_proj.shape[1]
-    gated_all = jnp.moveaxis(lax.all_gather(gated_out, EP), 0, 1).reshape(rows * count, inner_width)
-    resid_cols = lax.dynamic_slice_in_dim(gathered_wide, index * col_width, col_width, 1).T
+    gated_all = lax.all_gather(gated_out, EP).reshape(count * rows, inner_width)
+    resid_cols = lax.dynamic_slice_in_dim(gathered_wide, index * col_width, col_width, 1)
+    resid_cols = resid_cols.reshape(near, far, SLAB, col_width)[:, :, :rows].transpose(3, 1, 0, 2)
+    resid_cols = resid_cols.reshape(col_width, count * rows)
     resid_part = (resid_cols + contract(out_proj, gated_all, 0, 1)).astype(jnp.bfloat16)
-    resid_all = lax.all_gather(resid_part, EP).reshape(width, rows * count)
-
-    resid_wide = resid_all.astype(jnp.float32)
-    norm_all = lax.rsqrt(jnp.mean(resid_wide * resid_wide, axis=0, keepdims=True) + epsilon)
-    routed_in = (resid_wide * norm_all * ffn_gain[:, None]).astype(jnp.bfloat16)
-    shared_in = (resid_wide * ffn_gain[:, None]).astype(jnp.bfloat16)
-
-    order = jnp.arange(rows * count, dtype=jnp.int32)[None]
-    chosen_rows = chosen.reshape(rows, count)
-    earlier = (jnp.cumsum(chosen_rows, axis=0) - chosen_rows).reshape(1, rows * count)
-    slot = jnp.arange(CAP * count, dtype=jnp.int32)[:, None]
-    pick = (
-        (slot % count == order % count)
-        & (chosen > 0.5)
-        & (earlier.astype(jnp.int32) == slot // count)
-    ).astype(jnp.bfloat16)
-    expert_hidden = (
-        jax.nn.silu(contract(routed_in, expert_gate[0], 0, 0))
-        * contract(routed_in, expert_up[0], 0, 0)
-    ).astype(jnp.bfloat16)
-    expert_rows = matmul(pick, expert_hidden).astype(jnp.bfloat16)
-    result = matmul(expert_rows, expert_down[0]).astype(jnp.bfloat16)
-
-    block = near * features
-    shared_block = lax.dynamic_slice_in_dim(shared_in, (index // near) * block, block, 0)
-    shared_part = contract(shared_block, near_weights, 0, 0).astype(jnp.bfloat16)
-    shared_part = shared_part.reshape(rows, count, 2, near_units)
-    shared_part = shared_part.transpose(1, 2, 0, 3).reshape(count, CAP, rows * near_units)
-    outbound = jnp.concatenate(
-        [jnp.moveaxis(result.reshape(CAP, count, width), 1, 0), shared_part], axis=2
-    )
+    resid_part = jnp.pad(resid_part, ((0, 0), (0, LANES - count * rows)))
+    resid_all = near_gather(resid_part)
+
+    outbound, resid_own = expert_rows(
+        index.astype(jnp.int32).reshape(1),
+        resid_all,
+        ffn_gain.reshape(1, width),
+        chosen,
+        near_weights,
+        expert_gate,
+        expert_up,
+        expert_down,
+    )
+    outbound = jnp.moveaxis(outbound.reshape(CAP, count, -1), 1, 0)
     returned = lax.all_to_all(outbound, EP, 0, 0, tiled=True)
 
-    own = (
-        jnp.arange(rows * count, dtype=jnp.int32)[None]
-        == jnp.arange(rows, dtype=jnp.int32)[:, None] * count + index
-    ).astype(jnp.bfloat16)
-    resid_own = contract(own, resid_all, 1, 1)
     norm_scale = row_scale(resid_own)
     routed_own = (resid_own * norm_scale * ffn_gain).astype(jnp.bfloat16)
     scores = jnp.where(member, jax.nn.sigmoid(matmul(routed_own, router)), 0.0)

time: 207 us -> 186 us (0.90)
  blocking collectives: 103 us -> 50.4 us
  waiting for transfers between devices: 17.7 us -> 41.6 us
  starting transfers between devices: 20.1 us -> 39.4 us
  matrix products: 24 us -> 13.6 us
  other arithmetic: 23.7 us -> 16.2 us
  Pallas kernels: 0 us -> 5.93 us
    all_gather x3, blocking collectives: 103 us -> 50.4 us  [the longest x1 31.8 us: shards(): gated_all = lax.all_gather(gated_out, EP).reshape(count * rows, inner_width)]
    all_to_all x1 -> x3, waiting for transfers between devices: 1.45 us -> 25.2 us  [the longest x2 14.1 us: near_gather(): lax.all_to_all(jnp.broadcast_to(shard[None], (count, *shard.shape)), 'zh'...]
    all_to_all x1 -> x3, starting transfers between devices: 5.98 us -> 28.6 us  [the longest x2 22.2 us: near_gather(): lax.all_to_all(jnp.broadcast_to(shard[None], (count, *shard.shape)), 'zh'...]
    dot_general x11 -> x9, matrix products: 13.7 us -> 7.15 us  [matmul(): return jnp.dot(left, right, preferred_element_type=jnp.float32)]
    pallas_call x0 -> x1, Pallas kernels: none -> 5.93 us  [expert_rows(): pl.pallas_call(expert_kernel, name='expert_rows', out_shape=(jax.ShapeDty...]
    all_to_all x1, starting transfers between devices: 9.49 us -> 4.19 us  [shards(): returned = lax.all_to_all(outbound, EP, 0, 0, tiled=True)]
    dot_general x4 -> x1, matrix products: 5.53 us -> 1.7 us  [contract(): lax.dot_general(left, right, (((left_dim,), (right_dim,)), ((), ())), pre...]
    reshape x9, local copies, waits for them, and re-layouts: 1.49 us -> 4.45 us  [the longest x1 1.92 us: shards(): outbound = jnp.moveaxis(outbound.reshape(CAP, count, -1), 1, 0)]
  transfers between devices with their start and end apart: 3 -> 5, of which waited for: 2 -> 4; matrix products, arithmetic and copies ran while one was open for 23% -> 12% of each run, Pallas kernels for 0% -> 0%
where the time goes in v2:
time: 186 us; the launch traced here: 185 us
  blocking collectives  50.4 us (27%)
  waiting for transfers between devices  41.6 us (22%)
  starting transfers between devices  39.4 us (21%)
  local copies, waits for them, and re-layouts  16.7 us (9%)
  other arithmetic  16.2 us (9%)
  matrix products  13.6 us (7%)
  Pallas kernels  5.93 us (3%)
    all_gather x1, blocking collectives, shards(): gated_all = lax.all_gather(gated_out, EP).reshape(count * rows, inner_width)  31.8 us
    all_to_all x2, starting transfers between devices, near_gather(): lax.all_to_all(jnp.broadcast_to(shard[None], (count, *shard.shape)), 'zh'...  22.2 us
    all_gather x2, blocking collectives, near_gather(): return lax.all_gather(across, NEAR)  18.7 us
    all_to_all x1, waiting for transfers between devices, shards(): returned = lax.all_to_all(outbound, EP, 0, 0, tiled=True)  16.4 us
    all_to_all x2, waiting for transfers between devices, near_gather(): lax.all_to_all(jnp.broadcast_to(shard[None], (count, *shard.shape)), 'zh'...  14.1 us
    all_to_all x1, waiting for transfers between devices, shards(): lax.all_to_all(jnp.concatenate([parts.reshape(count, SLAB, -1), named], a...  11.1 us
    dot_general x9, matrix products, matmul(): return jnp.dot(left, right, preferred_element_type=jnp.float32)  7.15 us
    add x1, other arithmetic, shards(): decay_rate[..., None, None] * carried  6.98 us
  transfers between devices with their start and end apart: 5, of which 4 were waited for; matrix products, arithmetic and copies ran while one was open for 12% of the time, Pallas kernels for 0%

profile of v2, /device:TPU:69, one launch (start us, length us, event | category | flops | bytes accessed | tf_op | source)
XLA Modules:
  0.0 185.0 jit_solution(5868641287902598071)
XLA Ops:
  0.7 0.9 pad.13
  2.2 17.3 %all-to-all-start = ((bf16[8,4,2048]{2,1,0:T(4,128)(2,1)}), bf16[8,4,2048]{2,1,0:T(4,128)(2,1)S(1)}, u32[]{:S(2)}, u32[]{:S(2)}) async-start(bf16[8,4,2048]{2,1,0:T(4,128)(2,1)} %broadcast_in_dim.11), calls=%async_computation | async-start | bytes 262144 | tf_op jit(solution)/shard_map/all_to_all | solution.py:46
  21.8 1.3 subtract_exponential_fusion
  25.6 1.3 mul.280
  27.5 0.9 bitcast_bitcast_fusion
  29.1 3.8 %all-to-all-done = bf16[8,4,2048]{2,1,0:T(4,128)(2,1)S(1)} async-done(((bf16[8,4,2048]{2,1,0:T(4,128)(2,1)}), bf16[8,4,2048]{2,1,0:T(4,128)(2,1)S(1)}, u32[]{:S(2)}, u32[]{:S(2)}) %all-to-all-start) | async-done | bytes 131104 | tf_op jit(solution)/shard_map/all_to_all | solution.py:46
  32.9 10.1 %all-gather = bf16[32,4,2048]{2,1,0:T(4,128)(2,1)S(1)} all-gather(bf16[8,4,2048]{2,1,0:T(4,128)(2,1)S(1)} %all-to-all-done), channel_id=2, replica_groups=mesh['grp'=4,'zh'=8,'zl'=2,'core'=2] {'zl','core'}, dimensions={0}, use_global_device_ids=true | all-gather | bytes 655360 | tf_op jit(solution)/shard_map/all_gather | solution.py:49
  43.0 1.0 reshape.276
  44.5 1.4 multiply_convert_fusion
  45.9 1.2 convolution_convert_fusion.2
  47.0 1.2 convolution_convert_fusion.3
  48.6 1.4 convolution_convert_fusion.1
  51.0 6.4 %all-to-all-start.1 = ((bf16[32,4,321]{2,1,0:T(4,128)(2,1)}), bf16[32,4,321]{2,1,0:T(4,128)(2,1)S(1)}, u32[]{:S(2)}, u32[]{:S(2)}) async-start(bf16[32,4,321]{2,1,0:T(4,128)(2,1)} %pad_maximum_fusion.2), calls=%async_computation.1 | async-start | bytes 196608 | tf_op jit(solution)/shard_map/all_to_all | solution.py:251
  57.3 0.9 constant_dynamic-slice_fusion
  59.0 11.1 %all-to-all-done.1 = bf16[32,4,321]{2,1,0:T(4,128)(2,1)S(1)} async-done(((bf16[32,4,321]{2,1,0:T(4,128)(2,1)}), bf16[32,4,321]{2,1,0:T(4,128)(2,1)S(1)}, u32[]{:S(2)}, u32[]{:S(2)}) %all-to-all-start.1) | async-done | bytes 82208 | tf_op jit(solution)/shard_map/all_to_all | solution.py:251
  72.3 4.7 %fusion = f32[3,8,1,8,64]{4,2,3,1,0:T(1,128)S(1)} fusion(f32[3,8,128,1,1]{2,3,4,1,0:T(1,128)S(1)} %bitcast.146, f32[3,8,8,64,128]{4,3,2,1,0:T(8,128)} %bitcast.130, f32[3,8,128]{2,1,0:T(8,128)S(1)} %bitcast.143, f32[3,8,8,64]{3,2,1,0:T(8,128)S(1)} %broadcast_multiply_fusion.1, f32[3,8,8]{2,1,0:T(8,128)} %mul.262), kind=kOutput, calls=%fused_computation.1 | convolution fusion | flops 7864320 | bytes 6415104 | tf_op jit(solution)/shard_map/sgepn,sgn->sgep/dot_general | solution.py:298
  77.6 31.8 %all_gather.18 = bf16[32,3,4096]{2,1,0:T(4,128)(2,1)S(1)} all-gather(bf16[1,3,4096]{2,1,0:T(4,128)(2,1)S(1)} %multiply_convert_fusion.1), channel_id=1, replica_groups=mesh['grp'=4,'zh'=8,'zl'=2,'core'=2] {'zh','zl','core'}, dimensions={0}, use_global_device_ids=true | all-gather | bytes 811008 | tf_op jit(solution)/shard_map/all_gather | solution.py:308
  109.3 1.4 reshape.268
  110.8 1.7 fusion.10
  113.1 5.0 %all-to-all-start.2 = ((bf16[8,64,128]{2,1,0:T(8,128)(2,1)}), bf16[8,64,128]{2,1,0:T(8,128)(2,1)S(1)}, u32[]{:S(2)}, u32[]{:S(2)}) async-start(bf16[8,64,128]{2,1,0:T(8,128)(2,1)} %broadcast_in_dim.13), calls=%async_computation.2 | async-start | bytes 262144 | tf_op jit(solution)/shard_map/all_to_all | solution.py:46
  118.1 0.9 copy.134
  119.0 1.0 broadcast_multiply_fusion
  120.0 0.9 fusion.15
  120.9 10.3 %all-to-all-done.2 = bf16[8,64,128]{2,1,0:T(8,128)(2,1)S(1)} async-done(((bf16[8,64,128]{2,1,0:T(8,128)(2,1)}), bf16[8,64,128]{2,1,0:T(8,128)(2,1)S(1)}, u32[]{:S(2)}, u32[]{:S(2)}) %all-to-all-start.2) | async-done | bytes 131104 | tf_op jit(solution)/shard_map/all_to_all | solution.py:46
  131.2 6.6 %all-to-all-start.3 = ((bf16[4,64,256]{2,1,0:T(8,128)(2,1)}), bf16[4,64,256]{2,1,0:T(8,128)(2,1)S(1)}, u32[]{:S(2)}, u32[]{:S(2)}) async-start(bf16[4,64,256]{2,1,0:T(8,128)(2,1)} %pad_maximum_fusion.1), calls=%async_computation.3 | async-start | bytes 262144 | tf_op jit(solution)/shard_map/all_to_all | solution.py:230
  137.8 8.6 %all-gather.1 = bf16[32,64,128]{2,1,0:T(8,128)(2,1)} all-gather(bf16[8,64,128]{2,1,0:T(8,128)(2,1)S(1)} %all-to-all-done.2), channel_id=3, replica_groups=mesh['grp'=4,'zh'=8,'zl'=2,'core'=2] {'zl','core'}, dimensions={0}, use_global_device_ids=true | all-gather | bytes 655360 | tf_op jit(solution)/shard_map/all_gather | solution.py:49
  147.0 5.9 %expert_rows.1 = (bf16[64,2432]{1,0:T(8,128)(2,1)}, f32[3,2048]{1,0:T(4,128)}) custom-call(s32[1]{0:T(128)} %bitcast.place, bf16[4,8,64,128]{3,2,1,0:T(8,128)(2,1)} %bitcast.133, f32[1,2048]{1,0:T(1,128)} %bitcast.149, f32[32,3]{1,0:T(8,128)} %bitcast.145, bf16[256,256]{1,0:T(8,128)(2,1)} %bitcast.138, bf16[1,2048,512]{2,1,0:T(8,128)(2,1)} %gate_hbm.1, ...), custom_call_target="tpu_custom_call" | custom-call | tf_op jit(solution)/shard_map/expert_rows/pallas_call | solution.py:161
  153.0 1.9 %copy.151 = bf16[2,32,2432]{2,0,1:T(2,128)(2,1)} copy(bf16[2,32,2432]{2,1,0:T(8,128)(2,1)} %bitcast.141) | data formatting | bytes 622592 | tf_op jit(solution)/shard_map/reshape | solution.py:326
  154.9 4.2 %all-to-all-start.4 = ((bf16[32,2,2432]{2,1,0:T(2,128)(2,1)}), bf16[32,2,2432]{2,1,0:T(2,128)(2,1)S(1)}, u32[]{:S(2)}, u32[]{:S(2)}) async-start(bf16[32,2,2432]{2,1,0:T(2,128)(2,1)} %bitcast.127), calls=%async_computation.4 | async-start | bytes 622592 | tf_op jit(solution)/shard_map/all_to_all | solution.py:327
  159.2 7.0 %multiply_add_fusion = f32[3,64,64,128]{3,2,1,0:T(8,128)} fusion(f32[3,64,64,128]{3,2,1,0:T(8,128)} %param.28, f32[3,64,128]{2,1,0:T(8,128)S(1)} %broadcast_bitcast_fusion, f32[3,64,64]{2,1,0:T(8,128)S(1)} %broadcast_multiply_fusion, f32[3,64]{1,0:T(4,128)S(1)} %copy-done.14), kind=kLoop, calls=%fused_computation | loop fusion | flops 4718592 | bytes 12731136 | tf_op jit(solution)/shard_map/add | solution.py:295
  166.7 16.4 %all-to-all-done.4 = bf16[32,2,2432]{2,1,0:T(2,128)(2,1)S(1)} async-done(((bf16[32,2,2432]{2,1,0:T(2,128)(2,1)}), bf16[32,2,2432]{2,1,0:T(2,128)(2,1)S(1)}, u32[]{:S(2)}, u32[]{:S(2)}) %all-to-all-start.4) | async-done | bytes 311328 | tf_op jit(solution)/shard_map/all_to_all | solution.py:327
  184.0 1.0 fusion.8
  (106 shorter events, 14.5 us)
Async XLA Ops:
  0.6 183.3 %copy-start = (bf16[512,2048]{1,0:T(8,128)(2,1)S(1)}, bf16[512,2048]{1,0:T(8,128)(2,1)}, u32[]{:S(2)}) copy-start(bf16[512,2048]{1,0:T(8,128)(2,1)} %param.51) | copy-start | bytes 6291460
  0.6 47.6 %copy-start.3 = (bf16[2048,128]{1,0:T(8,128)(2,1)S(1)}, bf16[2048,128]{1,0:T(8,128)(2,1)}, u32[]{:S(2)}) copy-start(bf16[2048,128]{1,0:T(8,128)(2,1)} %param.30) | copy-start | bytes 1572868
  0.7 70.0 %copy-start.1 = (bf16[3,3,6144]{2,1,0:T(4,128)(2,1)S(1)}, bf16[3,3,6144]{2,1,0:T(4,128)(2,1)}, u32[]{:S(2)}) copy-start(bf16[3,3,6144]{2,1,0:T(4,128)(2,1)} %param.27) | copy-start | bytes 331780
  2.2 30.6 %all-to-all-start = ((bf16[8,4,2048]{2,1,0:T(4,128)(2,1)}), bf16[8,4,2048]{2,1,0:T(4,128)(2,1)S(1)}, u32[]{:S(2)}, u32[]{:S(2)}) async-start(bf16[8,4,2048]{2,1,0:T(4,128)(2,1)} %broadcast_in_dim.11), calls=%async_computation | async-start | bytes 262144 | tf_op jit(solution)/shard_map/all_to_all | solution.py:46
  21.1 1.9 %copy-start.15 = (pred[3,32]{1,0:T(4,128)(4,1)}, pred[3,32]{1,0:T(4,128)(4,1)S(1)}, u32[]{:S(2)}) copy-start(pred[3,32]{1,0:T(4,128)(4,1)S(1)} %fusion.31) | copy-start | bytes 292
  23.1 4.5 %copy-start.10 = (f32[3,64]{1,0:T(4,128)}, f32[3,64]{1,0:T(4,128)S(1)}, u32[]{:S(2)}) copy-start(f32[3,64]{1,0:T(4,128)S(1)} %get-tuple-element.18) | copy-start | bytes 2308
  23.1 4.5 %copy-start.13 = (f32[3,64]{1,0:T(4,128)}, f32[3,64]{1,0:T(4,128)S(1)}, u32[]{:S(2)}) copy-start(f32[3,64]{1,0:T(4,128)S(1)} %get-tuple-element.17) | copy-start | bytes 2308
  44.4 26.6 %copy-start.6 = (f32[6144]{0:T(1024)S(1)}, f32[6144]{0:T(1024)}, u32[]{:S(2)}) copy-start(f32[6144]{0:T(1024)} %param.39) | copy-start | bytes 73732
  44.4 27.8 %copy-start.5 = (f32[3,8,8]{2,1,0:T(8,128)S(1)}, f32[3,8,8]{2,1,0:T(8,128)}, u32[]{:S(2)}) copy-start(f32[3,8,8]{2,1,0:T(8,128)} %mul.265) | copy-start | bytes 2308
  48.3 28.7 %copy-start.7 = (f32[8,8]{1,0:T(8,128)S(1)}, f32[8,8]{1,0:T(8,128)}, u32[]{:S(2)}) copy-start(f32[8,8]{1,0:T(8,128)} %mul.280) | copy-start | bytes 772
  48.6 28.9 %copy-start.8 = (f32[4096]{0:T(1024)S(1)}, f32[4096]{0:T(1024)}, u32[]{:S(2)}) copy-start(f32[4096]{0:T(1024)} %param.41) | copy-start | bytes 49156
  51.0 19.2 %all-to-all-start.1 = ((bf16[32,4,321]{2,1,0:T(4,128)(2,1)}), bf16[32,4,321]{2,1,0:T(4,128)(2,1)S(1)}, u32[]{:S(2)}, u32[]{:S(2)}) async-start(bf16[32,4,321]{2,1,0:T(4,128)(2,1)} %pad_maximum_fusion.2), calls=%async_computation.1 | async-start | bytes 196608 | tf_op jit(solution)/shard_map/all_to_all | solution.py:251
  72.2 46.9 %copy-start.11 = (f32[3,64]{1,0:T(4,128)S(1)}, f32[3,64]{1,0:T(4,128)}, u32[]{:S(2)}) copy-start(f32[3,64]{1,0:T(4,128)} %copy-done.10) | copy-start | bytes 2308
  110.8 48.3 %copy-start.14 = (f32[3,64]{1,0:T(4,128)S(1)}, f32[3,64]{1,0:T(4,128)}, u32[]{:S(2)}) copy-start(f32[3,64]{1,0:T(4,128)} %copy-done.13) | copy-start | bytes 2308
  113.1 18.0 %all-to-all-start.2 = ((bf16[8,64,128]{2,1,0:T(8,128)(2,1)}), bf16[8,64,128]{2,1,0:T(8,128)(2,1)S(1)}, u32[]{:S(2)}, u32[]{:S(2)}) async-start(bf16[8,64,128]{2,1,0:T(8,128)(2,1)} %broadcast_in_dim.13), calls=%async_computation.2 | async-start | bytes 262144 | tf_op jit(solution)/shard_map/all_to_all | solution.py:46
  131.2 15.2 %all-to-all-start.3 = ((bf16[4,64,256]{2,1,0:T(8,128)(2,1)}), bf16[4,64,256]{2,1,0:T(8,128)(2,1)S(1)}, u32[]{:S(2)}, u32[]{:S(2)}) async-start(bf16[4,64,256]{2,1,0:T(8,128)(2,1)} %pad_maximum_fusion.1), calls=%async_computation.3 | async-start | bytes 262144 | tf_op jit(solution)/shard_map/all_to_all | solution.py:230
  146.4 0.6 copy-start.2
  154.9 28.2 %all-to-all-start.4 = ((bf16[32,2,2432]{2,1,0:T(2,128)(2,1)}), bf16[32,2,2432]{2,1,0:T(2,128)(2,1)S(1)}, u32[]{:S(2)}, u32[]{:S(2)}) async-start(bf16[32,2,2432]{2,1,0:T(2,128)(2,1)} %bitcast.127), calls=%async_computation.4 | async-start | bytes 622592 | tf_op jit(solution)/shard_map/all_to_all | solution.py:327
  159.1 7.0 %copy-start.4 = (f32[3,2048]{1,0:T(4,128)S(1)}, f32[3,2048]{1,0:T(4,128)}, u32[]{:S(2)}) copy-start(f32[3,2048]{1,0:T(4,128)} %get-tuple-element.5) | copy-start | bytes 73732
  159.1 7.2 %copy-start.9 = (f32[2048]{0:T(1024)S(1)}, f32[2048]{0:T(1024)}, u32[]{:S(2)}) copy-start(f32[2048]{0:T(1024)} %param.43) | copy-start | bytes 24580
  159.1 7.2 %copy-start.16 = (pred[3,32]{1,0:T(4,128)(4,1)S(1)}, pred[3,32]{1,0:T(4,128)(4,1)}, u32[]{:S(2)}) copy-start(pred[3,32]{1,0:T(4,128)(4,1)} %copy-done.15) | copy-start | bytes 292
  159.1 7.2 %copy-start.17 = (bf16[2048,32]{0,1:T(8,128)(2,1)S(1)}, bf16[2048,32]{0,1:T(8,128)(2,1)}, u32[]{:S(2)}) copy-start(bf16[2048,32]{0,1:T(8,128)(2,1)} %param.44) | copy-start | bytes 393220
  159.1 7.5 %copy-start.12 = (s32[3,32]{1,0:T(4,128)S(1)}, s32[3,32]{1,0:T(4,128)}, u32[]{:S(2)}) copy-start(s32[3,32]{1,0:T(4,128)} %reduce_window_sum.11) | copy-start | bytes 1156

commit v3 on v1

v3 whole, which is shorter than its diff:
```python
import jax
import jax.numpy as jnp
from jax import lax
from jax.sharding import Mesh
from jax.experimental import pallas as pl
from jax.experimental.pallas import tpu as pltpu
from jax.sharding import PartitionSpec as P

HEAD_DIM = 64
GROUPS = 8
STATE = 128
CAP = 2
EP = ("zh", "zl", "core")
NEAR = ("zl", "core")
GRP_EP = ("grp",) + EP
LANES = 128

epsilon = 1e-06
routed_scale = 2.5


def row_scale(values):
    return lax.rsqrt(jnp.mean(values * values, axis=-1, keepdims=True) + epsilon)


def matmul(left, right):
    return jnp.dot(left, right, preferred_element_type=jnp.float32)


def contract(left, right, left_dim, right_dim):
    return lax.dot_general(
        left, right, (((left_dim,), (right_dim,)), ((), ())), preferred_element_type=jnp.float32
    )


def split_pair(values):
    high = values.astype(jnp.bfloat16)
    low = (values - high.astype(jnp.float32)).astype(jnp.bfloat16)
    return high, low


def near_gather(shard):
    count = lax.axis_size("zh")
    across = lax.all_to_all(
        jnp.broadcast_to(shard[None], (count, *shard.shape)), "zh", 0, 0, tiled=True
    )
    return lax.all_gather(across, NEAR)


def kept_in(space, arrays):
    return [pltpu.with_memory_space_constraint(array, space) for array in arrays]


def fast_call(kernel, name, outs, scratch, scalars, fetched, arrays, far=()):
    vmem = pl.BlockSpec(memory_space=pltpu.VMEM)
    smem = pl.BlockSpec(memory_space=pltpu.SMEM)
    hbm = pl.BlockSpec(memory_space=pltpu.HBM)
    specs = [smem] * len(scalars) + [vmem] * (len(fetched) + len(arrays)) + [hbm] * len(far)
    landing = [pltpu.VMEM(array.shape, array.dtype) for array in far]
    waits = [pltpu.SemaphoreType.DMA((len(far),))] if far else []
    return pl.pallas_call(
        kernel,
        name=name,
        out_shape=tuple(pltpu.VMEM(shape, dtype) for shape, dtype in outs),
        in_specs=specs,
        out_specs=(vmem,) * len(outs),
        scratch_shapes=[pltpu.VMEM(shape, dtype) for shape, dtype in scratch] + landing + waits,
        compiler_params=pltpu.CompilerParams(vmem_limit_bytes=24 * 1024 * 1024),
    )(*scalars, *kept_in(pltpu.HBM, fetched), *kept_in(pltpu.VMEM, arrays), *kept_in(pltpu.HBM, far))


def open_kernel(hidden, gate, up, out, staged):
    rows, width = hidden.shape
    chunks = width // LANES
    values = hidden[...].astype(jnp.float32)
    for k in range(chunks):
        staged[pl.ds(k, rows, stride=chunks), :] = values[:, k * LANES : (k + 1) * LANES]
    mine = staged[...].astype(jnp.bfloat16)
    gates = gate[...].astype(jnp.float32)
    ups = up[...].astype(jnp.float32)
    count = out.shape[0]
    half = gate.shape[1] // count
    for z in range(count):
        span = slice(z * half, (z + 1) * half)
        out[z, : rows * chunks, :] = mine
        out[z, rows * chunks :, :] = jnp.concatenate(
            [gates[:, span], ups[:, span]], axis=1
        ).astype(jnp.bfloat16)


def project_kernel(
    place,
    ids,
    gain,
    gathered,
    gate_hbm,
    input_hbm,
    write_hbm,
    read_hbm,
    message,
    columns,
    flat,
    wide,
    normed,
    staged,
    gate_weights,
    input_weights,
    write_weights,
    read_weights,
    sems,
):
    copies = [
        pltpu.make_async_copy(gate_hbm, gate_weights, sems.at[0]),
        pltpu.make_async_copy(input_hbm, input_weights, sems.at[1]),
        pltpu.make_async_copy(write_hbm, write_weights, sems.at[2]),
        pltpu.make_async_copy(read_hbm, read_weights, sems.at[3]),
    ]
    for copy in copies:
        copy.start()
    near, far, chunk, lanes = gathered.shape
    count = near * far
    rows = ids.shape[0]
    blocks = chunk // rows
    lines = message.shape[1]
    flat[...] = gathered[...].reshape(count * chunk, lanes).astype(jnp.float32)
    square = jnp.zeros((rows * count, 1), jnp.float32)
    for k in range(blocks):
        for row in range(rows):
            for n in range(near):
                wide[k, pl.ds(row * count + n, far, stride=near), :] = flat[
                    pl.ds(n * far * chunk + row * blocks + k, far, stride=chunk), :
                ]
        part = wide[k]
        square += jnp.sum(part * part, axis=1, keepdims=True)
    scale = lax.rsqrt(square / (blocks * lanes) + epsilon)
    for k in range(blocks):
        span = slice(k * lanes, (k + 1) * lanes)
        normed[:, span] = (wide[k] * scale * gain[:, span]).astype(jnp.bfloat16)
    values = normed[...]
    for copy in copies:
        copy.wait()
    gate_part = jnp.dot(values, gate_weights[...], preferred_element_type=jnp.float32)
    input_part = jnp.dot(values, input_weights[...], preferred_element_type=jnp.float32)
    write_part = contract(values, write_weights[...], 1, 1)
    read_part = contract(values, read_weights[...], 1, 1)

    def of_row(part, row):
        return part[row * count : (row + 1) * count]

    small = lanes - rows * write_part.shape[1]
    expert = lax.broadcasted_iota(jnp.int32, (count, small), 0)
    lane = lax.broadcasted_iota(jnp.int32, (count, small), 1)
    member = jnp.zeros((count, small), jnp.float32)
    for row in range(rows):
        for k in range(ids.shape[1]):
            member = jnp.where((lane == row) & (expert == ids[row, k]), 1.0, member)
    for row in range(rows):
        staged[pl.ds(row, count, stride=lines), :] = of_row(gate_part, row)
        staged[pl.ds(rows + row, count, stride=lines), :] = of_row(input_part, row)
    staged[pl.ds(2 * rows, count, stride=lines), :] = jnp.concatenate(
        [of_row(write_part, row) for row in range(rows)] + [member], axis=1
    )
    staged[pl.ds(2 * rows + 1, count, stride=lines), :] = jnp.concatenate(
        [of_row(read_part, row) for row in range(rows)] + [jnp.zeros_like(member)], axis=1
    )
    message[...] = staged[...].astype(jnp.bfloat16).reshape(count, lines, lanes)

    me = place[0]
    height = columns.shape[0]
    across = jnp.concatenate(
        [wide[me * height // lanes], jnp.zeros((lanes - rows * count, lanes), jnp.float32)], axis=0
    ).T
    columns[...] = jnp.where(me % 2 == 0, across[:height], across[height:])


def expert_kernel(
    place,
    gain,
    resid,
    chosen,
    part,
    gate_hbm,
    up_hbm,
    down_hbm,
    out,
    own,
    wide,
    routed,
    shared,
    staged,
    spread,
    gate,
    up,
    down,
    sems,
):
    near, far, features, lanes = resid.shape
    width = near * far * features
    count, slabs = chosen.shape
    lines = out.shape[1]
    copies = [
        pltpu.make_async_copy(gate_hbm, gate, sems.at[0]),
        pltpu.make_async_copy(up_hbm, up, sems.at[1]),
        pltpu.make_async_copy(down_hbm, down, sems.at[2]),
    ]
    for copy in copies:
        copy.start()
    square = jnp.zeros((lanes, 1), jnp.float32)
    for z in range(far):
        for pair in range(near // 2):
            block = jnp.concatenate([resid[2 * pair, z], resid[2 * pair + 1, z]], axis=0)
            rows = block.astype(jnp.float32).T
            start = (z * near + 2 * pair) * features
            wide[:, start : start + 2 * features] = rows
            square += jnp.sum(rows * rows, axis=1, keepdims=True)
    scale = lax.rsqrt(square / width + epsilon)
    values = wide[...]
    routed[...] = (values * scale * gain[...]).astype(jnp.bfloat16)
    shared[...] = (values * gain[...]).astype(jnp.bfloat16)

    me = place[0]
    for row in range(slabs):
        own[row : row + 1, :] = wide[pl.ds(row * count + me, 1), :]
    spread[...] = jnp.zeros_like(spread)
    for z in range(far):
        start = pl.multiple_of((z * near + lax.rem(me, near)) * features, features)
        spread[pl.ds(start, features), :] = part[z]
    partial = jnp.dot(shared[...], spread[...], preferred_element_type=jnp.float32)
    chunks = width // LANES
    for row in range(slabs):
        staged[pl.ds(CAP * chunks + row, count, stride=lines), :] = partial[
            row * count : (row + 1) * count
        ]

    copies[0].wait()
    gate_pre = jnp.dot(routed[...], gate[0], preferred_element_type=jnp.float32)
    copies[1].wait()
    up_pre = jnp.dot(routed[...], up[0], preferred_element_type=jnp.float32)
    expert_hidden = (gate_pre / (1.0 + jnp.exp(-gate_pre)) * up_pre).astype(jnp.bfloat16)

    lane = lax.broadcasted_iota(jnp.int32, (count, lanes), 1)
    line = lax.broadcasted_iota(jnp.int32, (count, lanes), 0)
    flags = chosen[...]
    picks = []
    for s in range(CAP):
        pick = jnp.zeros((count, lanes), jnp.float32)
        earlier = jnp.zeros((count, 1), jnp.float32)
        for row in range(slabs):
            flag = flags[:, row : row + 1]
            taken = jnp.where(earlier == float(s), flag, 0.0)
            pick = jnp.where(lane == row * count + line, taken, pick)
            earlier = earlier + flag
        picks.append(pick)
    pick = jnp.concatenate(picks, axis=0).astype(jnp.bfloat16)
    rows = jnp.dot(pick, expert_hidden, preferred_element_type=jnp.float32).astype(jnp.bfloat16)
    copies[2].wait()
    result = jnp.dot(rows, down[0], preferred_element_type=jnp.float32)
    for s in range(CAP):
        for k in range(chunks):
            staged[pl.ds(s * chunks + k, count, stride=lines), :] = result[
                s * count : (s + 1) * count, k * LANES : (k + 1) * LANES
            ]
    used = CAP * chunks + slabs
    for k in range(used, lines):
        staged[pl.ds(k, count, stride=lines), :] = jnp.zeros((count, LANES), jnp.float32)
    out[...] = staged[...].astype(jnp.bfloat16).reshape(count, lines, LANES)


def shards(
    hidden,
    conv_window,
    ssm_state,
    gate_proj,
    input_proj,
    write_proj,
    read_proj,
    step_proj,
    step_bias,
    decay_log,
    decay_shift,
    skip_scale,
    conv_taps,
    conv_bias,
    mix_gain,
    group_gain,
    out_proj,
    ffn_gain,
    router,
    expert_ids,
    expert_gate,
    expert_up,
    expert_down,
    shared_gate,
    shared_up,
    shared_down,
):
    rows = hidden.shape[0]
    width = hidden.shape[1]
    index = lax.axis_index(EP)
    count = lax.axis_size(EP)
    near = lax.axis_size(NEAR)
    experts = router.shape[1]
    units = shared_gate.shape[1]
    features = shared_gate.shape[0]

    far = lax.axis_size("zh")
    chunks = width // LANES
    place = index.astype(jnp.int32).reshape(1)
    (opening,) = fast_call(
        open_kernel,
        "open_rows",
        [((far, rows * chunks + features, LANES), jnp.bfloat16)],
        [((rows * chunks, LANES), jnp.float32)],
        [],
        [hidden, shared_gate, shared_up],
        [],
    )
    opened = lax.all_to_all(opening, "zh", 0, 0, tiled=True)
    gathered = lax.all_gather(opened[:, : rows * chunks], NEAR)
    shared_weights = opened[:, rows * chunks :]
    col_width = out_proj.shape[1]
    message, resid_cols = fast_call(
        project_kernel,
        "project_rows",
        [((count, 8, LANES), jnp.bfloat16), ((col_width, LANES), jnp.float32)],
        [
            ((count * rows * chunks, LANES), jnp.float32),
            ((chunks, count * rows, LANES), jnp.float32),
            ((count * rows, width), jnp.bfloat16),
            ((count * 8, LANES), jnp.float32),
        ],
        [place, expert_ids],
        [mix_gain.reshape(1, width)],
        [gathered],
        [gate_proj, input_proj, write_proj.T, read_proj.T],
    )
    pieces = lax.all_to_all(message, EP, 0, 0, tiled=True)

    later = (hidden, conv_window, conv_taps, decay_shift, step_bias, decay_log)
    later, _ = lax.optimization_barrier((later, message))
    hidden_later, conv_window, conv_taps, decay_shift, step_bias, decay_log = later
    hidden_wide = hidden_later.astype(jnp.float32)
    normed_local = (hidden_wide * row_scale(hidden_wide) * mix_gain).astype(jnp.bfloat16)
    step_raw = matmul(normed_local, step_proj)

    gate_rows = jnp.moveaxis(pieces[:, :rows], 0, 1).reshape(rows, -1)
    input_rows = jnp.moveaxis(pieces[:, rows : 2 * rows], 0, 1).reshape(rows, -1)
    tail_width = rows * write_proj.shape[1]
    write_rows, read_rows = (
        jnp.moveaxis(pieces[:, 2 * rows + k, :tail_width].reshape(count, rows, -1), 0, 1).reshape(
            rows, -1
        )
        for k in range(2)
    )
    chosen = pieces[:, 2 * rows, tail_width : tail_width + rows].astype(jnp.float32)

    inner_width = gate_rows.shape[1]
    state_span = GROUPS * STATE
    head_count = step_bias.shape[0]
    per_group = head_count // GROUPS
    fresh_row = jnp.concatenate([input_rows, write_rows, read_rows], axis=1)
    window = jnp.concatenate([conv_window, fresh_row[:, None, :]], axis=1)
    convolved = jax.nn.silu(
        jnp.sum(window.astype(jnp.float32) * conv_taps.astype(jnp.float32)[None], axis=1)
        + conv_bias
    )
    head_input = convolved[:, :inner_width].reshape(rows, GROUPS, per_group, HEAD_DIM)
    write_vec = convolved[:, inner_width : inner_width + state_span].reshape(rows, GROUPS, STATE)
    read_vec = convolved[:, inner_width + state_span :].reshape(rows, GROUPS, STATE)
    step_size = jax.nn.softplus(step_raw + step_bias)
    decay_rate = jnp.exp(decay_shift - step_size * jnp.exp(decay_log)).reshape(
        rows, GROUPS, per_group
    )
    step_group = step_size.reshape(rows, GROUPS, per_group)
    carried = ssm_state.reshape(rows, GROUPS, per_group, HEAD_DIM, STATE)
    next_state = (
        decay_rate[..., None, None] * carried
        + (step_group[..., None] * head_input)[..., None] * write_vec[:, :, None, None, :]
    )
    mixed_out = jnp.einsum("sgepn,sgn->sgep", next_state, read_vec)
    mixed_out = mixed_out + skip_scale.reshape(GROUPS, per_group)[None, :, :, None] * head_input
    mixed_out = mixed_out.reshape(rows, inner_width).astype(jnp.bfloat16)
    gated_out = mixed_out.astype(jnp.float32) * jax.nn.silu(gate_rows.astype(jnp.float32))
    blocks = gated_out.reshape(rows, GROUPS, -1)
    gated_out = ((blocks * row_scale(blocks)).reshape(rows, inner_width) * group_gain).astype(
        jnp.bfloat16
    )

    gated_all = jnp.moveaxis(lax.all_gather(gated_out, EP), 0, 1).reshape(rows * count, inner_width)
    resid_part = (resid_cols[:, : rows * count] + contract(out_proj, gated_all, 0, 1)).astype(
        jnp.bfloat16
    )
    resid_part = jnp.pad(resid_part, ((0, 0), (0, LANES - count * rows)))
    resid_all = near_gather(resid_part)
    used = CAP * chunks + rows
    outbound, resid_own = fast_call(
        expert_kernel,
        "expert_rows",
        [((count, -(-used // 8) * 8, LANES), jnp.bfloat16), ((rows, width), jnp.float32)],
        [
            ((LANES, width), jnp.float32),
            ((LANES, width), jnp.bfloat16),
            ((LANES, width), jnp.bfloat16),
            ((count * -(-used // 8) * 8, LANES), jnp.float32),
            ((width, LANES), jnp.bfloat16),
        ],
        [place],
        [ffn_gain.reshape(1, width)],
        [resid_all, chosen, shared_weights],
        [expert_gate, expert_up, expert_down],
    )
    returned = lax.all_to_all(outbound, EP, 0, 0, tiled=True)

    expert_ids, outbound = lax.optimization_barrier((expert_ids, outbound))
    member = jnp.any(
        expert_ids[:, :, None] == jnp.arange(experts, dtype=jnp.int32)[None, None, :], axis=1
    )
    norm_scale = row_scale(resid_own)
    routed_own = (resid_own * norm_scale * ffn_gain).astype(jnp.bfloat16)
    scores = jnp.where(member, jax.nn.sigmoid(matmul(routed_own, router)), 0.0)
    weights = routed_scale * scores / jnp.sum(scores, axis=1, keepdims=True)
    own_member = member.astype(jnp.int32)
    own_slot = jnp.cumsum(own_member, axis=0) - own_member
    by_slot = jnp.concatenate([jnp.where(own_slot == s, weights, 0.0) for s in range(CAP)], axis=1)
    back = returned[:, : CAP * chunks].reshape(count, CAP, width)
    back = jnp.moveaxis(back, 1, 0).reshape(CAP * count, width)
    high, low = split_pair(by_slot)
    routed = matmul(high, back) + matmul(low, back)
    pre = returned[:, CAP * chunks : used].reshape(far, near, rows, 2, units // far)
    pre = jnp.sum(pre.astype(jnp.float32), axis=1).transpose(2, 1, 0, 3).reshape(2, rows, units)
    shared_hidden = (jax.nn.silu(norm_scale * pre[0]) * (norm_scale * pre[1])).astype(jnp.bfloat16)
    layer_out = (resid_own + routed + matmul(shared_hidden, shared_down)).astype(jnp.bfloat16)
    return (layer_out, next_state.reshape(ssm_state.shape), window[:, 1:])


def solution(mesh):
    torus = Mesh(mesh.devices.reshape(mesh.shape["grp"], -1, 2, 2), GRP_EP)
    return jax.shard_map(
        shards,
        mesh=torus,
        in_specs=(
            P(GRP_EP, None),
            P(GRP_EP, None, None),
            P(GRP_EP, None, None, None),
            P(None, EP),
            P(None, EP),
            P(None, EP),
            P(None, EP),
            P(),
            P(),
            P(),
            P(GRP_EP, None),
            P(),
            P(),
            P(),
            P(),
            P(),
            P(None, EP),
            P(),
            P(),
            P(GRP_EP, None),
            P(EP, None, None),
            P(EP, None, None),
            P(EP, None, None),
            P(EP, None),
            P(EP, None),
            P(),
        ),
        out_specs=(P(GRP_EP, None), P(GRP_EP, None, None, None), P(GRP_EP, None, None)),
        check_vma=False,
    )
```

time: 207 us -> 174 us (0.84)
  blocking collectives: 103 us -> 51.5 us
  waiting for transfers between devices: 17.7 us -> 53.1 us
  matrix products: 24 us -> 8.17 us
  other arithmetic: 23.7 us -> 13.2 us
  Pallas kernels: 0 us -> 10.3 us
  local copies, waits for them, and re-layouts: 16.2 us -> 6.09 us
  starting transfers between devices: 20.1 us -> 30 us
    all_gather x2, blocking collectives: 71.2 us -> 20.1 us  [the longest x1 10.1 us: shards(): gathered = lax.all_gather(opened[:, :rows * chunks], NEAR)]
    all_to_all x2 -> x3, waiting for transfers between devices: 1.45 us -> 36.6 us  [the longest x1 15.7 us: shards(): opened = lax.all_to_all(opening, 'zh', 0, 0, tiled=True)]
    all_to_all x2 -> x3, starting transfers between devices: 10.6 us -> 25.8 us  [the longest x1 17.3 us: shards(): opened = lax.all_to_all(opening, 'zh', 0, 0, tiled=True)]
    dot_general x11 -> x5, matrix products: 13.7 us -> 3.04 us  [matmul(): return jnp.dot(left, right, preferred_element_type=jnp.float32)]
    pallas_call x0 -> x3, Pallas kernels: none -> 10.3 us  [fast_call(): pl.pallas_call(kernel, name=name, out_shape=tuple((pltpu.VMEM(shape, dtyp...]
    all_to_all x1, starting transfers between devices: 9.49 us -> 4.21 us  [shards(): returned = lax.all_to_all(outbound, EP, 0, 0, tiled=True)]
    dot_general x4 -> x1, matrix products: 5.53 us -> 0.42 us  [contract(): lax.dot_general(left, right, (((left_dim,), (right_dim,)), ((), ())), pre...]
    convert_element_type x5 -> x1, other arithmetic: 3.25 us -> 0.09 us  [shards(): pieces[:, 2 * rows, tail_width:tail_width + rows].astype(jnp.float32)]
  transfers between devices with their start and end apart: 3 -> 4, of which waited for: 2 -> 4; matrix products, arithmetic and copies ran while one was open for 23% -> 8% of each run, Pallas kernels for 0% -> 0%
where the time goes in v3:
time: 174 us; the launch traced here: 173 us
  waiting for transfers between devices  53.1 us (31%)
  blocking collectives  51.5 us (30%)
  starting transfers between devices  30 us (17%)
  other arithmetic  13.2 us (8%)
  Pallas kernels  10.3 us (6%)
  matrix products  8.17 us (5%)
  local copies, waits for them, and re-layouts  6.09 us (4%)
    all_gather x1, blocking collectives, shards(): lax.all_gather(gated_out, EP)  31.4 us
    all_to_all x1, starting transfers between devices, shards(): opened = lax.all_to_all(opening, 'zh', 0, 0, tiled=True)  17.3 us
    all_to_all x1, waiting for transfers between devices, shards(): returned = lax.all_to_all(outbound, EP, 0, 0, tiled=True)  16.5 us
    all_to_all x1, waiting for transfers between devices, shards(): opened = lax.all_to_all(opening, 'zh', 0, 0, tiled=True)  15.7 us
    all_to_all x1, waiting for transfers between devices, near_gather(): lax.all_to_all(jnp.broadcast_to(shard[None], (count, *shard.shape)), 'zh'...  11.7 us
    pallas_call x3, Pallas kernels, fast_call(): pl.pallas_call(kernel, name=name, out_shape=tuple((pltpu.VMEM(shape, dtyp...  10.3 us
    all_gather x1, blocking collectives, shards(): gathered = lax.all_gather(opened[:, :rows * chunks], NEAR)  10.1 us
    all_gather x1, blocking collectives, near_gather(): return lax.all_gather(across, NEAR)  9.99 us
  transfers between devices with their start and end apart: 4, of which 4 were waited for; matrix products, arithmetic and copies ran while one was open for 8% of the time, Pallas kernels for 0%

profile of v3, /device:TPU:69, one launch (start us, length us, event | category | flops | bytes accessed | tf_op | source)
XLA Modules:
  0.0 173.4 jit_solution(7900066726919241547)
XLA Ops:
  0.6 1.8 %open_rows.1 = bf16[8,112,128]{2,1,0:T(8,128)(2,1)} custom-call(bf16[3,2048]{1,0:T(4,128)(2,1)} %hidden.1, bf16[64,512]{1,0:T(8,128)(2,1)} %gate.1, bf16[64,512]{1,0:T(8,128)(2,1)} %up.1), custom_call_target="tpu_custom_call" | custom-call | tf_op jit(solution)/shard_map/open_rows/pallas_call | solution.py:61
  2.5 17.3 %all-to-all-start = ((bf16[8,112,128]{2,1,0:T(8,128)(2,1)}), bf16[8,112,128]{2,1,0:T(8,128)(2,1)S(1)}, u32[]{:S(2)}, u32[]{:S(2)}) async-start(bf16[8,112,128]{2,1,0:T(8,128)(2,1)} %open_rows.1), calls=%async_computation | async-start | bytes 458752 | tf_op jit(solution)/shard_map/all_to_all | solution.py:318
  19.7 0.7 mul.251
  20.5 15.7 %all-to-all-done = bf16[8,112,128]{2,1,0:T(8,128)(2,1)S(1)} async-done(((bf16[8,112,128]{2,1,0:T(8,128)(2,1)}), bf16[8,112,128]{2,1,0:T(8,128)(2,1)S(1)}, u32[]{:S(2)}, u32[]{:S(2)}) %all-to-all-start) | async-done | bytes 229408 | tf_op jit(solution)/shard_map/all_to_all | solution.py:318
  36.2 10.1 %all-gather = bf16[32,48,128]{2,1,0:T(8,128)(2,1)S(1)} all-gather(bf16[8,48,128]{2,1,0:T(8,128)(2,1)S(1)} %slice.66), channel_id=2, replica_groups=mesh['grp'=4,'zh'=8,'zl'=2,'core'=2] {'zl','core'}, dimensions={0}, use_global_device_ids=true | all-gather | bytes 491520 | tf_op jit(solution)/shard_map/all_gather | solution.py:319
  46.3 0.7 copy-done.1
  47.0 3.4 %project_rows.1 = (bf16[32,8,128]{2,1,0:T(8,128)(2,1)}, f32[64,128]{1,0:T(8,128)S(1)}) custom-call(s32[1]{0:T(128)} %bitcast.place, s32[3,6]{1,0:T(4,128)S(1)} %copy-done.1, f32[1,2048]{1,0:T(1,128)} %bitcast.106, bf16[4,8,48,128]{3,2,1,0:T(8,128)(2,1)S(1)} %bitcast.91, bf16[2048,128]{1,0:T(8,128)(2,1)} %gate_hbm.2, bf16[2048,128]{1,0:T(8,128)(2,1)} %input_hbm.1, ...), custom_call_target="tpu_custom_call" | custom-call | tf_op jit(solution)/shard_map/project_rows/pallas_call | solution.py:61
  50.4 4.2 %all-to-all-start.1 = ((bf16[32,8,128]{2,1,0:T(8,128)(2,1)}), bf16[32,8,128]{2,1,0:T(8,128)(2,1)S(1)}, u32[]{:S(2)}, u32[]{:S(2)}) async-start(bf16[32,8,128]{2,1,0:T(8,128)(2,1)} %get-tuple-element.15), calls=%async_computation.1 | async-start | bytes 131072 | tf_op jit(solution)/shard_map/all_to_all | solution.py:337
  54.6 0.8 fusion.23
  55.5 0.8 convert_element_type.119
  56.3 0.7 exp.38
  56.9 1.2 subtract_exponential_fusion
  58.4 9.2 %all-to-all-done.1 = bf16[32,8,128]{2,1,0:T(8,128)(2,1)S(1)} async-done(((bf16[32,8,128]{2,1,0:T(8,128)(2,1)}), bf16[32,8,128]{2,1,0:T(8,128)(2,1)S(1)}, u32[]{:S(2)}, u32[]{:S(2)}) %all-to-all-start.1) | async-done | bytes 65568 | tf_op jit(solution)/shard_map/all_to_all | solution.py:337
  68.3 1.3 multiply_reduce_fusion
  69.5 0.8 divide_multiply_fusion
  70.8 4.7 %fusion = f32[3,8,1,8,64]{4,2,3,1,0:T(1,128)S(1)} fusion(f32[3,8,128,1,1]{2,3,4,1,0:T(1,128)S(1)} %bitcast.105, f32[3,8,8,64,128]{4,3,2,1,0:T(8,128)} %bitcast.93, f32[3,8,128]{2,1,0:T(8,128)S(1)} %bitcast.103, f32[3,8,8,64]{3,2,1,0:T(8,128)S(1)} %broadcast_multiply_fusion.1, f32[3,8,8]{2,1,0:T(8,128)S(1)} %mul.238), kind=kOutput, calls=%fused_computation.1 | convolution fusion | flops 7864320 | bytes 6415104 | tf_op jit(solution)/shard_map/sgepn,sgn->sgep/dot_general | solution.py:380
  75.5 0.8 multiply_reduce_fusion.1
  76.4 1.0 reshape.214
  77.5 31.4 %all_gather.18 = bf16[32,3,4096]{2,1,0:T(4,128)(2,1)S(1)} all-gather(bf16[1,3,4096]{2,1,0:T(4,128)(2,1)S(1)} %multiply_convert_fusion), channel_id=1, replica_groups=mesh['grp'=4,'zh'=8,'zl'=2,'core'=2] {'zh','zl','core'}, dimensions={0}, use_global_device_ids=true | all-gather | bytes 811008 | tf_op jit(solution)/shard_map/all_gather | solution.py:389
  108.9 0.6 copy.71
  109.5 0.4 fusion.10
  110.0 0.7 broadcast_in_dim.10
  110.6 4.3 %all-to-all-start.2 = ((bf16[8,64,128]{2,1,0:T(8,128)(2,1)}), bf16[8,64,128]{2,1,0:T(8,128)(2,1)S(1)}, u32[]{:S(2)}, u32[]{:S(2)}) async-start(bf16[8,64,128]{2,1,0:T(8,128)(2,1)} %broadcast_in_dim.10), calls=%async_computation.2 | async-start | bytes 262144 | tf_op jit(solution)/shard_map/all_to_all | solution.py:44
  115.2 0.9 fusion.15
  116.0 11.7 %all-to-all-done.2 = bf16[8,64,128]{2,1,0:T(8,128)(2,1)S(1)} async-done(((bf16[8,64,128]{2,1,0:T(8,128)(2,1)}), bf16[8,64,128]{2,1,0:T(8,128)(2,1)S(1)}, u32[]{:S(2)}, u32[]{:S(2)}) %all-to-all-start.2) | async-done | bytes 131104 | tf_op jit(solution)/shard_map/all_to_all | solution.py:44
  127.8 10.0 %all-gather.1 = bf16[32,64,128]{2,1,0:T(8,128)(2,1)S(1)} all-gather(bf16[8,64,128]{2,1,0:T(8,128)(2,1)S(1)} %all-to-all-done.2), channel_id=3, replica_groups=mesh['grp'=4,'zh'=8,'zl'=2,'core'=2] {'zl','core'}, dimensions={0}, use_global_device_ids=true | all-gather | bytes 655360 | tf_op jit(solution)/shard_map/all_gather | solution.py:47
  137.7 5.1 %expert_rows.1 = (bf16[32,40,128]{2,1,0:T(8,128)(2,1)}, f32[3,2048]{1,0:T(4,128)S(1)}) custom-call(s32[1]{0:T(128)} %bitcast.place, f32[1,2048]{1,0:T(1,128)} %bitcast.107, bf16[4,8,64,128]{3,2,1,0:T(8,128)(2,1)S(1)} %bitcast.90, f32[32,3]{1,0:T(8,128)S(1)} %bitcast.92, bf16[8,64,128]{2,1,0:T(8,128)(2,1)S(1)} %slice.75.part, bf16[1,2048,512]{2,1,0:T(8,128)(2,1)} %gate_hbm.3, ...), custom_call_target="tpu_custom_call" | custom-call | tf_op jit(solution)/shard_map/expert_rows/pallas_call | solution.py:61
  142.8 4.2 %all-to-all-start.3 = ((bf16[32,40,128]{2,1,0:T(8,128)(2,1)}), bf16[32,40,128]{2,1,0:T(8,128)(2,1)S(1)}, u32[]{:S(2)}, u32[]{:S(2)}) async-start(bf16[32,40,128]{2,1,0:T(8,128)(2,1)} %get-tuple-element.23), calls=%async_computation.3 | async-start | bytes 655360 | tf_op jit(solution)/shard_map/all_to_all | solution.py:412
  147.1 7.0 %multiply_add_fusion = f32[3,64,64,128]{3,2,1,0:T(8,128)} fusion(f32[3,64,64,128]{3,2,1,0:T(8,128)} %param.28, f32[3,64,128]{2,1,0:T(8,128)S(1)} %broadcast_bitcast_fusion, f32[3,64,64]{2,1,0:T(8,128)S(1)} %broadcast_multiply_fusion, f32[3,64]{1,0:T(4,128)S(1)} %get-tuple-element.37), kind=kLoop, calls=%fused_computation | loop fusion | flops 4718592 | bytes 12731136 | tf_op jit(solution)/shard_map/add | solution.py:377
  154.4 0.3 fusion.46
  154.8 16.5 %all-to-all-done.3 = bf16[32,40,128]{2,1,0:T(8,128)(2,1)S(1)} async-done(((bf16[32,40,128]{2,1,0:T(8,128)(2,1)}), bf16[32,40,128]{2,1,0:T(8,128)(2,1)S(1)}, u32[]{:S(2)}, u32[]{:S(2)}) %all-to-all-start.3) | async-done | bytes 327712 | tf_op jit(solution)/shard_map/all_to_all | solution.py:412
  172.3 1.0 fusion.8
  (65 shorter events, 3.0 us)
Async XLA Ops:
  0.6 171.7 %copy-start = (bf16[512,2048]{1,0:T(8,128)(2,1)S(1)}, bf16[512,2048]{1,0:T(8,128)(2,1)}, u32[]{:S(2)}) copy-start(bf16[512,2048]{1,0:T(8,128)(2,1)} %param.51) | copy-start | bytes 6291460
  2.5 33.7 %all-to-all-start = ((bf16[8,112,128]{2,1,0:T(8,128)(2,1)}), bf16[8,112,128]{2,1,0:T(8,128)(2,1)S(1)}, u32[]{:S(2)}, u32[]{:S(2)}) async-start(bf16[8,112,128]{2,1,0:T(8,128)(2,1)} %open_rows.1), calls=%async_computation | async-start | bytes 458752 | tf_op jit(solution)/shard_map/all_to_all | solution.py:318
  36.2 41.2 %copy-start.5 = (f32[4096]{0:T(1024)S(1)}, f32[4096]{0:T(1024)}, u32[]{:S(2)}) copy-start(f32[4096]{0:T(1024)} %param.41) | copy-start | bytes 49156
  46.3 0.7 copy-start.1
  50.4 17.2 %all-to-all-start.1 = ((bf16[32,8,128]{2,1,0:T(8,128)(2,1)}), bf16[32,8,128]{2,1,0:T(8,128)(2,1)S(1)}, u32[]{:S(2)}, u32[]{:S(2)}) async-start(bf16[32,8,128]{2,1,0:T(8,128)(2,1)} %get-tuple-element.15), calls=%async_computation.1 | async-start | bytes 131072 | tf_op jit(solution)/shard_map/all_to_all | solution.py:337
  68.1 41.4 %copy-start.4 = (bf16[4096,64]{0,1:T(8,128)(2,1)S(1)}, bf16[4096,64]{0,1:T(8,128)(2,1)}, u32[]{:S(2)}) copy-start(bf16[4096,64]{0,1:T(8,128)(2,1)} %param.42) | copy-start | bytes 1572868
  70.7 44.5 %copy-start.3 = (bf16[3,3,6144]{2,1,0:T(4,128)(2,1)S(1)}, bf16[3,3,6144]{2,1,0:T(4,128)(2,1)}, u32[]{:S(2)}) copy-start(bf16[3,3,6144]{2,1,0:T(4,128)(2,1)} %param.27) | copy-start | bytes 331780
  110.6 17.1 %all-to-all-start.2 = ((bf16[8,64,128]{2,1,0:T(8,128)(2,1)}), bf16[8,64,128]{2,1,0:T(8,128)(2,1)S(1)}, u32[]{:S(2)}, u32[]{:S(2)}) async-start(bf16[8,64,128]{2,1,0:T(8,128)(2,1)} %broadcast_in_dim.10), calls=%async_computation.2 | async-start | bytes 262144 | tf_op jit(solution)/shard_map/all_to_all | solution.py:44
  142.8 28.4 %all-to-all-start.3 = ((bf16[32,40,128]{2,1,0:T(8,128)(2,1)}), bf16[32,40,128]{2,1,0:T(8,128)(2,1)S(1)}, u32[]{:S(2)}, u32[]{:S(2)}) async-start(bf16[32,40,128]{2,1,0:T(8,128)(2,1)} %get-tuple-element.23), calls=%async_computation.3 | async-start | bytes 655360 | tf_op jit(solution)/shard_map/all_to_all | solution.py:412
  147.1 7.0 %copy-start.2 = (s32[3,6]{1,0:T(4,128)S(1)}, s32[3,6]{1,0:T(4,128)}, u32[]{:S(2)}) copy-start(s32[3,6]{1,0:T(4,128)} %ids.1) | copy-start | bytes 220
  147.1 7.3 %copy-start.6 = (f32[2048]{0:T(1024)S(1)}, f32[2048]{0:T(1024)}, u32[]{:S(2)}) copy-start(f32[2048]{0:T(1024)} %param.43) | copy-start | bytes 24580
  147.1 7.3 %copy-start.7 = (bf16[2048,32]{0,1:T(8,128)(2,1)S(1)}, bf16[2048,32]{0,1:T(8,128)(2,1)}, u32[]{:S(2)}) copy-start(bf16[2048,32]{0,1:T(8,128)(2,1)} %param.44) | copy-start | bytes 393220

commit v4 on v3

--- a/solution.py
+++ b/solution.py
@@ -39,25 +39,23 @@
     return high, low
 
 
-def near_gather(shard):
-    count = lax.axis_size("zh")
-    across = lax.all_to_all(
-        jnp.broadcast_to(shard[None], (count, *shard.shape)), "zh", 0, 0, tiled=True
-    )
-    return lax.all_gather(across, NEAR)
+def near_gather(copies):
+    return lax.all_gather(lax.all_to_all(copies, "zh", 0, 0, tiled=True), NEAR)
 
 
 def kept_in(space, arrays):
     return [pltpu.with_memory_space_constraint(array, space) for array in arrays]
 
 
-def fast_call(kernel, name, outs, scratch, scalars, fetched, arrays, far=()):
+def fast_call(kernel, name, outs, scratch, scalars, fetched, arrays, far=[], remote=[]):
     vmem = pl.BlockSpec(memory_space=pltpu.VMEM)
     smem = pl.BlockSpec(memory_space=pltpu.SMEM)
     hbm = pl.BlockSpec(memory_space=pltpu.HBM)
-    specs = [smem] * len(scalars) + [vmem] * (len(fetched) + len(arrays)) + [hbm] * len(far)
+    specs = [smem] * len(scalars) + [vmem] * (len(fetched) + len(arrays))
+    specs += [hbm] * (len(far) + len(remote))
     landing = [pltpu.VMEM(array.shape, array.dtype) for array in far]
     waits = [pltpu.SemaphoreType.DMA((len(far),))] if far else []
+    waits += [pltpu.SemaphoreType.DMA((8,))] * len(remote)
     return pl.pallas_call(
         kernel,
         name=name,
@@ -66,26 +64,22 @@
         out_specs=(vmem,) * len(outs),
         scratch_shapes=[pltpu.VMEM(shape, dtype) for shape, dtype in scratch] + landing + waits,
         compiler_params=pltpu.CompilerParams(vmem_limit_bytes=24 * 1024 * 1024),
-    )(*scalars, *kept_in(pltpu.HBM, fetched), *kept_in(pltpu.VMEM, arrays), *kept_in(pltpu.HBM, far))
-
-
-def open_kernel(hidden, gate, up, out, staged):
+    )(
+        *kept_in(pltpu.HBM, scalars + fetched),
+        *kept_in(pltpu.VMEM, arrays),
+        *kept_in(pltpu.HBM, far + remote),
+    )
+
+
+def open_kernel(hidden, out, staged):
     rows, width = hidden.shape
     chunks = width // LANES
     values = hidden[...].astype(jnp.float32)
     for k in range(chunks):
         staged[pl.ds(k, rows, stride=chunks), :] = values[:, k * LANES : (k + 1) * LANES]
     mine = staged[...].astype(jnp.bfloat16)
-    gates = gate[...].astype(jnp.float32)
-    ups = up[...].astype(jnp.float32)
-    count = out.shape[0]
-    half = gate.shape[1] // count
-    for z in range(count):
-        span = slice(z * half, (z + 1) * half)
-        out[z, : rows * chunks, :] = mine
-        out[z, rows * chunks :, :] = jnp.concatenate(
-            [gates[:, span], ups[:, span]], axis=1
-        ).astype(jnp.bfloat16)
+    for z in range(out.shape[0]):
+        out[z] = mine
 
 
 def project_kernel(
@@ -117,12 +111,15 @@
     ]
     for copy in copies:
         copy.start()
-    near, far, chunk, lanes = gathered.shape
-    count = near * far
+    near, _, lanes = gathered.shape
+    count, lines, _ = message.shape
+    far = count // near
     rows = ids.shape[0]
-    blocks = chunk // rows
-    lines = message.shape[1]
-    flat[...] = gathered[...].reshape(count * chunk, lanes).astype(jnp.float32)
+    blocks = gain.shape[1] // lanes
+    chunk = rows * blocks
+    flat[...] = (
+        gathered[:, : far * chunk, :].reshape(count * chunk, lanes).astype(jnp.float32)
+    )
     square = jnp.zeros((rows * count, 1), jnp.float32)
     for k in range(blocks):
         for row in range(rows):
@@ -173,15 +170,37 @@
     columns[...] = jnp.where(me % 2 == 0, across[:height], across[height:])
 
 
+def output_kernel(gathered, columns, weights_hbm, out, flat, wide, rows, weights, sems):
+    copy = pltpu.make_async_copy(weights_hbm, weights, sems.at[0])
+    copy.start()
+    near, far, chunk, lanes = gathered.shape
+    count = near * far
+    blocks = weights.shape[1] // lanes
+    slabs = chunk // blocks
+    flat[...] = gathered[...].reshape(count * chunk, lanes).astype(jnp.float32)
+    rows[slabs * count :, :] = jnp.zeros((lanes - slabs * count, blocks * lanes), jnp.bfloat16)
+    for k in range(blocks):
+        for row in range(slabs):
+            for n in range(near):
+                wide[k, pl.ds(row * count + n, far, stride=near), :] = flat[
+                    pl.ds(n * far * chunk + row * blocks + k, far, stride=chunk), :
+                ]
+        rows[: slabs * count, k * lanes : (k + 1) * lanes] = wide[k].astype(jnp.bfloat16)
+    copy.wait()
+    mine = (columns[...] + contract(weights[...], rows[...], 1, 1)).astype(jnp.bfloat16)
+    for z in range(out.shape[0]):
+        out[z] = mine
+
+
 def expert_kernel(
     place,
     gain,
     resid,
     chosen,
-    part,
     gate_hbm,
     up_hbm,
     down_hbm,
+    part_hbm,
     out,
     own,
     wide,
@@ -193,6 +212,7 @@
     up,
     down,
     sems,
+    part_sems,
 ):
     near, far, features, lanes = resid.shape
     width = near * far * features
@@ -203,6 +223,18 @@
         pltpu.make_async_copy(up_hbm, up, sems.at[1]),
         pltpu.make_async_copy(down_hbm, down, sems.at[2]),
     ]
+    me = place[0]
+    first = part_hbm.shape[1] - CAP * near * features
+    for n in range(near):
+        for s in range(CAP):
+            start = pl.multiple_of(first + (s * near + lax.rem(me, near)) * features, features)
+            copies.append(
+                pltpu.make_async_copy(
+                    part_hbm.at[n, pl.ds(start, features)],
+                    spread.at[pl.ds(n * features, features), pl.ds(s * LANES, LANES)],
+                    part_sems.at[n * CAP + s],
+                )
+            )
     for copy in copies:
         copy.start()
     square = jnp.zeros((lanes, 1), jnp.float32)
@@ -218,19 +250,21 @@
     routed[...] = (values * scale * gain[...]).astype(jnp.bfloat16)
     shared[...] = (values * gain[...]).astype(jnp.bfloat16)
 
-    me = place[0]
     for row in range(slabs):
         own[row : row + 1, :] = wide[pl.ds(row * count + me, 1), :]
-    spread[...] = jnp.zeros_like(spread)
-    for z in range(far):
-        start = pl.multiple_of((z * near + lax.rem(me, near)) * features, features)
-        spread[pl.ds(start, features), :] = part[z]
-    partial = jnp.dot(shared[...], spread[...], preferred_element_type=jnp.float32)
+    block = near * features
+    for copy in copies[3:]:
+        copy.wait()
+    start = pl.multiple_of((me // near) * block, block)
+    partial = jnp.dot(
+        shared[:, pl.ds(start, block)], spread[...], preferred_element_type=jnp.float32
+    )
     chunks = width // LANES
-    for row in range(slabs):
-        staged[pl.ds(CAP * chunks + row, count, stride=lines), :] = partial[
-            row * count : (row + 1) * count
-        ]
+    for s in range(CAP):
+        for row in range(slabs):
+            staged[pl.ds(CAP * chunks + s * slabs + row, count, stride=lines), :] = partial[
+                row * count : (row + 1) * count, s * LANES : (s + 1) * LANES
+            ]
 
     copies[0].wait()
     gate_pre = jnp.dot(routed[...], gate[0], preferred_element_type=jnp.float32)
@@ -260,7 +294,7 @@
             staged[pl.ds(s * chunks + k, count, stride=lines), :] = result[
                 s * count : (s + 1) * count, k * LANES : (k + 1) * LANES
             ]
-    used = CAP * chunks + slabs
+    used = CAP * (chunks + slabs)
     for k in range(used, lines):
         staged[pl.ds(k, count, stride=lines), :] = jnp.zeros((count, LANES), jnp.float32)
     out[...] = staged[...].astype(jnp.bfloat16).reshape(count, lines, LANES)
@@ -309,15 +343,19 @@
     (opening,) = fast_call(
         open_kernel,
         "open_rows",
-        [((far, rows * chunks + features, LANES), jnp.bfloat16)],
+        [((far, rows * chunks, LANES), jnp.bfloat16)],
         [((rows * chunks, LANES), jnp.float32)],
         [],
-        [hidden, shared_gate, shared_up],
+        [hidden],
         [],
     )
-    opened = lax.all_to_all(opening, "zh", 0, 0, tiled=True)
-    gathered = lax.all_gather(opened[:, : rows * chunks], NEAR)
-    shared_weights = opened[:, rows * chunks :]
+    opened = lax.all_to_all(opening, "zh", 0, 0, tiled=True).reshape(-1, LANES)
+    later, _ = lax.optimization_barrier(((shared_gate, shared_up), opening))
+    blocks = [
+        jnp.moveaxis(weights.reshape(features, near, LANES), 1, 0).reshape(-1, LANES)
+        for weights in later
+    ]
+    gathered = lax.all_gather(jnp.concatenate([opened, *blocks], axis=0), NEAR)
     col_width = out_proj.shape[1]
     message, resid_cols = fast_call(
         project_kernel,
@@ -386,13 +424,27 @@
         jnp.bfloat16
     )
 
-    gated_all = jnp.moveaxis(lax.all_gather(gated_out, EP), 0, 1).reshape(rows * count, inner_width)
-    resid_part = (resid_cols[:, : rows * count] + contract(out_proj, gated_all, 0, 1)).astype(
-        jnp.bfloat16
-    )
-    resid_part = jnp.pad(resid_part, ((0, 0), (0, LANES - count * rows)))
+    gated_all = near_gather(
+        jnp.broadcast_to(
+            gated_out.reshape(1, -1, LANES), (far, rows * inner_width // LANES, LANES)
+        )
+    )
+    (resid_part,) = fast_call(
+        output_kernel,
+        "output_rows",
+        [((far, col_width, LANES), jnp.bfloat16)],
+        [
+            ((count * rows * inner_width // LANES, LANES), jnp.float32),
+            ((inner_width // LANES, rows * count, LANES), jnp.float32),
+            ((LANES, inner_width), jnp.bfloat16),
+        ],
+        [],
+        [],
+        [gated_all, resid_cols],
+        [out_proj.T],
+    )
     resid_all = near_gather(resid_part)
-    used = CAP * chunks + rows
+    used = CAP * (chunks + rows)
     outbound, resid_own = fast_call(
         expert_kernel,
         "expert_rows",
@@ -402,12 +454,13 @@
             ((LANES, width), jnp.bfloat16),
             ((LANES, width), jnp.bfloat16),
             ((count * -(-used // 8) * 8, LANES), jnp.float32),
-            ((width, LANES), jnp.bfloat16),
+            ((near * features, CAP * LANES), jnp.bfloat16),
         ],
         [place],
         [ffn_gain.reshape(1, width)],
-        [resid_all, chosen, shared_weights],
+        [resid_all, chosen],
         [expert_gate, expert_up, expert_down],
+        [gathered],
     )
     returned = lax.all_to_all(outbound, EP, 0, 0, tiled=True)
 
@@ -426,8 +479,8 @@
     back = jnp.moveaxis(back, 1, 0).reshape(CAP * count, width)
     high, low = split_pair(by_slot)
     routed = matmul(high, back) + matmul(low, back)
-    pre = returned[:, CAP * chunks : used].reshape(far, near, rows, 2, units // far)
-    pre = jnp.sum(pre.astype(jnp.float32), axis=1).transpose(2, 1, 0, 3).reshape(2, rows, units)
+    pre = returned[:, CAP * chunks : used].reshape(far, near, 2, rows, units // near)
+    pre = jnp.sum(pre.astype(jnp.float32), axis=0).transpose(1, 2, 0, 3).reshape(2, rows, units)
     shared_hidden = (jax.nn.silu(norm_scale * pre[0]) * (norm_scale * pre[1])).astype(jnp.bfloat16)
     layer_out = (resid_own + routed + matmul(shared_hidden, shared_down)).astype(jnp.bfloat16)
     return (layer_out, next_state.reshape(ssm_state.shape), window[:, 1:])

time: 174 us -> 175 us (level)
  blocking collectives: 51.5 us -> 31.6 us
  waiting for transfers between devices: 53.1 us -> 62.9 us
  local copies, waits for them, and re-layouts: 6.09 us -> 9.94 us
  Pallas kernels: 10.3 us -> 13.6 us
  starting transfers between devices: 30 us -> 32.8 us
    all_gather x3, blocking collectives: 51.5 us -> 31.6 us  [the longest x2 19.9 us: near_gather(): return lax.all_gather(lax.all_to_all(copies, 'zh', 0, 0, tiled=True), NEAR)]
    all_to_all x2 -> x3, waiting for transfers between devices: 27.4 us -> 38.3 us  [the longest x2 28.3 us: near_gather(): return lax.all_gather(lax.all_to_all(copies, 'zh', 0, 0, tiled=True), NEAR)]
    pallas_call x3 -> x4, Pallas kernels: 10.3 us -> 13.6 us  [fast_call(): pl.pallas_call(kernel, name=name, out_shape=tuple((pltpu.VMEM(shape, dtyp...]
    all_to_all x2 -> x3, starting transfers between devices: 21.6 us -> 24.4 us  [the longest x1 17.3 us: shards(): opened = lax.all_to_all(opening, 'zh', 0, 0, tiled=True).reshape(-1, LANES)]
  transfers between devices with their start and end apart: 4 -> 5, of which waited for: 4 -> 5; matrix products, arithmetic and copies ran while one was open for 8% -> 10% of each run, Pallas kernels for 0% -> 0%
where the time goes in v4:
time: 175 us; the launch traced here: 173 us
  waiting for transfers between devices  62.9 us (36%)
  starting transfers between devices  32.8 us (19%)
  blocking collectives  31.6 us (18%)
  other arithmetic  13.8 us (8%)
  Pallas kernels  13.6 us (8%)
  local copies, waits for them, and re-layouts  9.94 us (6%)
  matrix products  7.79 us (4%)
    all_to_all x2, waiting for transfers between devices, near_gather(): return lax.all_gather(lax.all_to_all(copies, 'zh', 0, 0, tiled=True), NEAR)  28.3 us
    all_gather x2, blocking collectives, near_gather(): return lax.all_gather(lax.all_to_all(copies, 'zh', 0, 0, tiled=True), NEAR)  19.9 us
    all_to_all x1, starting transfers between devices, shards(): opened = lax.all_to_all(opening, 'zh', 0, 0, tiled=True).reshape(-1, LANES)  17.3 us
    all_to_all x1, waiting for transfers between devices, shards(): returned = lax.all_to_all(outbound, EP, 0, 0, tiled=True)  16.5 us
    pallas_call x4, Pallas kernels, fast_call(): pl.pallas_call(kernel, name=name, out_shape=tuple((pltpu.VMEM(shape, dtyp...  13.6 us
    all_gather x1, blocking collectives, shards(): gathered = lax.all_gather(jnp.concatenate([opened, *blocks], axis=0), NEAR)  11.6 us
    all_to_all x1, waiting for transfers between devices, shards(): opened = lax.all_to_all(opening, 'zh', 0, 0, tiled=True).reshape(-1, LANES)  10 us
    all_to_all x1, waiting for transfers between devices, shards(): pieces = lax.all_to_all(message, EP, 0, 0, tiled=True)  8.07 us
  transfers between devices with their start and end apart: 5, of which 5 were waited for; matrix products, arithmetic and copies ran while one was open for 10% of the time, Pallas kernels for 0%

profile of v4, /device:TPU:69, one launch (start us, length us, event | category | flops | bytes accessed | tf_op | source)
XLA Modules:
  0.0 173.4 jit_solution(11714685751481980730)
XLA Ops:
  0.7 1.5 open_rows.1
  2.2 17.3 %all-to-all-start = ((bf16[8,48,128]{2,1,0:T(8,128)(2,1)}), bf16[8,48,128]{2,1,0:T(8,128)(2,1)S(1)}, u32[]{:S(2)}, u32[]{:S(2)}) async-start(bf16[8,48,128]{2,1,0:T(8,128)(2,1)} %open_rows.1), calls=%async_computation | async-start | bytes 196608 | tf_op jit(solution)/shard_map/all_to_all | solution.py:352
  19.4 0.9 reshape.173
  20.3 0.9 reshape.171
  21.2 0.7 mul.243
  21.9 10.0 %all-to-all-done = bf16[8,48,128]{2,1,0:T(8,128)(2,1)S(1)} async-done(((bf16[8,48,128]{2,1,0:T(8,128)(2,1)}), bf16[8,48,128]{2,1,0:T(8,128)(2,1)S(1)}, u32[]{:S(2)}, u32[]{:S(2)}) %all-to-all-start) | async-done | bytes 98336 | tf_op jit(solution)/shard_map/all_to_all | solution.py:352
  32.0 11.6 %all-gather = bf16[3584,128]{1,0:T(8,128)(2,1)S(1)} all-gather(bf16[896,128]{1,0:T(8,128)(2,1)S(1)} %pad_maximum_fusion), channel_id=2, replica_groups=mesh['grp'=4,'zh'=8,'zl'=2,'core'=2] {'zl','core'}, dimensions={0}, use_global_device_ids=true | all-gather | bytes 1146880 | tf_op jit(solution)/shard_map/all_gather | solution.py:358
  43.6 3.4 %project_rows.1 = (bf16[32,8,128]{2,1,0:T(8,128)(2,1)}, f32[64,128]{1,0:T(8,128)S(1)}) custom-call(s32[1]{0:T(128)} %bitcast.place, s32[3,6]{1,0:T(4,128)} %ids.1, f32[1,2048]{1,0:T(1,128)} %bitcast.127, bf16[4,896,128]{2,1,0:T(8,128)(2,1)S(1)} %bitcast.102, bf16[2048,128]{1,0:T(8,128)(2,1)} %gate_hbm.2, bf16[2048,128]{1,0:T(8,128)(2,1)} %input_hbm.1, ...), custom_call_target="tpu_custom_call" | custom-call | tf_op jit(solution)/shard_map/project_rows/pallas_call | solution.py:59
  47.0 4.2 %all-to-all-start.1 = ((bf16[32,8,128]{2,1,0:T(8,128)(2,1)}), bf16[32,8,128]{2,1,0:T(8,128)(2,1)S(1)}, u32[]{:S(2)}, u32[]{:S(2)}) async-start(bf16[32,8,128]{2,1,0:T(8,128)(2,1)} %get-tuple-element.18), calls=%async_computation.1 | async-start | bytes 131072 | tf_op jit(solution)/shard_map/all_to_all | solution.py:375
  51.2 0.8 fusion.21
  52.1 0.8 convert_element_type.102
  53.5 1.2 subtract_exponential_fusion
  56.2 8.1 %all-to-all-done.1 = bf16[32,8,128]{2,1,0:T(8,128)(2,1)S(1)} async-done(((bf16[32,8,128]{2,1,0:T(8,128)(2,1)}), bf16[32,8,128]{2,1,0:T(8,128)(2,1)S(1)}, u32[]{:S(2)}, u32[]{:S(2)}) %all-to-all-start.1) | async-done | bytes 65568 | tf_op jit(solution)/shard_map/all_to_all | solution.py:375
  64.9 1.3 multiply_reduce_fusion
  68.3 0.8 broadcast_multiply_fusion.1
  69.2 4.7 %fusion = f32[3,8,1,8,64]{4,2,3,1,0:T(1,128)S(1)} fusion(f32[3,8,128,1,1]{2,3,4,1,0:T(1,128)} %bitcast.125, f32[3,8,8,64,128]{4,3,2,1,0:T(8,128)} %bitcast.107, f32[3,8,128]{2,1,0:T(8,128)} %bitcast.122, f32[3,8,8,64]{3,2,1,0:T(8,128)S(1)} %broadcast_multiply_fusion.1, f32[3,8,8]{2,1,0:T(8,128)} %mul.230), kind=kOutput, calls=%fused_computation.1 | convolution fusion | flops 7864320 | bytes 6415104 | tf_op jit(solution)/shard_map/sgepn,sgn->sgep/dot_general | solution.py:418
  73.9 0.8 multiply_reduce_fusion.1
  74.8 1.0 reshape.184
  75.7 0.7 fusion.15
  77.2 3.6 %all-to-all-start.2 = ((bf16[8,96,128]{2,1,0:T(8,128)(2,1)}), bf16[8,96,128]{2,1,0:T(8,128)(2,1)S(1)}, u32[]{:S(2)}, u32[]{:S(2)}) async-start(bf16[8,96,128]{2,1,0:T(8,128)(2,1)} %broadcast_in_dim.10), calls=%async_computation.2 | async-start | bytes 393216 | tf_op jit(solution)/shard_map/all_to_all | solution.py:43
  81.8 13.9 %all-to-all-done.2 = bf16[8,96,128]{2,1,0:T(8,128)(2,1)S(1)} async-done(((bf16[8,96,128]{2,1,0:T(8,128)(2,1)}), bf16[8,96,128]{2,1,0:T(8,128)(2,1)S(1)}, u32[]{:S(2)}, u32[]{:S(2)}) %all-to-all-start.2) | async-done | bytes 196640 | tf_op jit(solution)/shard_map/all_to_all | solution.py:43
  95.7 12.1 %all-gather.1 = bf16[32,96,128]{2,1,0:T(8,128)(2,1)S(1)} all-gather(bf16[8,96,128]{2,1,0:T(8,128)(2,1)S(1)} %all-to-all-done.2), channel_id=3, replica_groups=mesh['grp'=4,'zh'=8,'zl'=2,'core'=2] {'zl','core'}, dimensions={0}, use_global_device_ids=true | all-gather | bytes 983040 | tf_op jit(solution)/shard_map/all_gather | solution.py:43
  107.8 2.7 %output_rows.1 = bf16[8,64,128]{2,1,0:T(8,128)(2,1)} custom-call(bf16[4,8,96,128]{3,2,1,0:T(8,128)(2,1)S(1)} %bitcast.104, f32[64,128]{1,0:T(8,128)S(1)} %get-tuple-element.25.columns, bf16[64,4096]{1,0:T(8,128)(2,1)} %bitcast.110), custom_call_target="tpu_custom_call" | custom-call | tf_op jit(solution)/shard_map/output_rows/pallas_call | solution.py:59
  110.5 3.6 %all-to-all-start.3 = ((bf16[8,64,128]{2,1,0:T(8,128)(2,1)}), bf16[8,64,128]{2,1,0:T(8,128)(2,1)S(1)}, u32[]{:S(2)}, u32[]{:S(2)}) async-start(bf16[8,64,128]{2,1,0:T(8,128)(2,1)} %output_rows.1), calls=%async_computation.3 | async-start | bytes 262144 | tf_op jit(solution)/shard_map/all_to_all | solution.py:43
  114.1 0.9 fusion.13
  115.0 14.4 %all-to-all-done.3 = bf16[8,64,128]{2,1,0:T(8,128)(2,1)S(1)} async-done(((bf16[8,64,128]{2,1,0:T(8,128)(2,1)}), bf16[8,64,128]{2,1,0:T(8,128)(2,1)S(1)}, u32[]{:S(2)}, u32[]{:S(2)}) %all-to-all-start.3) | async-done | bytes 131104 | tf_op jit(solution)/shard_map/all_to_all | solution.py:43
  129.4 7.9 %all-gather.2 = bf16[32,64,128]{2,1,0:T(8,128)(2,1)S(1)} all-gather(bf16[8,64,128]{2,1,0:T(8,128)(2,1)S(1)} %all-to-all-done.3), channel_id=4, replica_groups=mesh['grp'=4,'zh'=8,'zl'=2,'core'=2] {'zl','core'}, dimensions={0}, use_global_device_ids=true | all-gather | bytes 655360 | tf_op jit(solution)/shard_map/all_gather | solution.py:43
  137.3 5.9 %expert_rows.1 = (bf16[32,40,128]{2,1,0:T(8,128)(2,1)}, f32[3,2048]{1,0:T(4,128)S(1)}) custom-call(s32[1]{0:T(128)} %bitcast.place, f32[1,2048]{1,0:T(1,128)} %bitcast.128, bf16[4,8,64,128]{3,2,1,0:T(8,128)(2,1)S(1)} %bitcast.105, f32[32,3]{1,0:T(8,128)S(1)} %bitcast.106, bf16[1,2048,512]{2,1,0:T(8,128)(2,1)} %gate_hbm.3, bf16[1,2048,512]{2,1,0:T(8,128)(2,1)} %up_hbm.1, ...), custom_call_target="tpu_custom_call" | custom-call | tf_op jit(solution)/shard_map/expert_rows/pallas_call | solution.py:59
  143.2 4.2 %all-to-all-start.4 = ((bf16[32,40,128]{2,1,0:T(8,128)(2,1)}), bf16[32,40,128]{2,1,0:T(8,128)(2,1)S(1)}, u32[]{:S(2)}, u32[]{:S(2)}) async-start(bf16[32,40,128]{2,1,0:T(8,128)(2,1)} %get-tuple-element.27), calls=%async_computation.4 | async-start | bytes 655360 | tf_op jit(solution)/shard_map/all_to_all | solution.py:465
  147.5 7.0 %multiply_add_fusion = f32[3,64,64,128]{3,2,1,0:T(8,128)} fusion(f32[3,64,64,128]{3,2,1,0:T(8,128)} %param.28, f32[3,64,128]{2,1,0:T(8,128)S(1)} %broadcast_bitcast_fusion, f32[3,64,64]{2,1,0:T(8,128)S(1)} %broadcast_multiply_fusion, f32[3,64]{1,0:T(4,128)S(1)} %copy-done.8), kind=kLoop, calls=%fused_computation | loop fusion | flops 4718592 | bytes 12731136 | tf_op jit(solution)/shard_map/add | solution.py:415
  155.2 16.5 %all-to-all-done.4 = bf16[32,40,128]{2,1,0:T(8,128)(2,1)S(1)} async-done(((bf16[32,40,128]{2,1,0:T(8,128)(2,1)}), bf16[32,40,128]{2,1,0:T(8,128)(2,1)S(1)}, u32[]{:S(2)}, u32[]{:S(2)}) %all-to-all-start.4) | async-done | bytes 327712 | tf_op jit(solution)/shard_map/all_to_all | solution.py:465
  172.4 1.0 fusion.8
  (69 shorter events, 7.9 us)
Async XLA Ops:
  0.6 171.7 %copy-start = (bf16[512,2048]{1,0:T(8,128)(2,1)S(1)}, bf16[512,2048]{1,0:T(8,128)(2,1)}, u32[]{:S(2)}) copy-start(bf16[512,2048]{1,0:T(8,128)(2,1)} %param.51) | copy-start | bytes 6291460
  0.6 65.5 %copy-start.4 = (f32[6144]{0:T(1024)S(1)}, f32[6144]{0:T(1024)}, u32[]{:S(2)}) copy-start(f32[6144]{0:T(1024)} %param.39) | copy-start | bytes 73732
  2.2 29.8 %all-to-all-start = ((bf16[8,48,128]{2,1,0:T(8,128)(2,1)}), bf16[8,48,128]{2,1,0:T(8,128)(2,1)S(1)}, u32[]{:S(2)}, u32[]{:S(2)}) async-start(bf16[8,48,128]{2,1,0:T(8,128)(2,1)} %open_rows.1), calls=%async_computation | async-start | bytes 196608 | tf_op jit(solution)/shard_map/all_to_all | solution.py:352
  43.6 33.6 %copy-start.1 = (bf16[3584,128]{1,0:T(8,128)(2,1)}, bf16[3584,128]{1,0:T(8,128)(2,1)S(1)}, u32[]{:S(2)}) copy-start(bf16[3584,128]{1,0:T(8,128)(2,1)S(1)} %all-gather) | copy-start | bytes 2752516
  47.0 17.2 %all-to-all-start.1 = ((bf16[32,8,128]{2,1,0:T(8,128)(2,1)}), bf16[32,8,128]{2,1,0:T(8,128)(2,1)S(1)}, u32[]{:S(2)}, u32[]{:S(2)}) async-start(bf16[32,8,128]{2,1,0:T(8,128)(2,1)} %get-tuple-element.18), calls=%async_computation.1 | async-start | bytes 131072 | tf_op jit(solution)/shard_map/all_to_all | solution.py:375
  54.8 10.1 %copy-start.7 = (f32[3,64]{1,0:T(4,128)}, f32[3,64]{1,0:T(4,128)S(1)}, u32[]{:S(2)}) copy-start(f32[3,64]{1,0:T(4,128)S(1)} %get-tuple-element.41) | copy-start | bytes 2308
  66.2 47.9 %copy-start.2 = (bf16[3,3,6144]{2,1,0:T(4,128)(2,1)S(1)}, bf16[3,3,6144]{2,1,0:T(4,128)(2,1)}, u32[]{:S(2)}) copy-start(bf16[3,3,6144]{2,1,0:T(4,128)(2,1)} %param.27) | copy-start | bytes 331780
  68.3 5.6 %copy-start.3 = (f32[3,8,8,64]{3,2,1,0:T(8,128)S(1)}, f32[3,8,8,64]{3,2,1,0:T(8,128)}, u32[]{:S(2)}) copy-start(f32[3,8,8,64]{3,2,1,0:T(8,128)} %reshape.186) | copy-start | bytes 147460
  77.2 18.5 %all-to-all-start.2 = ((bf16[8,96,128]{2,1,0:T(8,128)(2,1)}), bf16[8,96,128]{2,1,0:T(8,128)(2,1)S(1)}, u32[]{:S(2)}, u32[]{:S(2)}) async-start(bf16[8,96,128]{2,1,0:T(8,128)(2,1)} %broadcast_in_dim.10), calls=%async_computation.2 | async-start | bytes 393216 | tf_op jit(solution)/shard_map/all_to_all | solution.py:43
  80.9 66.5 %copy-start.8 = (f32[3,64]{1,0:T(4,128)S(1)}, f32[3,64]{1,0:T(4,128)}, u32[]{:S(2)}) copy-start(f32[3,64]{1,0:T(4,128)} %copy-done.7) | copy-start | bytes 2308
  110.5 18.9 %all-to-all-start.3 = ((bf16[8,64,128]{2,1,0:T(8,128)(2,1)}), bf16[8,64,128]{2,1,0:T(8,128)(2,1)S(1)}, u32[]{:S(2)}, u32[]{:S(2)}) async-start(bf16[8,64,128]{2,1,0:T(8,128)(2,1)} %output_rows.1), calls=%async_computation.3 | async-start | bytes 262144 | tf_op jit(solution)/shard_map/all_to_all | solution.py:43
  143.2 28.5 %all-to-all-start.4 = ((bf16[32,40,128]{2,1,0:T(8,128)(2,1)}), bf16[32,40,128]{2,1,0:T(8,128)(2,1)S(1)}, u32[]{:S(2)}, u32[]{:S(2)}) async-start(bf16[32,40,128]{2,1,0:T(8,128)(2,1)} %get-tuple-element.27), calls=%async_computation.4 | async-start | bytes 655360 | tf_op jit(solution)/shard_map/all_to_all | solution.py:465
  147.5 7.0 %copy-start.6 = (s32[3,6]{1,0:T(4,128)S(1)}, s32[3,6]{1,0:T(4,128)}, u32[]{:S(2)}) copy-start(s32[3,6]{1,0:T(4,128)} %ids.1) | copy-start | bytes 220
  147.5 7.3 %copy-start.5 = (f32[2048]{0:T(1024)S(1)}, f32[2048]{0:T(1024)}, u32[]{:S(2)}) copy-start(f32[2048]{0:T(1024)} %param.43) | copy-start | bytes 24580
  147.5 7.3 %copy-start.9 = (bf16[2048,32]{0,1:T(8,128)(2,1)S(1)}, bf16[2048,32]{0,1:T(8,128)(2,1)}, u32[]{:S(2)}) copy-start(bf16[2048,32]{0,1:T(8,128)(2,1)} %param.44) | copy-start | bytes 393220

commit v5 on v4

--- a/solution.py
+++ b/solution.py
@@ -54,7 +54,7 @@
     specs = [smem] * len(scalars) + [vmem] * (len(fetched) + len(arrays))
     specs += [hbm] * (len(far) + len(remote))
     landing = [pltpu.VMEM(array.shape, array.dtype) for array in far]
-    waits = [pltpu.SemaphoreType.DMA((len(far),))] if far else []
+    waits = [pltpu.SemaphoreType.DMA((4,))] if far else []
     waits += [pltpu.SemaphoreType.DMA((8,))] * len(remote)
     return pl.pallas_call(
         kernel,
@@ -170,6 +170,93 @@
     columns[...] = jnp.where(me % 2 == 0, across[:height], across[height:])
 
 
+def mixer_kernel(
+    gain, bias, heads, window, taps, pieces, state_hbm, out, fresh, fed, written, named, flat, state, sems
+):
+    far = out.shape[0]
+    slabs = fresh.shape[0]
+    past = taps.shape[0] - 1
+    count, lines, lanes = pieces.shape
+    groups = written.shape[1]
+    blocks = fed.shape[1]
+    share = blocks // groups
+    quarter = lanes // share
+    pair = lanes // state.shape[2]
+    copies = [
+        pltpu.make_async_copy(state_hbm.at[row], state.at[row], sems.at[row])
+        for row in range(slabs)
+    ]
+    for copy in copies:
+        copy.start()
+    flat[...] = pieces[...].reshape(count * lines, lanes).astype(jnp.float32)
+    named[...] = flat[pl.ds(2 * slabs, count, stride=lines), :]
+    line = lax.broadcasted_iota(jnp.int32, (blocks, lanes), 0)
+    lane = lax.broadcasted_iota(jnp.int32, (blocks, lanes), 1)
+    lane_of = lax.broadcasted_iota(jnp.int32, (groups, lanes), 1)
+    wide_lane = lax.broadcasted_iota(jnp.int32, (lanes, lanes), 1)
+    even = heads[pl.ds(0, blocks, stride=pair), :]
+    odd = heads[pl.ds(1, blocks, stride=pair), :]
+
+    def per_head(column):
+        return jnp.where(
+            lane < lanes // 2, even[:, column : column + 1], odd[:, column : column + 1]
+        )
+
+    def by_group(values):
+        spread = jnp.zeros((blocks, lanes), jnp.float32)
+        for g in range(groups):
+            spread = jnp.where(line // share == g, values(g), spread)
+        return spread
+
+    skip = per_head(2 * slabs)
+    for row in range(slabs):
+        gate = flat[pl.ds(row, count, stride=lines), :]
+        vectors = []
+        for kind in range(2):
+            vector = jnp.zeros((groups, lanes), jnp.float32)
+            for q in range(share):
+                part = flat[pl.ds(q * lines + 2 * slabs + kind, groups, stride=share * lines), :]
+                shift = (q - row) * quarter % lanes
+                part = pltpu.roll(part, shift, 1) if shift else part
+                vector = jnp.where(lane_of // quarter == q, part, vector)
+            vectors.append(vector)
+        newest = jnp.concatenate(
+            [flat[pl.ds(slabs + row, count, stride=lines), :]] + vectors, axis=0
+        )
+        fresh[row] = newest.astype(jnp.bfloat16)
+        taken = newest * taps[past].astype(jnp.float32)
+        for t in range(past):
+            taken += window[row * past + t].astype(jnp.float32) * taps[t].astype(jnp.float32)
+        taken += bias[...]
+        convolved = taken / (1.0 + jnp.exp(-taken))
+        head_input = convolved[:blocks]
+        write = convolved[blocks : blocks + groups]
+        read = convolved[blocks + groups :]
+        steps = per_head(row) * head_input
+        fed[row] = steps
+        written[row] = write
+        overlap = jnp.sum(write * read, axis=1, keepdims=True)
+        direct = by_group(lambda g: overlap[g : g + 1])
+        copies[row].wait()
+        columns = jnp.zeros((lanes, lanes), jnp.float32)
+        for j in range(blocks):
+            block = state[row, pair * j : pair * (j + 1)].reshape(lanes, lanes)
+            g = j // share
+            total = jnp.sum(block * read[g : g + 1], axis=1, keepdims=True)
+            columns = jnp.where(wide_lane == j, total, columns)
+        mixed = per_head(slabs + row) * columns.T[:blocks] + steps * direct + skip * head_input
+        mixed = mixed.astype(jnp.bfloat16).astype(jnp.float32)
+        gated = mixed * (gate / (1.0 + jnp.exp(-gate)))
+        square = jnp.sum(gated * gated, axis=1, keepdims=True)
+        total = by_group(
+            lambda g: jnp.sum(square[g * share : (g + 1) * share], axis=0, keepdims=True)
+        )
+        scale = lax.rsqrt(total / (share * lanes) + epsilon)
+        result = (gated * scale * gain[...]).astype(jnp.bfloat16)
+        for z in range(far):
+            out[z, row * blocks : (row + 1) * blocks] = result
+
+
 def output_kernel(gathered, columns, weights_hbm, out, flat, wide, rows, weights, sems):
     copy = pltpu.make_async_copy(weights_hbm, weights, sems.at[0])
     copy.start()
@@ -216,7 +303,8 @@
 ):
     near, far, features, lanes = resid.shape
     width = near * far * features
-    count, slabs = chosen.shape
+    count = chosen.shape[0]
+    slabs = own.shape[0]
     lines = out.shape[1]
     copies = [
         pltpu.make_async_copy(gate_hbm, gate, sems.at[0]),
@@ -274,7 +362,7 @@
 
     lane = lax.broadcasted_iota(jnp.int32, (count, lanes), 1)
     line = lax.broadcasted_iota(jnp.int32, (count, lanes), 0)
-    flags = chosen[...]
+    flags = chosen[:, slabs * (LANES // (slabs + 1)) :]
     picks = []
     for s in range(CAP):
         pick = jnp.zeros((count, lanes), jnp.float32)
@@ -350,11 +438,17 @@
         [],
     )
     opened = lax.all_to_all(opening, "zh", 0, 0, tiled=True).reshape(-1, LANES)
-    later, _ = lax.optimization_barrier(((shared_gate, shared_up), opening))
+    later = (shared_gate, shared_up, conv_window, conv_taps, conv_bias, group_gain)
+    later, _ = lax.optimization_barrier((later, opening))
     blocks = [
         jnp.moveaxis(weights.reshape(features, near, LANES), 1, 0).reshape(-1, LANES)
-        for weights in later
+        for weights in later[:2]
     ]
+    span = conv_bias.shape[0] // LANES
+    window_blocks = later[2].reshape(-1, span, LANES)
+    taps_blocks = later[3].reshape(-1, span, LANES)
+    bias_blocks = later[4].reshape(-1, LANES)
+    group_gain = later[5].reshape(-1, LANES)
     gathered = lax.all_gather(jnp.concatenate([opened, *blocks], axis=0), NEAR)
     col_width = out_proj.shape[1]
     message, resid_cols = fast_call(
@@ -374,61 +468,36 @@
     )
     pieces = lax.all_to_all(message, EP, 0, 0, tiled=True)
 
-    later = (hidden, conv_window, conv_taps, decay_shift, step_bias, decay_log)
+    later = (hidden, decay_shift, step_bias, decay_log, skip_scale)
     later, _ = lax.optimization_barrier((later, message))
-    hidden_later, conv_window, conv_taps, decay_shift, step_bias, decay_log = later
+    hidden_later, decay_shift, step_bias, decay_log, skip_scale = later
     hidden_wide = hidden_later.astype(jnp.float32)
     normed_local = (hidden_wide * row_scale(hidden_wide) * mix_gain).astype(jnp.bfloat16)
     step_raw = matmul(normed_local, step_proj)
 
-    gate_rows = jnp.moveaxis(pieces[:, :rows], 0, 1).reshape(rows, -1)
-    input_rows = jnp.moveaxis(pieces[:, rows : 2 * rows], 0, 1).reshape(rows, -1)
-    tail_width = rows * write_proj.shape[1]
-    write_rows, read_rows = (
-        jnp.moveaxis(pieces[:, 2 * rows + k, :tail_width].reshape(count, rows, -1), 0, 1).reshape(
-            rows, -1
-        )
-        for k in range(2)
-    )
-    chosen = pieces[:, 2 * rows, tail_width : tail_width + rows].astype(jnp.float32)
-
-    inner_width = gate_rows.shape[1]
-    state_span = GROUPS * STATE
-    head_count = step_bias.shape[0]
-    per_group = head_count // GROUPS
-    fresh_row = jnp.concatenate([input_rows, write_rows, read_rows], axis=1)
-    window = jnp.concatenate([conv_window, fresh_row[:, None, :]], axis=1)
-    convolved = jax.nn.silu(
-        jnp.sum(window.astype(jnp.float32) * conv_taps.astype(jnp.float32)[None], axis=1)
-        + conv_bias
-    )
-    head_input = convolved[:, :inner_width].reshape(rows, GROUPS, per_group, HEAD_DIM)
-    write_vec = convolved[:, inner_width : inner_width + state_span].reshape(rows, GROUPS, STATE)
-    read_vec = convolved[:, inner_width + state_span :].reshape(rows, GROUPS, STATE)
+    inner_width = out_proj.shape[0]
+    blocks = inner_width // LANES
     step_size = jax.nn.softplus(step_raw + step_bias)
-    decay_rate = jnp.exp(decay_shift - step_size * jnp.exp(decay_log)).reshape(
-        rows, GROUPS, per_group
-    )
-    step_group = step_size.reshape(rows, GROUPS, per_group)
-    carried = ssm_state.reshape(rows, GROUPS, per_group, HEAD_DIM, STATE)
-    next_state = (
-        decay_rate[..., None, None] * carried
-        + (step_group[..., None] * head_input)[..., None] * write_vec[:, :, None, None, :]
-    )
-    mixed_out = jnp.einsum("sgepn,sgn->sgep", next_state, read_vec)
-    mixed_out = mixed_out + skip_scale.reshape(GROUPS, per_group)[None, :, :, None] * head_input
-    mixed_out = mixed_out.reshape(rows, inner_width).astype(jnp.bfloat16)
-    gated_out = mixed_out.astype(jnp.float32) * jax.nn.silu(gate_rows.astype(jnp.float32))
-    blocks = gated_out.reshape(rows, GROUPS, -1)
-    gated_out = ((blocks * row_scale(blocks)).reshape(rows, inner_width) * group_gain).astype(
-        jnp.bfloat16
-    )
-
-    gated_all = near_gather(
-        jnp.broadcast_to(
-            gated_out.reshape(1, -1, LANES), (far, rows * inner_width // LANES, LANES)
-        )
-    )
+    decay_rate = jnp.exp(decay_shift - step_size * jnp.exp(decay_log))
+    heads = jnp.concatenate([step_size, decay_rate, skip_scale[None]], axis=0)
+    heads = jnp.pad(heads, ((0, LANES - heads.shape[0]), (0, 0))).T
+    gated_rows, fresh, fed, write_vec, chosen = fast_call(
+        mixer_kernel,
+        "mix_rows",
+        [
+            ((far, rows * blocks, LANES), jnp.bfloat16),
+            ((rows, span, LANES), jnp.bfloat16),
+            ((rows, blocks, LANES), jnp.float32),
+            ((rows, GROUPS, STATE), jnp.float32),
+            ((count, LANES), jnp.float32),
+        ],
+        [((count * 8, LANES), jnp.float32)],
+        [],
+        [group_gain, bias_blocks],
+        [heads, window_blocks, taps_blocks, pieces],
+        [ssm_state],
+    )
+    gated_all = near_gather(gated_rows)
     (resid_part,) = fast_call(
         output_kernel,
         "output_rows",
@@ -464,7 +533,16 @@
     )
     returned = lax.all_to_all(outbound, EP, 0, 0, tiled=True)
 
-    expert_ids, outbound = lax.optimization_barrier((expert_ids, outbound))
+    later = (expert_ids, conv_window, fresh, fed, write_vec, decay_rate)
+    later, _ = lax.optimization_barrier((later, outbound))
+    expert_ids, conv_window, fresh, fed, write_vec, decay_rate = later
+    next_window = jnp.concatenate([conv_window[:, 1:], fresh.reshape(rows, 1, -1)], axis=1)
+    per_group = step_size.shape[1] // GROUPS
+    next_state = (
+        decay_rate[:, :, None, None] * ssm_state
+        + fed.reshape(rows, -1, HEAD_DIM)[..., None]
+        * jnp.repeat(write_vec, per_group, axis=1)[:, :, None, :]
+    )
     member = jnp.any(
         expert_ids[:, :, None] == jnp.arange(experts, dtype=jnp.int32)[None, None, :], axis=1
     )
@@ -483,7 +561,7 @@
     pre = jnp.sum(pre.astype(jnp.float32), axis=0).transpose(1, 2, 0, 3).reshape(2, rows, units)
     shared_hidden = (jax.nn.silu(norm_scale * pre[0]) * (norm_scale * pre[1])).astype(jnp.bfloat16)
     layer_out = (resid_own + routed + matmul(shared_hidden, shared_down)).astype(jnp.bfloat16)
-    return (layer_out, next_state.reshape(ssm_state.shape), window[:, 1:])
+    return (layer_out, next_state, next_window)
 
 
 def solution(mesh):

time: 175 us -> 164 us (0.937)
  blocking collectives: 31.6 us -> 67 us
  waiting for transfers between devices: 62.9 us -> 33.1 us
  starting transfers between devices: 32.8 us -> 25.7 us
  local copies, waits for them, and re-layouts: 9.94 us -> 4.77 us
  Pallas kernels: 13.6 us -> 17.8 us
  other arithmetic: 13.8 us -> 9.69 us
  matrix products: 7.79 us -> 3.95 us
    all_to_all x0 -> x2, blocking collectives: none -> 34.6 us  [near_gather(): return lax.all_gather(lax.all_to_all(copies, 'zh', 0, 0, tiled=True), NEAR)]
    all_to_all x2 -> x0, waiting for transfers between devices: 28.3 us -> none  [near_gather(): return lax.all_gather(lax.all_to_all(copies, 'zh', 0, 0, tiled=True), NEAR)]
    all_to_all x2 -> x0, starting transfers between devices: 7.18 us -> none  [near_gather(): return lax.all_gather(lax.all_to_all(copies, 'zh', 0, 0, tiled=True), NEAR)]
    dot_general x1 -> x0, matrix products: 4.75 us -> none  [shards(): mixed_out = jnp.einsum('sgepn,sgn->sgep', next_state, read_vec)]
    pallas_call x4 -> x5, Pallas kernels: 13.6 us -> 17.8 us  [fast_call(): pl.pallas_call(kernel, name=name, out_shape=tuple((pltpu.VMEM(shape, dtyp...]
    mul x6 -> x2, local copies, waits for them, and re-layouts: 2.89 us -> 0.09 us  [shards(): fed.reshape(rows, -1, HEAD_DIM)[..., None]]
    all_to_all x1, waiting for transfers between devices: 16.5 us -> 14.7 us  [shards(): returned = lax.all_to_all(outbound, EP, 0, 0, tiled=True)]
  transfers between devices with their start and end apart: 5 -> 3, of which waited for: 5 -> 3; matrix products, arithmetic and copies ran while one was open for 10% -> 10% of each run, Pallas kernels for 0% -> 0%
where the time goes in v5:
time: 164 us; the launch traced here: 163 us
  blocking collectives  67 us (41%)
  waiting for transfers between devices  33.1 us (20%)
  starting transfers between devices  25.7 us (16%)
  Pallas kernels  17.8 us (11%)
  other arithmetic  9.69 us (6%)
  local copies, waits for them, and re-layouts  4.77 us (3%)
  matrix products  3.95 us (2%)
    all_to_all x2, blocking collectives, near_gather(): return lax.all_gather(lax.all_to_all(copies, 'zh', 0, 0, tiled=True), NEAR)  34.6 us
    all_gather x2, blocking collectives, near_gather(): return lax.all_gather(lax.all_to_all(copies, 'zh', 0, 0, tiled=True), NEAR)  20.8 us
    pallas_call x5, Pallas kernels, fast_call(): pl.pallas_call(kernel, name=name, out_shape=tuple((pltpu.VMEM(shape, dtyp...  17.8 us
    all_to_all x1, starting transfers between devices, shards(): opened = lax.all_to_all(opening, 'zh', 0, 0, tiled=True).reshape(-1, LANES)  17.3 us
    all_to_all x1, waiting for transfers between devices, shards(): returned = lax.all_to_all(outbound, EP, 0, 0, tiled=True)  14.7 us
    all_gather x1, blocking collectives, shards(): gathered = lax.all_gather(jnp.concatenate([opened, *blocks], axis=0), NEAR)  11.6 us
    all_to_all x1, waiting for transfers between devices, shards(): pieces = lax.all_to_all(message, EP, 0, 0, tiled=True)  9.47 us
    all_to_all x1, waiting for transfers between devices, shards(): opened = lax.all_to_all(opening, 'zh', 0, 0, tiled=True).reshape(-1, LANES)  8.9 us
  transfers between devices with their start and end apart: 3, of which 3 were waited for; matrix products, arithmetic and copies ran while one was open for 10% of the time, Pallas kernels for 0%

profile of v5, /device:TPU:69, one launch (start us, length us, event | category | flops | bytes accessed | tf_op | source)
XLA Modules:
  0.0 162.8 jit_solution(13054930610810232888)
XLA Ops:
  0.6 1.5 open_rows.1
  2.2 17.3 %all-to-all-start = ((bf16[8,48,128]{2,1,0:T(8,128)(2,1)}), bf16[8,48,128]{2,1,0:T(8,128)(2,1)S(1)}, u32[]{:S(2)}, u32[]{:S(2)}) async-start(bf16[8,48,128]{2,1,0:T(8,128)(2,1)} %open_rows.1), calls=%async_computation | async-start | bytes 196608 | tf_op jit(solution)/shard_map/all_to_all | solution.py:440
  19.4 0.9 reshape.92
  20.3 0.9 reshape.90
  21.2 1.0 reshape.94.window
  22.2 0.8 copy.82
  23.0 8.9 %all-to-all-done = bf16[8,48,128]{2,1,0:T(8,128)(2,1)S(1)} async-done(((bf16[8,48,128]{2,1,0:T(8,128)(2,1)}), bf16[8,48,128]{2,1,0:T(8,128)(2,1)S(1)}, u32[]{:S(2)}, u32[]{:S(2)}) %all-to-all-start) | async-done | bytes 98336 | tf_op jit(solution)/shard_map/all_to_all | solution.py:440
  32.0 11.6 %all-gather = bf16[3584,128]{1,0:T(8,128)(2,1)S(1)} all-gather(bf16[896,128]{1,0:T(8,128)(2,1)S(1)} %pad_maximum_fusion), channel_id=2, replica_groups=mesh['grp'=4,'zh'=8,'zl'=2,'core'=2] {'zl','core'}, dimensions={0}, use_global_device_ids=true | all-gather | bytes 1146880 | tf_op jit(solution)/shard_map/all_gather | solution.py:452
  43.6 3.4 %project_rows.1 = (bf16[32,8,128]{2,1,0:T(8,128)(2,1)}, f32[64,128]{1,0:T(8,128)S(1)}) custom-call(s32[1]{0:T(128)} %bitcast.place, s32[3,6]{1,0:T(4,128)} %ids.1, f32[1,2048]{1,0:T(1,128)} %bitcast.79, bf16[4,896,128]{2,1,0:T(8,128)(2,1)S(1)} %bitcast.59, bf16[2048,128]{1,0:T(8,128)(2,1)} %gate_hbm.2, bf16[2048,128]{1,0:T(8,128)(2,1)} %input_hbm.1, ...), custom_call_target="tpu_custom_call" | custom-call | tf_op jit(solution)/shard_map/project_rows/pallas_call | solution.py:59
  47.0 4.2 %all-to-all-start.1 = ((bf16[32,8,128]{2,1,0:T(8,128)(2,1)}), bf16[32,8,128]{2,1,0:T(8,128)(2,1)S(1)}, u32[]{:S(2)}, u32[]{:S(2)}) async-start(bf16[32,8,128]{2,1,0:T(8,128)(2,1)} %get-tuple-element.33), calls=%async_computation.1 | async-start | bytes 131072 | tf_op jit(solution)/shard_map/all_to_all | solution.py:469
  51.2 0.7 exp.18
  51.9 0.9 fusion.6
  52.7 1.3 subtract_exponential_fusion
  54.0 0.7 pad_maximum_fusion.2
  54.7 0.1 copy.63
  54.8 9.5 %all-to-all-done.1.pieces = bf16[32,8,128]{2,1,0:T(8,128)(2,1)S(1)} async-done(((bf16[32,8,128]{2,1,0:T(8,128)(2,1)}), bf16[32,8,128]{2,1,0:T(8,128)(2,1)S(1)}, u32[]{:S(2)}, u32[]{:S(2)}) %all-to-all-start.1) | async-done | bytes 65568 | tf_op jit(solution)/shard_map/all_to_all | solution.py:469
  64.2 4.8 %mix_rows.1 = (bf16[8,96,128]{2,1,0:T(8,128)(2,1)S(1)}, bf16[3,48,128]{2,1,0:T(8,128)(2,1)S(1)}, f32[3,32,128]{2,1,0:T(8,128)S(1)}, f32[3,8,128]{2,1,0:T(8,128)S(1)}, f32[32,128]{1,0:T(8,128)S(1)}) custom-call(f32[32,128]{1,0:T(8,128)} %bitcast.78, f32[48,128]{1,0:T(8,128)} %bitcast.77, f32[64,128]{1,0:T(8,128)S(1)} %pad_bitcast_fusion.heads, ...), custom_call_target="tpu_custom_call" | custom-call | tf_op jit(solution)/shard_map/mix_rows/pallas_call | solution.py:59
  69.0 17.8 %all_to_all.25 = bf16[8,96,128]{2,1,0:T(8,128)(2,1)S(1)} all-to-all(bf16[8,96,128]{2,1,0:T(8,128)(2,1)S(1)} %get-tuple-element.41), channel_id=1, replica_groups=mesh['grp'=4,'zh'=8,'zl'=2,'core'=2] {'zh'}, dimensions={0} | all-to-all | bytes 393216 | tf_op jit(solution)/shard_map/all_to_all | solution.py:43
  86.9 11.9 %all-gather.1 = bf16[32,96,128]{2,1,0:T(8,128)(2,1)S(1)} all-gather(bf16[8,96,128]{2,1,0:T(8,128)(2,1)S(1)} %all_to_all.25), channel_id=3, replica_groups=mesh['grp'=4,'zh'=8,'zl'=2,'core'=2] {'zl','core'}, dimensions={0}, use_global_device_ids=true | all-gather | bytes 983040 | tf_op jit(solution)/shard_map/all_gather | solution.py:43
  98.8 2.1 %output_rows.1 = bf16[8,64,128]{2,1,0:T(8,128)(2,1)S(1)} custom-call(bf16[4,8,96,128]{3,2,1,0:T(8,128)(2,1)S(1)} %bitcast.61, f32[64,128]{1,0:T(8,128)S(1)} %get-tuple-element.42.columns, bf16[64,4096]{1,0:T(8,128)(2,1)} %bitcast.66), custom_call_target="tpu_custom_call" | custom-call | tf_op jit(solution)/shard_map/output_rows/pallas_call | solution.py:59
  100.9 16.8 %all_to_all.26 = bf16[8,64,128]{2,1,0:T(8,128)(2,1)S(1)} all-to-all(bf16[8,64,128]{2,1,0:T(8,128)(2,1)S(1)} %output_rows.1), channel_id=1, replica_groups=mesh['grp'=4,'zh'=8,'zl'=2,'core'=2] {'zh'}, dimensions={0} | all-to-all | bytes 262144 | tf_op jit(solution)/shard_map/all_to_all | solution.py:43
  117.7 8.9 %all-gather.2 = bf16[32,64,128]{2,1,0:T(8,128)(2,1)S(1)} all-gather(bf16[8,64,128]{2,1,0:T(8,128)(2,1)S(1)} %all_to_all.26), channel_id=4, replica_groups=mesh['grp'=4,'zh'=8,'zl'=2,'core'=2] {'zl','core'}, dimensions={0}, use_global_device_ids=true | all-gather | bytes 655360 | tf_op jit(solution)/shard_map/all_gather | solution.py:43
  126.6 5.9 %expert_rows.1 = (bf16[32,40,128]{2,1,0:T(8,128)(2,1)}, f32[3,2048]{1,0:T(4,128)S(1)}) custom-call(s32[1]{0:T(128)} %bitcast.place, f32[1,2048]{1,0:T(1,128)} %bitcast.80, bf16[4,8,64,128]{3,2,1,0:T(8,128)(2,1)S(1)} %bitcast.62, f32[32,128]{1,0:T(8,128)S(1)} %get-tuple-element.43.chosen, bf16[1,2048,512]{2,1,0:T(8,128)(2,1)} %gate_hbm.3, ...), custom_call_target="tpu_custom_call" | custom-call | tf_op jit(solution)/shard_map/expert_rows/pallas_call | solution.py:59
  132.5 4.2 %all-to-all-start.4 = ((bf16[32,40,128]{2,1,0:T(8,128)(2,1)}), bf16[32,40,128]{2,1,0:T(8,128)(2,1)S(1)}, u32[]{:S(2)}, u32[]{:S(2)}) async-start(bf16[32,40,128]{2,1,0:T(8,128)(2,1)} %get-tuple-element.48), calls=%async_computation.4 | async-start | bytes 655360 | tf_op jit(solution)/shard_map/all_to_all | solution.py:534
  136.9 0.1 multiply_reduce_fusion
  137.1 1.2 fusion.28
  138.6 6.9 %multiply_add_fusion = f32[3,64,64,128]{3,2,1,0:T(8,128)} fusion(f32[3,64,64,128]{3,2,1,0:T(8,128)} %state_hbm.1, f32[3,64,128]{2,1,0:T(8,128)S(1)} %broadcast_bitcast_fusion, f32[3,64,64]{2,1,0:T(8,128)S(1)} %mul.127, f32[3,64]{1,0:T(4,128)S(1)} %get-tuple-element.50), kind=kLoop, calls=%fused_computation | loop fusion | flops 4718592 | bytes 12731136 | tf_op jit(solution)/shard_map/add | solution.py:542
  145.5 0.8 pad_maximum_fusion.1
  146.4 14.7 %all-to-all-done.4 = bf16[32,40,128]{2,1,0:T(8,128)(2,1)S(1)} async-done(((bf16[32,40,128]{2,1,0:T(8,128)(2,1)}), bf16[32,40,128]{2,1,0:T(8,128)(2,1)S(1)}, u32[]{:S(2)}, u32[]{:S(2)}) %all-to-all-start.4) | async-done | bytes 327712 | tf_op jit(solution)/shard_map/all_to_all | solution.py:534
  161.3 0.2 fusion.23
  161.5 0.2 fusion
  161.8 1.0 fusion.1
  (31 shorter events, 0.7 us)
Async XLA Ops:
  0.6 161.1 %copy-start = (bf16[512,2048]{1,0:T(8,128)(2,1)S(1)}, bf16[512,2048]{1,0:T(8,128)(2,1)}, u32[]{:S(2)}) copy-start(bf16[512,2048]{1,0:T(8,128)(2,1)} %param.51) | copy-start | bytes 6291460
  2.2 29.8 %all-to-all-start = ((bf16[8,48,128]{2,1,0:T(8,128)(2,1)}), bf16[8,48,128]{2,1,0:T(8,128)(2,1)S(1)}, u32[]{:S(2)}, u32[]{:S(2)}) async-start(bf16[8,48,128]{2,1,0:T(8,128)(2,1)} %open_rows.1), calls=%async_computation | async-start | bytes 196608 | tf_op jit(solution)/shard_map/all_to_all | solution.py:440
  43.6 83.0 %copy-start.1 = (bf16[3584,128]{1,0:T(8,128)(2,1)}, bf16[3584,128]{1,0:T(8,128)(2,1)S(1)}, u32[]{:S(2)}) copy-start(bf16[3584,128]{1,0:T(8,128)(2,1)S(1)} %all-gather) | copy-start | bytes 2752516
  47.0 17.2 %all-to-all-start.1 = ((bf16[32,8,128]{2,1,0:T(8,128)(2,1)}), bf16[32,8,128]{2,1,0:T(8,128)(2,1)S(1)}, u32[]{:S(2)}, u32[]{:S(2)}) async-start(bf16[32,8,128]{2,1,0:T(8,128)(2,1)} %get-tuple-element.33), calls=%async_computation.1 | async-start | bytes 131072 | tf_op jit(solution)/shard_map/all_to_all | solution.py:469
  69.0 67.7 %copy-start.4 = (s32[3,6]{1,0:T(4,128)S(1)}, s32[3,6]{1,0:T(4,128)}, u32[]{:S(2)}) copy-start(s32[3,6]{1,0:T(4,128)} %ids.1) | copy-start | bytes 220
  69.0 68.0 %copy-start.3 = (f32[2048]{0:T(1024)S(1)}, f32[2048]{0:T(1024)}, u32[]{:S(2)}) copy-start(f32[2048]{0:T(1024)} %param.43) | copy-start | bytes 24580
  86.9 51.6 %copy-start.2 = (bf16[3,3,6144]{2,1,0:T(4,128)(2,1)S(1)}, bf16[3,3,6144]{2,1,0:T(4,128)(2,1)}, u32[]{:S(2)}) copy-start(bf16[3,3,6144]{2,1,0:T(4,128)(2,1)} %param.27) | copy-start | bytes 331780
  132.5 28.5 %all-to-all-start.4 = ((bf16[32,40,128]{2,1,0:T(8,128)(2,1)}), bf16[32,40,128]{2,1,0:T(8,128)(2,1)S(1)}, u32[]{:S(2)}, u32[]{:S(2)}) async-start(bf16[32,40,128]{2,1,0:T(8,128)(2,1)} %get-tuple-element.48), calls=%async_computation.4 | async-start | bytes 655360 | tf_op jit(solution)/shard_map/all_to_all | solution.py:534

commit v6 on v5

--- a/solution.py
+++ b/solution.py
@@ -47,22 +47,54 @@
     return [pltpu.with_memory_space_constraint(array, space) for array in arrays]
 
 
+class Late:
+    def __init__(self, source, landing, sem):
+        self.copy = pltpu.make_async_copy(source, landing, sem)
+        self.landing = landing
+        self.shape = landing.shape
+        self.here = False
+
+    def __getitem__(self, place):
+        if not self.here:
+            self.copy.wait()
+            self.here = True
+        return self.landing[place]
+
+
 def fast_call(kernel, name, outs, scratch, scalars, fetched, arrays, far=[], remote=[]):
     vmem = pl.BlockSpec(memory_space=pltpu.VMEM)
-    smem = pl.BlockSpec(memory_space=pltpu.SMEM)
     hbm = pl.BlockSpec(memory_space=pltpu.HBM)
-    specs = [smem] * len(scalars) + [vmem] * (len(fetched) + len(arrays))
-    specs += [hbm] * (len(far) + len(remote))
+    late = len(scalars) + len(fetched)
+    specs = [hbm] * late + [vmem] * len(arrays) + [hbm] * (len(far) + len(remote))
     landing = [pltpu.VMEM(array.shape, array.dtype) for array in far]
     waits = [pltpu.SemaphoreType.DMA((4,))] if far else []
     waits += [pltpu.SemaphoreType.DMA((8,))] * len(remote)
+    ends = [pltpu.SMEM(array.shape, array.dtype) for array in scalars]
+    ends += [pltpu.VMEM(array.shape, array.dtype) for array in fetched]
+    ends += [pltpu.SemaphoreType.DMA((late,))] if late else []
+
+    def body(*refs):
+        if not late:
+            return kernel(*refs)
+        sems = refs[-1]
+        operands = [
+            Late(refs[k], refs[len(refs) - 1 - late + k], sems.at[k]) for k in range(late)
+        ]
+        for operand in operands:
+            operand.copy.start()
+        kernel(*operands, *refs[late : len(refs) - 1 - late])
+        assert all(operand.here for operand in operands)
+
     return pl.pallas_call(
-        kernel,
+        body,
         name=name,
         out_shape=tuple(pltpu.VMEM(shape, dtype) for shape, dtype in outs),
         in_specs=specs,
         out_specs=(vmem,) * len(outs),
-        scratch_shapes=[pltpu.VMEM(shape, dtype) for shape, dtype in scratch] + landing + waits,
+        scratch_shapes=[pltpu.VMEM(shape, dtype) for shape, dtype in scratch]
+        + landing
+        + waits
+        + ends,
         compiler_params=pltpu.CompilerParams(vmem_limit_bytes=24 * 1024 * 1024),
     )(
         *kept_in(pltpu.HBM, scalars + fetched),
@@ -311,6 +343,16 @@
         pltpu.make_async_copy(up_hbm, up, sems.at[1]),
         pltpu.make_async_copy(down_hbm, down, sems.at[2]),
     ]
+    for copy in copies:
+        copy.start()
+    square = jnp.zeros((lanes, 1), jnp.float32)
+    for z in range(far):
+        for pair in range(near // 2):
+            block = jnp.concatenate([resid[2 * pair, z], resid[2 * pair + 1, z]], axis=0)
+            rows = block.astype(jnp.float32).T
+            start = (z * near + 2 * pair) * features
+            wide[:, start : start + 2 * features] = rows
+            square += jnp.sum(rows * rows, axis=1, keepdims=True)
     me = place[0]
     first = part_hbm.shape[1] - CAP * near * features
     for n in range(near):
@@ -323,16 +365,8 @@
                     part_sems.at[n * CAP + s],
                 )
             )
-    for copy in copies:
+    for copy in copies[3:]:
         copy.start()
-    square = jnp.zeros((lanes, 1), jnp.float32)
-    for z in range(far):
-        for pair in range(near // 2):
-            block = jnp.concatenate([resid[2 * pair, z], resid[2 * pair + 1, z]], axis=0)
-            rows = block.astype(jnp.float32).T
-            start = (z * near + 2 * pair) * features
-            wide[:, start : start + 2 * features] = rows
-            square += jnp.sum(rows * rows, axis=1, keepdims=True)
     scale = lax.rsqrt(square / width + epsilon)
     values = wide[...]
     routed[...] = (values * scale * gain[...]).astype(jnp.bfloat16)

time: 164 us -> 163 us (level)
  no operation moved by 1% of the time
where the time goes in v6:
time: 163 us; the launch traced here: 162 us
  blocking collectives  67.1 us (41%)
  waiting for transfers between devices  33 us (20%)
  starting transfers between devices  25.7 us (16%)
  Pallas kernels  17 us (10%)
  other arithmetic  9.69 us (6%)
  local copies, waits for them, and re-layouts  4.77 us (3%)
  matrix products  3.95 us (2%)
    all_to_all x2, blocking collectives, near_gather(): return lax.all_gather(lax.all_to_all(copies, 'zh', 0, 0, tiled=True), NEAR)  34.6 us
    all_gather x2, blocking collectives, near_gather(): return lax.all_gather(lax.all_to_all(copies, 'zh', 0, 0, tiled=True), NEAR)  20.8 us
    all_to_all x1, starting transfers between devices, shards(): opened = lax.all_to_all(opening, 'zh', 0, 0, tiled=True).reshape(-1, LANES)  17.3 us
    pallas_call x5, Pallas kernels, fast_call(): pl.pallas_call(body, name=name, out_shape=tuple((pltpu.VMEM(shape, dtype)...  17 us
    all_to_all x1, waiting for transfers between devices, shards(): returned = lax.all_to_all(outbound, EP, 0, 0, tiled=True)  14.7 us
    all_gather x1, blocking collectives, shards(): gathered = lax.all_gather(jnp.concatenate([opened, *blocks], axis=0), NEAR)  11.6 us
    all_to_all x1, waiting for transfers between devices, shards(): pieces = lax.all_to_all(message, EP, 0, 0, tiled=True)  9.47 us
    all_to_all x1, waiting for transfers between devices, shards(): opened = lax.all_to_all(opening, 'zh', 0, 0, tiled=True).reshape(-1, LANES)  8.9 us
  transfers between devices with their start and end apart: 3, of which 3 were waited for; matrix products, arithmetic and copies ran while one was open for 10% of the time, Pallas kernels for 0%

profile of v6, /device:TPU:69, one launch (start us, length us, event | category | flops | bytes accessed | tf_op | source)
XLA Modules:
  0.0 162.0 jit_solution(4906119346576838386)
XLA Ops:
  0.6 1.5 open_rows.1
  2.2 17.3 %all-to-all-start = ((bf16[8,48,128]{2,1,0:T(8,128)(2,1)}), bf16[8,48,128]{2,1,0:T(8,128)(2,1)S(1)}, u32[]{:S(2)}, u32[]{:S(2)}) async-start(bf16[8,48,128]{2,1,0:T(8,128)(2,1)} %open_rows.1), calls=%async_computation | async-start | bytes 196608 | tf_op jit(solution)/shard_map/all_to_all | solution.py:474
  19.5 0.9 reshape.92
  20.3 0.9 reshape.90
  21.2 1.0 reshape.94.refs_3_
  22.3 0.8 copy.82
  23.1 8.9 %all-to-all-done = bf16[8,48,128]{2,1,0:T(8,128)(2,1)S(1)} async-done(((bf16[8,48,128]{2,1,0:T(8,128)(2,1)}), bf16[8,48,128]{2,1,0:T(8,128)(2,1)S(1)}, u32[]{:S(2)}, u32[]{:S(2)}) %all-to-all-start) | async-done | bytes 98336 | tf_op jit(solution)/shard_map/all_to_all | solution.py:474
  32.0 11.6 %all-gather = bf16[3584,128]{1,0:T(8,128)(2,1)S(1)} all-gather(bf16[896,128]{1,0:T(8,128)(2,1)S(1)} %pad_maximum_fusion), channel_id=2, replica_groups=mesh['grp'=4,'zh'=8,'zl'=2,'core'=2] {'zl','core'}, dimensions={0}, use_global_device_ids=true | all-gather | bytes 1146880 | tf_op jit(solution)/shard_map/all_gather | solution.py:486
  43.6 3.0 %project_rows.1 = (bf16[32,8,128]{2,1,0:T(8,128)(2,1)}, f32[64,128]{1,0:T(8,128)S(1)}) custom-call(s32[1]{0:T(128)} %bitcast.refs_0_, s32[3,6]{1,0:T(4,128)} %refs_1_.1, f32[1,2048]{1,0:T(1,128)} %bitcast.79, bf16[4,896,128]{2,1,0:T(8,128)(2,1)S(1)} %bitcast.59, bf16[2048,128]{1,0:T(8,128)(2,1)} %refs_4_.2, bf16[2048,128]{1,0:T(8,128)(2,1)} %refs_5_.2, ...), custom_call_target="tpu_custom_call" | custom-call | tf_op jit(solution)/shard_map/project_rows/pallas_call | solution.py:88
  46.6 4.2 %all-to-all-start.1 = ((bf16[32,8,128]{2,1,0:T(8,128)(2,1)}), bf16[32,8,128]{2,1,0:T(8,128)(2,1)S(1)}, u32[]{:S(2)}, u32[]{:S(2)}) async-start(bf16[32,8,128]{2,1,0:T(8,128)(2,1)} %get-tuple-element.33), calls=%async_computation.1 | async-start | bytes 131072 | tf_op jit(solution)/shard_map/all_to_all | solution.py:503
  50.8 0.7 exp.18
  51.5 0.9 fusion.6
  52.4 1.3 subtract_exponential_fusion
  53.6 0.7 pad_maximum_fusion.2
  54.3 0.1 copy.63
  54.4 9.5 %all-to-all-done.1.refs_5_ = bf16[32,8,128]{2,1,0:T(8,128)(2,1)S(1)} async-done(((bf16[32,8,128]{2,1,0:T(8,128)(2,1)}), bf16[32,8,128]{2,1,0:T(8,128)(2,1)S(1)}, u32[]{:S(2)}, u32[]{:S(2)}) %all-to-all-start.1) | async-done | bytes 65568 | tf_op jit(solution)/shard_map/all_to_all | solution.py:503
  63.9 4.9 %mix_rows.1 = (bf16[8,96,128]{2,1,0:T(8,128)(2,1)S(1)}, bf16[3,48,128]{2,1,0:T(8,128)(2,1)S(1)}, f32[3,32,128]{2,1,0:T(8,128)S(1)}, f32[3,8,128]{2,1,0:T(8,128)S(1)}, f32[32,128]{1,0:T(8,128)S(1)}) custom-call(f32[32,128]{1,0:T(8,128)} %bitcast.78, f32[48,128]{1,0:T(8,128)} %bitcast.77, f32[64,128]{1,0:T(8,128)S(1)} %pad_bitcast_fusion.refs_2_, ...), custom_call_target="tpu_custom_call" | custom-call | tf_op jit(solution)/shard_map/mix_rows/pallas_call | solution.py:88
  68.8 17.8 %all_to_all.25 = bf16[8,96,128]{2,1,0:T(8,128)(2,1)S(1)} all-to-all(bf16[8,96,128]{2,1,0:T(8,128)(2,1)S(1)} %get-tuple-element.41), channel_id=1, replica_groups=mesh['grp'=4,'zh'=8,'zl'=2,'core'=2] {'zh'}, dimensions={0} | all-to-all | bytes 393216 | tf_op jit(solution)/shard_map/all_to_all | solution.py:43
  86.6 11.9 %all-gather.1 = bf16[32,96,128]{2,1,0:T(8,128)(2,1)S(1)} all-gather(bf16[8,96,128]{2,1,0:T(8,128)(2,1)S(1)} %all_to_all.25), channel_id=3, replica_groups=mesh['grp'=4,'zh'=8,'zl'=2,'core'=2] {'zl','core'}, dimensions={0}, use_global_device_ids=true | all-gather | bytes 983040 | tf_op jit(solution)/shard_map/all_gather | solution.py:43
  98.6 2.1 %output_rows.1 = bf16[8,64,128]{2,1,0:T(8,128)(2,1)S(1)} custom-call(bf16[4,8,96,128]{3,2,1,0:T(8,128)(2,1)S(1)} %bitcast.61, f32[64,128]{1,0:T(8,128)S(1)} %get-tuple-element.42.refs_1_, bf16[64,4096]{1,0:T(8,128)(2,1)} %bitcast.66), custom_call_target="tpu_custom_call" | custom-call | tf_op jit(solution)/shard_map/output_rows/pallas_call | solution.py:88
  100.7 16.8 %all_to_all.26 = bf16[8,64,128]{2,1,0:T(8,128)(2,1)S(1)} all-to-all(bf16[8,64,128]{2,1,0:T(8,128)(2,1)S(1)} %output_rows.1), channel_id=1, replica_groups=mesh['grp'=4,'zh'=8,'zl'=2,'core'=2] {'zh'}, dimensions={0} | all-to-all | bytes 262144 | tf_op jit(solution)/shard_map/all_to_all | solution.py:43
  117.5 8.9 %all-gather.2 = bf16[32,64,128]{2,1,0:T(8,128)(2,1)S(1)} all-gather(bf16[8,64,128]{2,1,0:T(8,128)(2,1)S(1)} %all_to_all.26), channel_id=4, replica_groups=mesh['grp'=4,'zh'=8,'zl'=2,'core'=2] {'zl','core'}, dimensions={0}, use_global_device_ids=true | all-gather | bytes 655360 | tf_op jit(solution)/shard_map/all_gather | solution.py:43
  126.4 5.4 %expert_rows.1 = (bf16[32,40,128]{2,1,0:T(8,128)(2,1)}, f32[3,2048]{1,0:T(4,128)S(1)}) custom-call(s32[1]{0:T(128)} %bitcast.refs_0_, f32[1,2048]{1,0:T(1,128)} %bitcast.80, bf16[4,8,64,128]{3,2,1,0:T(8,128)(2,1)S(1)} %bitcast.62, f32[32,128]{1,0:T(8,128)S(1)} %get-tuple-element.43.refs_3_, bf16[1,2048,512]{2,1,0:T(8,128)(2,1)} %refs_4_.3, ...), custom_call_target="tpu_custom_call" | custom-call | tf_op jit(solution)/shard_map/expert_rows/pallas_call | solution.py:88
  131.8 4.2 %all-to-all-start.4 = ((bf16[32,40,128]{2,1,0:T(8,128)(2,1)}), bf16[32,40,128]{2,1,0:T(8,128)(2,1)S(1)}, u32[]{:S(2)}, u32[]{:S(2)}) async-start(bf16[32,40,128]{2,1,0:T(8,128)(2,1)} %get-tuple-element.48), calls=%async_computation.4 | async-start | bytes 655360 | tf_op jit(solution)/shard_map/all_to_all | solution.py:568
  136.2 0.1 multiply_reduce_fusion
  136.3 1.2 fusion.28
  137.9 6.9 %multiply_add_fusion = f32[3,64,64,128]{3,2,1,0:T(8,128)} fusion(f32[3,64,64,128]{3,2,1,0:T(8,128)} %refs_6_.2, f32[3,64,128]{2,1,0:T(8,128)S(1)} %broadcast_bitcast_fusion, f32[3,64,64]{2,1,0:T(8,128)S(1)} %mul.127, f32[3,64]{1,0:T(4,128)S(1)} %get-tuple-element.50), kind=kLoop, calls=%fused_computation | loop fusion | flops 4718592 | bytes 12731136 | tf_op jit(solution)/shard_map/add | solution.py:576
  144.8 0.8 pad_maximum_fusion.1
  145.6 14.7 %all-to-all-done.4 = bf16[32,40,128]{2,1,0:T(8,128)(2,1)S(1)} async-done(((bf16[32,40,128]{2,1,0:T(8,128)(2,1)}), bf16[32,40,128]{2,1,0:T(8,128)(2,1)S(1)}, u32[]{:S(2)}, u32[]{:S(2)}) %all-to-all-start.4) | async-done | bytes 327712 | tf_op jit(solution)/shard_map/all_to_all | solution.py:568
  160.5 0.2 fusion.23
  160.7 0.2 fusion
  161.0 1.0 fusion.1
  (31 shorter events, 0.7 us)
Async XLA Ops:
  0.6 160.4 %copy-start = (bf16[512,2048]{1,0:T(8,128)(2,1)S(1)}, bf16[512,2048]{1,0:T(8,128)(2,1)}, u32[]{:S(2)}) copy-start(bf16[512,2048]{1,0:T(8,128)(2,1)} %param.51) | copy-start | bytes 6291460
  2.2 29.8 %all-to-all-start = ((bf16[8,48,128]{2,1,0:T(8,128)(2,1)}), bf16[8,48,128]{2,1,0:T(8,128)(2,1)S(1)}, u32[]{:S(2)}, u32[]{:S(2)}) async-start(bf16[8,48,128]{2,1,0:T(8,128)(2,1)} %open_rows.1), calls=%async_computation | async-start | bytes 196608 | tf_op jit(solution)/shard_map/all_to_all | solution.py:474
  43.6 82.8 %copy-start.1 = (bf16[3584,128]{1,0:T(8,128)(2,1)}, bf16[3584,128]{1,0:T(8,128)(2,1)S(1)}, u32[]{:S(2)}) copy-start(bf16[3584,128]{1,0:T(8,128)(2,1)S(1)} %all-gather) | copy-start | bytes 2752516
  46.6 17.2 %all-to-all-start.1 = ((bf16[32,8,128]{2,1,0:T(8,128)(2,1)}), bf16[32,8,128]{2,1,0:T(8,128)(2,1)S(1)}, u32[]{:S(2)}, u32[]{:S(2)}) async-start(bf16[32,8,128]{2,1,0:T(8,128)(2,1)} %get-tuple-element.33), calls=%async_computation.1 | async-start | bytes 131072 | tf_op jit(solution)/shard_map/all_to_all | solution.py:503
  68.8 67.2 %copy-start.4 = (s32[3,6]{1,0:T(4,128)S(1)}, s32[3,6]{1,0:T(4,128)}, u32[]{:S(2)}) copy-start(s32[3,6]{1,0:T(4,128)} %refs_1_.1) | copy-start | bytes 220
  68.8 67.5 %copy-start.3 = (f32[2048]{0:T(1024)S(1)}, f32[2048]{0:T(1024)}, u32[]{:S(2)}) copy-start(f32[2048]{0:T(1024)} %param.43) | copy-start | bytes 24580
  86.6 51.1 %copy-start.2 = (bf16[3,3,6144]{2,1,0:T(4,128)(2,1)S(1)}, bf16[3,3,6144]{2,1,0:T(4,128)(2,1)}, u32[]{:S(2)}) copy-start(bf16[3,3,6144]{2,1,0:T(4,128)(2,1)} %param.27) | copy-start | bytes 331780
  131.8 28.5 %all-to-all-start.4 = ((bf16[32,40,128]{2,1,0:T(8,128)(2,1)}), bf16[32,40,128]{2,1,0:T(8,128)(2,1)S(1)}, u32[]{:S(2)}, u32[]{:S(2)}) async-start(bf16[32,40,128]{2,1,0:T(8,128)(2,1)} %get-tuple-element.48), calls=%async_computation.4 | async-start | bytes 655360 | tf_op jit(solution)/shard_map/all_to_all | solution.py:568
